TPU v7x, 1024 devices: a whole 8x8x8 slice. The times are simulated.
1024 devices in a mesh: ep: 64 (over z, y), tp: 16 (over x, core).
Axes of the slice: x: 8, y: 8, z: 8, core: 2. Of those that a mesh axis runs over, the one named last changes fastest.
Arguments:
- tokens: bfloat16 [8192, 2048], P('ep'), may hold values from -6 to 6
- norm_gain: float32 [2048], replicated, may hold values from 0.1 to 1.9
- expert_ids: int32 [8192, 6], P('ep'), may hold values from 0 to 511, all different within a row; in each aligned block of 128 rows (0 to 127, 128 to 255, ...) at most 2 rows name the same one
- route_weights: float32 [8192, 6], P('ep'), may hold values from 0.1 to 1
- expert_gate: bfloat16 [1024, 2048, 256], P(('ep', 'tp')), may hold values from -0.125 to 0.125
- expert_up: bfloat16 [1024, 2048, 256], P(('ep', 'tp')), may hold values from -0.125 to 0.125
- expert_down: bfloat16 [1024, 256, 2048], P(('ep', 'tp')), may hold values from -0.25 to 0.25
- shared_gate: bfloat16 [2048, 512], P(None, 'tp'), may hold values from -0.125 to 0.125
- shared_up: bfloat16 [2048, 512], P(None, 'tp'), may hold values from -0.125 to 0.125
- shared_down: bfloat16 [512, 2048], P(None, 'tp'), may hold values from -0.25 to 0.25
Outputs:
- mixed: bfloat16 [8192, 2048], P('ep', 'tp')
Inputs may be any that keep to these rules, and one draw needn't show every extreme that they name: `expert_ids`: each row names 6 different experts. In each aligned block of 128 rows (the rows of one index of ep) no expert is named by more than 2 rows, a bound that some block reaches.
All inputs are finite; a program needn't handle non-finite values.
Results may differ from a plain program's by a relative error of at most 0.0073.
Values may be sent and summed in bfloat16 or wider, within the bound.
No kernel may reach another device: no remote copies, remote signals or barrier semaphores. Data moves between devices by JAX's collectives and lax.ppermute only.
A program may use at most 32 MiB of HBM per device.

v0:
```python
import jax
import jax.numpy as jnp
from jax import lax
from jax.sharding import Mesh
from jax.sharding import PartitionSpec as P

TP = ("tp_0", "tp_1")
EP_TP = ("ep", "tp_0", "tp_1")


NORM_EPSILON = 1e-06


def swapped(block, axis, distance):
    count = lax.axis_size(axis)
    route = []
    for low in range(count):
        high = low | 1 << distance
        if high != low and high < count:
            route += [(low, high), (high, low)]
    return lax.ppermute(block, axis, route)


def cut_along(shard, dim, length):
    lengths = shard.shape
    parts = shard.reshape(*lengths[:dim], length, lengths[dim] // length, *lengths[dim + 1 :])
    return jnp.moveaxis(parts, dim, 0)


def laid_out(parts, dim):
    parts = jnp.moveaxis(parts, 0, dim)
    lengths = parts.shape
    return parts.reshape(*lengths[:dim], lengths[dim] * lengths[dim + 1], *lengths[dim + 2 :])


def moved_by_axis(parts, axes, turns):
    lengths = [lax.axis_size(a) for a in axes]
    parts = parts.reshape(*lengths, *parts.shape[1:])
    for k in turns:
        parts = lax.all_to_all(parts, axes[k], split_axis=k, concat_axis=k, tiled=True)
    return parts.reshape(-1, *parts.shape[len(axes) :])


def one_axis_at_a_time(shard, axes, turns, split_dim, concat_dim):
    parts = cut_along(shard, split_dim, lax.axis_size(axes))
    return laid_out(moved_by_axis(parts, axes, turns), concat_dim)


def local(
    tokens,
    norm_gain,
    expert_ids,
    route_weights,
    expert_gate,
    expert_up,
    expert_down,
    shared_gate,
    shared_up,
    shared_down,
):
    ep_count = lax.axis_size("ep")
    tp_count = lax.axis_size(TP)
    pair_count = tp_count // 2
    tp_index = lax.axis_index(TP)
    column = tp_index // 2
    half_index = tp_index % 2
    token_count, model_width = tokens.shape
    top_count = expert_ids.shape[1]
    expert_count = ep_count * pair_count
    capacity = 2 * max(1, token_count * top_count // expert_count)
    half_cap = capacity // 2
    as_float = tokens.astype(jnp.float32)
    inverse_rms = lax.rsqrt(jnp.mean(as_float * as_float, axis=-1, keepdims=True) + NORM_EPSILON)
    normed = (as_float * inverse_rms * norm_gain).astype(jnp.bfloat16)
    expert_iota = jnp.arange(expert_count, dtype=jnp.int32)
    token_iota = jnp.arange(token_count, dtype=jnp.int32)
    counts = jnp.sum(
        (expert_ids[:, :, None] == expert_iota[None, None, :]).astype(jnp.bfloat16), axis=1
    )
    strict_lower = (token_iota[:, None] > token_iota[None, :]).astype(jnp.bfloat16)
    prefix = jnp.dot(strict_lower, counts, preferred_element_type=jnp.float32)
    slot_index = jnp.take_along_axis(prefix, expert_ids, axis=1).astype(jnp.int32)
    target = expert_ids // pair_count
    owner_column = expert_ids % pair_count
    is_mine = owner_column == column
    position = target * capacity + slot_index
    slot_iota = jnp.arange(ep_count * capacity, dtype=jnp.int32)
    matches = is_mine[None, :, :] & (position[None, :, :] == slot_iota[:, None, None])
    slot_taken = jnp.any(matches, axis=2)
    token_of_slot = jnp.sum(jnp.where(slot_taken, token_iota[None, :], 0), axis=1)
    filled = jnp.any(slot_taken, axis=1)
    buffer = jnp.where(
        filled[:, None], jnp.take(normed, token_of_slot, axis=0), jnp.zeros((), jnp.bfloat16)
    )
    buffer = buffer.reshape(ep_count, capacity, model_width)
    gate_local = expert_gate[0]
    up_local = expert_up[0]
    down_local = expert_down[0]
    received = lax.all_to_all(buffer, "ep", split_axis=0, concat_axis=0, tiled=True)
    flat_rows = received.reshape(-1, model_width)
    hidden = (
        jax.nn.silu(jnp.dot(flat_rows, gate_local, preferred_element_type=jnp.float32))
        * jnp.dot(flat_rows, up_local, preferred_element_type=jnp.float32)
    ).astype(jnp.bfloat16)
    partial_out = jnp.dot(hidden, down_local, preferred_element_type=jnp.float32).astype(
        jnp.bfloat16
    )
    partial_out = partial_out.reshape(received.shape[0], received.shape[1], model_width)
    kept_part = lax.dynamic_slice_in_dim(partial_out, half_index * half_cap, half_cap, 1)
    other_part = lax.dynamic_slice_in_dim(partial_out, (1 - half_index) * half_cap, half_cap, 1)
    partner_part = swapped(other_part, TP, 0)
    expert_out = (kept_part.astype(jnp.float32) + partner_part.astype(jnp.float32)).astype(
        jnp.bfloat16
    )
    returned = lax.all_to_all(expert_out, "ep", split_axis=0, concat_axis=0, tiled=True)
    pieces = one_axis_at_a_time(
        returned.reshape(1, ep_count * half_cap, model_width), TP, (1, 0), 2, 0
    )
    flat_rows = pieces.reshape(tp_count * ep_count * half_cap, model_width // tp_count)
    source = 2 * owner_column + slot_index // half_cap
    row_index = source * (ep_count * half_cap) + target * half_cap + slot_index % half_cap
    picked = jnp.take(flat_rows, row_index, axis=0).astype(jnp.float32)
    routed = jnp.sum(picked * route_weights[:, :, None], axis=1)
    shared_act = (
        jax.nn.silu(jnp.dot(normed, shared_gate, preferred_element_type=jnp.float32))
        * jnp.dot(normed, shared_up, preferred_element_type=jnp.float32)
    ).astype(jnp.bfloat16)
    shared_out = jnp.dot(
        lax.all_gather(shared_act, TP, axis=1, tiled=True),
        shared_down,
        preferred_element_type=jnp.float32,
    )
    return (routed + shared_out).astype(jnp.bfloat16)


def solution(mesh):
    finer = Mesh(mesh.devices.reshape(mesh.shape["ep"], 8, 2), ("ep", "tp_0", "tp_1"))
    in_specs = (
        P("ep", None),
        P(),
        P("ep", None),
        P("ep", None),
        P(EP_TP, None, None),
        P(EP_TP, None, None),
        P(EP_TP, None, None),
        P(None, TP),
        P(None, TP),
        P(None, TP),
    )
    out_specs = P("ep", TP)
    return jax.shard_map(local, mesh=finer, in_specs=in_specs, out_specs=out_specs, check_vma=False)
```

profile of v0, /device:TPU:1, one launch (start us, length us, event | category | flops | bytes accessed | tf_op | source)
XLA Modules:
  0.0 123.8 jit_solution(16259322290102595430)
XLA Ops:
  0.0 0.0 copy-start
  0.0 0.8 bitcast_or_fusion
  0.8 0.9 fusion.12
  1.7 0.1 copy.60
  1.8 0.1 reshape.87
  2.0 0.2 fusion.22
  2.1 0.0 copy-start.5
  2.2 0.0 copy-start.1
  2.2 0.0 copy-start.6
  2.2 6.3 %gather_fusion.2 = f32[768]{0:T(1024)S(1)} fusion(f32[128,512]{1,0:T(8,128)S(1)} %fusion.22, s32[768]{0:T(1024)S(1)} %reshape.87), kind=kCustom, calls=%fused_computation.2 | custom fusion | bytes 12288 | tf_op jit(solution)/shard_map/jit(take_along_axis)/gather | solution.py:82
  8.5 0.1 reshape.90
  8.6 0.1 copy.61
  8.7 0.0 copy-done.5
  8.8 0.1 fusion.14
  8.9 0.1 select_reduce_fusion
  9.0 0.1 reduce_sum.45
  9.2 0.0 copy-done.1
  9.2 0.2 fusion.4
  9.4 0.2 broadcast_in_dim.64
  9.6 0.0 copy-done.6
  9.6 0.2 fusion.6
  9.8 0.9 gather_fusion
  10.7 0.3 gather.16
  11.0 1.6 %broadcast_select_fusion.1 = bf16[64,2,2048]{2,1,0:T(2,128)(2,1)} fusion(pred[64,2]{1,0:T(8,128)(4,1)S(1)} %broadcast_in_dim.64, bf16[64,2,2048]{2,1,0:T(2,128)(2,1)S(1)} %gather.16, pred[64,2]{1,0:T(8,128)(4,1)S(1)} %compare_and_fusion), kind=kLoop, calls=%fused_computation.22 | loop fusion | flops 524288 | bytes 1048832 | tf_op jit(solution)/shard_map/jit(_where)/select_n | solution.py:92
  12.6 23.9 %all-to-all-start = ((bf16[64,2,2048]{2,1,0:T(2,128)(2,1)}), bf16[64,2,2048]{2,1,0:T(2,128)(2,1)S(1)}, u32[]{:S(2)}, u32[]{:S(2)}) async-start(bf16[64,2,2048]{2,1,0:T(2,128)(2,1)} %broadcast_select_fusion.1), calls=%async_computation | async-start | bytes 1048576 | tf_op jit(solution)/shard_map/all_to_all | solution.py:99
  36.6 17.4 %all-to-all-done = bf16[64,2,2048]{2,1,0:T(2,128)(2,1)S(1)} async-done(((bf16[64,2,2048]{2,1,0:T(2,128)(2,1)}), bf16[64,2,2048]{2,1,0:T(2,128)(2,1)S(1)}, u32[]{:S(2)}, u32[]{:S(2)}) %all-to-all-start) | async-done | bytes 524320 | tf_op jit(solution)/shard_map/all_to_all | solution.py:99
  54.0 0.2 reshape.68
  54.2 1.5 %fusion.10 = f32[128,256]{1,0:T(8,128)S(1)} fusion(bf16[128,2048]{1,0:T(8,128)(2,1)S(1)} %reshape.68, bf16[1,2048,256]{2,1,0:T(8,128)(2,1)} %param.14), kind=kOutput, calls=%fused_computation.19 | convolution fusion | flops 134217728 | bytes 1703936 | tf_op jit(solution)/shard_map/dot_general | solution.py:102
  55.7 0.0 copy-done
  55.7 2.0 %convolution_convert_fusion = bf16[128,2048]{1,0:T(8,128)(2,1)S(1)} fusion(bf16[128,2048]{1,0:T(8,128)(2,1)S(1)} %reshape.68, bf16[1,256,2048]{2,1,0:T(8,128)(2,1)S(1)} %copy-done, bf16[1,2048,256]{2,1,0:T(8,128)(2,1)} %param.15, f32[128,256]{1,0:T(8,128)S(1)} %fusion.10), kind=kOutput, calls=%fused_computation.3 | convolution fusion | flops 268894208 | bytes 3276800 | tf_op jit(solution)/shard_map/dot_general | solution.py:105
  57.8 0.3 reshape.69
  58.1 1.1 constant_dynamic-slice_fusion.1
  59.2 0.2 copy.71
  59.4 5.2 %collective-permute-start = (bf16[64,1,2048]{2,0,1:T(8,128)(2,1)S(1)}, bf16[64,1,2048]{2,0,1:T(8,128)(2,1)S(1)}, u32[]{:S(2)}, u32[]{:S(2)}) collective-permute-start(bf16[64,1,2048]{2,0,1:T(8,128)(2,1)S(1)} %copy.71), channel_id=1, source_target_pairs={{0,1},{1,0},{2,3},{3,2},{4,5},{5,4},{6,7},{7,6},{8,9},{9,8},{10,11... | collective-permute-start | bytes 786440 | tf_op jit(solution)/shard_map/ppermute | solution.py:21
  64.5 1.1 collective-permute-done
  65.7 0.2 add_convert_fusion
  65.9 0.5 broadcast.157
  66.4 0.8 reduce.3
  67.1 0.2 reshape.101
  67.3 17.6 %all_to_all.20 = bf16[64,2,1024]{2,1,0:T(2,128)(2,1)S(1)} all-to-all(bf16[64,2,1024]{2,1,0:T(2,128)(2,1)S(1)} %reshape.101), channel_id=1, replica_groups=mesh['ep'=64,'tp_0'=8,'tp_1'=2] {'ep'}, dimensions={0} | all-to-all | bytes 524288 | tf_op jit(solution)/shard_map/all_to_all | solution.py:115
  84.9 0.2 reshape.102
  85.2 1.5 %reduce.2 = bf16[64,2048]{1,0:T(8,128)(2,1)S(1)} reduce(bf16[64,1,2048]{2,1,0:T(2,128)(2,1)S(1)} %reshape.102, bf16[]{:T(256)} %constant.156), dimensions={1}, to_apply=%all_to_all.13.reduce_sub_computation | reduce | bytes 524290 | tf_op jit(solution)/shard_map/all_to_all | solution.py:115
  86.7 0.0 copy-start.2
  86.7 0.1 copy.66
  86.8 0.0 copy-start.7
  86.8 6.4 %all_to_all.21 = bf16[8,2,1,64,128]{4,3,0,2,1:T(8,128)(2,1)S(1)} all-to-all(bf16[8,2,1,64,128]{4,3,0,2,1:T(8,128)(2,1)S(1)} %copy.66), channel_id=1, replica_groups=mesh['ep'=64,'tp_0'=8,'tp_1'=2] {'tp_1'}, dimensions={1} | all-to-all | bytes 524288 | tf_op jit(solution)/shard_map/all_to_all | solution.py:40
  93.2 0.7 copy.67
  93.9 6.5 %all-to-all-start.3 = ((bf16[8,2,1,64,128]{4,3,1,2,0:T(8,128)(2,1)}), bf16[8,2,1,64,128]{4,3,1,2,0:T(8,128)(2,1)S(1)}, u32[]{:S(2)}, u32[]{:S(2)}) async-start(bf16[8,2,1,64,128]{4,3,1,2,0:T(8,128)(2,1)} %copy.67), calls=%async_computation.3 | async-start | bytes 524288 | tf_op jit(solution)/shard_map/all_to_all | solution.py:40
  100.4 0.0 copy-done.2
  100.4 0.3 fusion.27
  100.6 0.0 copy-done.7
  100.7 0.1 copy.69
  100.8 0.1 copy.62
  100.9 0.1 copy.68
  101.0 0.1 reshape.81
  101.2 0.0 copy-done.3
  101.2 0.3 fusion.3
  101.5 19.2 %all_gather.3 = bf16[128,512]{0,1:T(8,128)(2,1)S(1)} all-gather(bf16[128,32]{0,1:T(8,128)(2,1)S(1)} %fusion.3), channel_id=1, replica_groups=mesh['ep'=64,'tp_0'=8,'tp_1'=2] {'tp_0','tp_1'}, dimensions={1}, use_global_device_ids=true | all-gather | bytes 139264 | tf_op jit(solution)/shard_map/all_gather | solution.py:129
  120.6 0.0 all-to-all-done.3
  120.6 0.0 copy-start.4
  120.6 1.9 %gather_fusion.1 = bf16[768,128]{1,0:T(8,128)(2,1)S(1)} fusion(bf16[1024,128]{1,0:T(8,128)(2,1)S(1)} %bitcast.35, s32[1024]{0:T(1024)S(1)} %pad_clamp_fusion), kind=kCustom, calls=%fused_computation.1 | custom fusion | bytes 396288 | tf_op jit(solution)/shard_map/jit(_take)/gather | solution.py:122
  122.5 0.1 reshape.80
  122.6 0.3 multiply_reduce_fusion
  123.0 0.8 fusion.2
  (10 shorter events, 0.1 us)
Async XLA Ops:
  0.0 55.7 %copy-start = (bf16[1,256,2048]{2,1,0:T(8,128)(2,1)S(1)}, bf16[1,256,2048]{2,1,0:T(8,128)(2,1)}, u32[]{:S(2)}) copy-start(bf16[1,256,2048]{2,1,0:T(8,128)(2,1)} %param.16) | copy-start | bytes 3145732
  2.1 6.5 %copy-start.5 = (s32[128,6]{0,1:T(8,128)S(1)}, s32[128,6]{0,1:T(8,128)}, u32[]{:S(2)}) copy-start(s32[128,6]{0,1:T(8,128)} %param.12) | copy-start | bytes 9220
  2.2 7.0 %copy-start.1 = (bf16[128,2048]{1,0:T(8,128)(2,1)S(1)}, bf16[128,2048]{1,0:T(8,128)(2,1)}, u32[]{:S(2)}) copy-start(bf16[128,2048]{1,0:T(8,128)(2,1)} %param.10) | copy-start | bytes 1572868
  2.2 7.4 %copy-start.6 = (f32[2048]{0:T(1024)S(1)}, f32[2048]{0:T(1024)}, u32[]{:S(2)}) copy-start(f32[2048]{0:T(1024)} %param.11) | copy-start | bytes 24580
  12.6 41.4 %all-to-all-start = ((bf16[64,2,2048]{2,1,0:T(2,128)(2,1)}), bf16[64,2,2048]{2,1,0:T(2,128)(2,1)S(1)}, u32[]{:S(2)}, u32[]{:S(2)}) async-start(bf16[64,2,2048]{2,1,0:T(2,128)(2,1)} %broadcast_select_fusion.1), calls=%async_computation | async-start | bytes 1048576 | tf_op jit(solution)/shard_map/all_to_all | solution.py:99
  59.4 6.3 %collective-permute-start = (bf16[64,1,2048]{2,0,1:T(8,128)(2,1)S(1)}, bf16[64,1,2048]{2,0,1:T(8,128)(2,1)S(1)}, u32[]{:S(2)}, u32[]{:S(2)}) collective-permute-start(bf16[64,1,2048]{2,0,1:T(8,128)(2,1)S(1)} %copy.71), channel_id=1, source_target_pairs={{0,1},{1,0},{2,3},{3,2},{4,5},{5,4},{6,7},{7,6},{8,9},{9,8},{10,11... | collective-permute-start | bytes 786440 | tf_op jit(solution)/shard_map/ppermute | solution.py:21
  86.7 13.6 %copy-start.2 = (bf16[2048,32]{0,1:T(8,128)(2,1)S(1)}, bf16[2048,32]{0,1:T(8,128)(2,1)}, u32[]{:S(2)}) copy-start(bf16[2048,32]{0,1:T(8,128)(2,1)} %param.17) | copy-start | bytes 393220
  86.8 13.8 %copy-start.7 = (f32[128,6]{0,1:T(8,128)S(1)}, f32[128,6]{0,1:T(8,128)}, u32[]{:S(2)}) copy-start(f32[128,6]{0,1:T(8,128)} %param.13) | copy-start | bytes 9220
  93.2 8.0 %copy-start.3 = (bf16[2048,32]{0,1:T(8,128)(2,1)S(1)}, bf16[2048,32]{0,1:T(8,128)(2,1)}, u32[]{:S(2)}) copy-start(bf16[2048,32]{0,1:T(8,128)(2,1)} %param.18) | copy-start | bytes 393220
  93.9 26.7 %all-to-all-start.3 = ((bf16[8,2,1,64,128]{4,3,1,2,0:T(8,128)(2,1)}), bf16[8,2,1,64,128]{4,3,1,2,0:T(8,128)(2,1)S(1)}, u32[]{:S(2)}, u32[]{:S(2)}) async-start(bf16[8,2,1,64,128]{4,3,1,2,0:T(8,128)(2,1)} %copy.67), calls=%async_computation.3 | async-start | bytes 524288 | tf_op jit(solution)/shard_map/all_to_all | solution.py:40
  120.6 2.3 %copy-start.4 = (bf16[512,128]{1,0:T(8,128)(2,1)S(1)}, bf16[512,128]{1,0:T(8,128)(2,1)}, u32[]{:S(2)}) copy-start(bf16[512,128]{1,0:T(8,128)(2,1)} %param.19) | copy-start | bytes 393220
where the time goes:
time: 124 us
  blocking collectives  43.1 us (35%)
  starting transfers between devices  35.6 us (29%)
  waiting for transfers between devices  18.5 us (15%)
  local copies, waits for them, and re-layouts  14.3 us (12%)
  other arithmetic  6.82 us (6%)
  matrix products  5.1 us (4%)
    all_to_all x1, starting transfers between devices, local(): lax.all_to_all(buffer, 'ep', split_axis=0, concat_axis=0, tiled=True)  23.9 us
    all_gather x1, blocking collectives, local(): lax.all_gather(shared_act, TP, axis=1, tiled=True)  19.2 us
    all_to_all x1, blocking collectives, local(): lax.all_to_all(expert_out, 'ep', split_axis=0, concat_axis=0, tiled=True)  17.6 us
    all_to_all x1, waiting for transfers between devices, local(): lax.all_to_all(buffer, 'ep', split_axis=0, concat_axis=0, tiled=True)  17.4 us
    gather x5, local copies, waits for them, and re-layouts, local(): jnp.take_along_axis(prefix, expert_ids, axis=1).astype(jnp.int32)  6.72 us
    all_to_all x1, starting transfers between devices, moved_by_axis(): lax.all_to_all(parts, axes[k], split_axis=k, concat_axis=k, tiled=True)  6.48 us
    all_to_all x1, blocking collectives, moved_by_axis(): lax.all_to_all(parts, axes[k], split_axis=k, concat_axis=k, tiled=True)  6.35 us
    ppermute x1, starting transfers between devices, swapped(): return lax.ppermute(block, axis, route)  5.17 us
  transfers between devices with their start and end apart: 3, of which 2 were waited for; matrix products, arithmetic and copies ran while one was open for 1% of the time, Pallas kernels for 0%

commit v1 on v0

v1 whole, which is shorter than its diff:
```python
import jax
import jax.numpy as jnp
from jax import lax
from jax.sharding import Mesh
from jax.sharding import PartitionSpec as P

TP = ("x", "core")
EP = ("z", "y")
ALL = ("z", "y", "x", "core")

NORM_EPSILON = 1e-06


def dot(a, b, dims=((1,), (0,))):
    return lax.dot_general(a, b, (dims, ((), ())), preferred_element_type=jnp.float32)


def local(
    tokens,
    norm_gain,
    expert_ids,
    route_weights,
    expert_gate,
    expert_up,
    expert_down,
    shared_gate,
    shared_up,
    shared_down,
):
    groups = lax.axis_size(EP)
    columns = lax.axis_size("x")
    cores = lax.axis_size("core")
    column = lax.axis_index("x")
    core = lax.axis_index("core")
    rows, width = tokens.shape
    top_count = expert_ids.shape[1]
    cap = 2
    slots = groups * cap
    block = width // (columns * cores)

    as_float = tokens.astype(jnp.float32)
    inverse_rms = lax.rsqrt(jnp.mean(as_float * as_float, axis=-1, keepdims=True) + NORM_EPSILON)
    normed = (as_float * inverse_rms * norm_gain).astype(jnp.bfloat16)

    token_iota = jnp.arange(rows, dtype=jnp.int32)
    strict_lower = (token_iota[:, None] > token_iota[None, :]).astype(jnp.bfloat16)

    slot_iota = jnp.arange(slots, dtype=jnp.int32)
    slot_expert = (slot_iota // cap) * columns + column
    named = jnp.zeros((rows, slots), jnp.bool_)
    for k in range(top_count):
        named = named | (expert_ids[:, k : k + 1] == slot_expert[None, :])
    earlier = dot(strict_lower, named.astype(jnp.bfloat16))
    chosen = named & (earlier == (slot_iota % cap).astype(jnp.float32)[None, :])
    buffer = dot(chosen.astype(jnp.bfloat16), normed, ((0,), (0,))).astype(jnp.bfloat16)
    buffer = buffer.reshape(groups, cap, width)
    received = lax.all_to_all(buffer, EP, split_axis=0, concat_axis=0, tiled=True)

    shared_act = (
        jax.nn.silu(dot(shared_gate, normed, ((0,), (1,)))) * dot(shared_up, normed, ((0,), (1,)))
    ).astype(jnp.bfloat16)
    other_act = lax.ppermute(shared_act, "core", [(0, 1), (1, 0)])
    pair_act = jnp.where(
        core == 0,
        jnp.concatenate([shared_act, other_act], 0),
        jnp.concatenate([other_act, shared_act], 0),
    )

    all_iota = jnp.arange(columns * groups, dtype=jnp.int32)
    all_expert = (all_iota % groups) * columns + all_iota // groups
    weight = jnp.zeros((rows, columns * groups), jnp.float32)
    taken = jnp.zeros((rows, columns * groups), jnp.bool_)
    for k in range(top_count):
        hit = expert_ids[:, k : k + 1] == all_expert[None, :]
        taken = taken | hit
        weight = jnp.where(hit, route_weights[:, k : k + 1], weight)
    ahead = dot(strict_lower, taken.astype(jnp.bfloat16))

    flat_rows = received.reshape(slots, width)
    hidden = (
        jax.nn.silu(dot(flat_rows, expert_gate[0])) * dot(flat_rows, expert_up[0])
    ).astype(jnp.bfloat16)
    down = expert_down[0].reshape(-1, columns, cores, block)
    down_kept = lax.dynamic_index_in_dim(down, core, 2, keepdims=False).reshape(-1, width // cores)
    down_sent = lax.dynamic_index_in_dim(down, 1 - core, 2, keepdims=False).reshape(-1, width // cores)
    sent = dot(hidden, down_sent).astype(jnp.bfloat16)
    partner = lax.ppermute(sent, "core", [(0, 1), (1, 0)])
    kept = dot(hidden, down_kept).astype(jnp.bfloat16)
    expert_out = (kept.astype(jnp.float32) + partner.astype(jnp.float32)).astype(jnp.bfloat16)
    returned = lax.all_to_all(
        expert_out.reshape(groups, cap, columns * block), EP, split_axis=0, concat_axis=0, tiled=True
    )
    by_column = jnp.moveaxis(returned.reshape(slots, columns, block), 1, 0)
    payload = jnp.concatenate(
        [by_column, jnp.broadcast_to(pair_act[None], (columns,) + pair_act.shape)], axis=1
    )
    gathered = lax.all_to_all(payload, "x", split_axis=0, concat_axis=0, tiled=True)
    picked = gathered[:, :slots].reshape(columns, groups, cap, block)
    high = lax.reduce_precision(weight, 8, 7)
    low = weight - high
    routed = jnp.zeros((rows, block), jnp.float32)
    for s in range(cap):
        values = picked[:, :, s].reshape(columns * groups, block)
        here = ahead == s
        for part in (high, low):
            routed = routed + dot(jnp.where(here, part, 0.0).astype(jnp.bfloat16), values)
    act = gathered[:, slots:].reshape(-1, rows)
    shared_out = dot(act, shared_down, ((0,), (0,)))
    return (routed + shared_out).astype(jnp.bfloat16)


def solution(mesh):
    ep = mesh.shape["ep"]
    tp = mesh.shape["tp"]
    finer = Mesh(mesh.devices.reshape(8, ep // 8, tp // 2, 2), ALL)
    in_specs = (
        P(EP, None),
        P(),
        P(EP, None),
        P(EP, None),
        P(ALL, None, None),
        P(ALL, None, None),
        P(ALL, None, None),
        P(None, TP),
        P(None, TP),
        P(None, TP),
    )
    out_specs = P(EP, TP)
    return jax.shard_map(local, mesh=finer, in_specs=in_specs, out_specs=out_specs, check_vma=False)
```

time: 124 us -> 100 us (0.81)
  the two profiles are of different devices: /device:TPU:1 before, /device:TPU:16 now
where the time goes in v1:
time: 100 us; the launch traced here: 99.5 us
  waiting for transfers between devices  41.9 us (42%)
  starting transfers between devices  39.4 us (39%)
  local copies, waits for them, and re-layouts  11.1 us (11%)
  matrix products  5.45 us (5%)
  other arithmetic  1.29 us (1%)
    all_to_all x1, starting transfers between devices, local(): lax.all_to_all(buffer, EP, split_axis=0, concat_axis=0, tiled=True)  23.3 us
    all_to_all x1, waiting for transfers between devices, local(): lax.all_to_all(buffer, EP, split_axis=0, concat_axis=0, tiled=True)  17 us
    all_to_all x1, waiting for transfers between devices, local(): lax.all_to_all(payload, 'x', split_axis=0, concat_axis=0, tiled=True)  12 us
    all_to_all x1, waiting for transfers between devices, local(): lax.all_to_all(expert_out.reshape(groups, cap, columns * block), EP, spli...  10.3 us
    all_to_all x1, starting transfers between devices, local(): lax.all_to_all(payload, 'x', split_axis=0, concat_axis=0, tiled=True)  6.89 us
    unnamed x30, local copies, waits for them, and re-layouts  6.05 us
    dot_general x13, matrix products, dot(): lax.dot_general(a, b, (dims, ((), ())), preferred_element_type=jnp.float32)  5.45 us
    all_to_all x1, starting transfers between devices, local(): lax.all_to_all(expert_out.reshape(groups, cap, columns * block), EP, spli...  5.42 us
  transfers between devices with their start and end apart: 5, of which 5 were waited for; matrix products, arithmetic and copies ran while one was open for 4% of the time, Pallas kernels for 0%

profile of v1, /device:TPU:16, one launch (start us, length us, event | category | flops | bytes accessed | tf_op | source)
XLA Modules:
  0.0 99.5 jit_solution(4862122683130662176)
XLA Ops:
  0.0 0.0 copy-start
  0.0 0.0 copy-start.2
  0.0 0.9 slice_bitcast_fusion.11
  0.9 0.0 copy-start.6
  0.9 0.0 copy-start.8
  0.9 1.2 %fusion.6 = f32[128]{0:T(128)S(1)} fusion(bf16[128,2048]{1,0:T(8,128)(2,1)} %param.10), kind=kLoop, calls=%fused_computation.19 | loop fusion | flops 786304 | bytes 524800 | tf_op jit(solution)/shard_map/reduce_sum | solution.py:42
  2.2 0.0 copy-start.13
  2.2 0.0 copy-done.6
  2.2 0.0 copy-done.8
  2.2 0.0 copy-done.2
  2.2 0.7 copy-done.13
  2.9 0.6 convolution_convert_fusion
  3.5 1.1 %reshape.111 = bf16[64,2,2048]{2,1,0:T(2,128)(2,1)} reshape(bf16[128,2048]{1,0:T(8,128)(2,1)S(1)} %convolution_convert_fusion) | data formatting | bytes 1048576 | tf_op jit(solution)/shard_map/reshape | solution.py:56
  4.7 23.3 %all-to-all-start = ((bf16[64,2,2048]{2,1,0:T(2,128)(2,1)}), bf16[64,2,2048]{2,1,0:T(2,128)(2,1)S(1)}, u32[]{:S(2)}, u32[]{:S(2)}) async-start(bf16[64,2,2048]{2,1,0:T(2,128)(2,1)} %reshape.111), calls=%async_computation | async-start | bytes 1048576 | tf_op jit(solution)/shard_map/all_to_all | solution.py:57
  28.0 1.5 %copy.15 = bf16[1,256,2048]{1,2,0:T(8,128)(2,1)S(1)} copy(bf16[1,256,2048]{2,1,0:T(8,128)(2,1)} %param.16) | data formatting | bytes 2097152 | tf_op args[6]
  29.5 0.9 constant_dynamic-slice_fusion
  30.4 17.0 %all-to-all-done = bf16[64,2,2048]{2,1,0:T(2,128)(2,1)S(1)} async-done(((bf16[64,2,2048]{2,1,0:T(2,128)(2,1)}), bf16[64,2,2048]{2,1,0:T(2,128)(2,1)S(1)}, u32[]{:S(2)}, u32[]{:S(2)}) %all-to-all-start) | async-done | bytes 524320 | tf_op jit(solution)/shard_map/all_to_all | solution.py:57
  47.4 0.2 reshape.112
  47.6 0.0 copy-done
  47.6 0.0 copy-start.10
  47.6 0.3 fusion.10
  47.9 0.9 copy-done.10
  48.8 0.0 copy-start.1
  48.8 0.3 fusion.1
  49.1 0.7 copy-done.1
  49.9 0.3 convolution_convert_fusion.1
  50.2 1.9 %collective-permute-start = (bf16[128,1024]{1,0:T(8,128)(2,1)S(1)}, bf16[128,1024]{1,0:T(8,128)(2,1)S(1)}, u32[]{:S(2)}, u32[]{:S(2)}) collective-permute-start(bf16[128,1024]{1,0:T(8,128)(2,1)S(1)} %convolution_convert_fusion.1), channel_id=1, source_target_pairs={{0,1},{1,0},{2,3},{3,2},{4,5},{5,4},{6,7},{7,6},{8,9},{9,8},{10,11... | collective-permute-start | bytes 786440 | tf_op jit(solution)/shard_map/ppermute | solution.py:87
  52.1 1.5 %collective-permute-done = bf16[128,1024]{1,0:T(8,128)(2,1)S(1)} collective-permute-done((bf16[128,1024]{1,0:T(8,128)(2,1)S(1)}, bf16[128,1024]{1,0:T(8,128)(2,1)S(1)}, u32[]{:S(2)}, u32[]{:S(2)}) %collective-permute-start) | collective-permute-done | bytes 262176 | tf_op jit(solution)/shard_map/ppermute | solution.py:87
  53.6 0.3 add_convert_fusion
  53.9 0.0 copy-start.3
  53.9 0.8 reshape.115
  54.7 0.0 copy-start.11
  54.7 5.4 %all-to-all-start.1 = ((bf16[64,2,1024]{2,1,0:T(2,128)(2,1)}), bf16[64,2,1024]{2,1,0:T(2,128)(2,1)S(1)}, u32[]{:S(2)}, u32[]{:S(2)}) async-start(bf16[64,2,1024]{2,1,0:T(2,128)(2,1)} %reshape.115), calls=%async_computation.1 | async-start | bytes 524288 | tf_op jit(solution)/shard_map/all_to_all | solution.py:90
  60.2 0.0 copy-done.3
  60.2 0.0 copy-done.11
  60.2 0.0 copy-start.12
  60.2 0.3 convolution_bitcast_fusion.1
  60.5 0.5 copy-done.12
  61.1 0.4 fusion.5
  61.4 1.9 %collective-permute-start.1 = (bf16[32,128]{1,0:T(8,128)(2,1)S(1)}, bf16[32,128]{1,0:T(8,128)(2,1)S(1)}, u32[]{:S(2)}, u32[]{:S(2)}) collective-permute-start(bf16[32,128]{1,0:T(8,128)(2,1)S(1)} %fusion.5), channel_id=1, source_target_pairs={{0,1},{1,0},{2,3},{3,2},{4,5},{5,4},{6,7},{7,6},{8,9},{9,8},{10,11... | collective-permute-start | bytes 24584 | tf_op jit(solution)/shard_map/ppermute | solution.py:62
  63.4 1.1 %collective-permute-done.1 = bf16[32,128]{1,0:T(8,128)(2,1)S(1)} collective-permute-done((bf16[32,128]{1,0:T(8,128)(2,1)S(1)}, bf16[32,128]{1,0:T(8,128)(2,1)S(1)}, u32[]{:S(2)}, u32[]{:S(2)}) %collective-permute-start.1) | collective-permute-done | bytes 8224 | tf_op jit(solution)/shard_map/ppermute | solution.py:62
  64.5 10.3 %all-to-all-done.1 = bf16[64,2,1024]{2,1,0:T(2,128)(2,1)S(1)} async-done(((bf16[64,2,1024]{2,1,0:T(2,128)(2,1)}), bf16[64,2,1024]{2,1,0:T(2,128)(2,1)S(1)}, u32[]{:S(2)}, u32[]{:S(2)}) %all-to-all-start.1) | async-done | bytes 262176 | tf_op jit(solution)/shard_map/all_to_all | solution.py:90
  74.8 0.2 reshape.116
  75.0 0.8 copy.16
  75.8 0.0 copy-start.5
  75.8 6.9 %all-to-all-start.2 = ((bf16[8,192,128]{2,1,0:T(8,128)(2,1)}), bf16[8,192,128]{2,1,0:T(8,128)(2,1)S(1)}, u32[]{:S(2)}, u32[]{:S(2)}) async-start(bf16[8,192,128]{2,1,0:T(8,128)(2,1)} %copy.16), calls=%async_computation.2 | async-start | bytes 786432 | tf_op jit(solution)/shard_map/all_to_all | solution.py:97
  82.7 0.0 copy-done.5
  82.7 0.0 copy-start.7
  82.8 0.0 copy-start.9
  82.8 0.6 copy-done.7
  83.4 0.0 copy-done.9
  83.4 0.4 broadcast_compare_fusion
  83.8 12.0 %all-to-all-done.2 = bf16[8,192,128]{2,1,0:T(8,128)(2,1)S(1)} async-done(((bf16[8,192,128]{2,1,0:T(8,128)(2,1)}), bf16[8,192,128]{2,1,0:T(8,128)(2,1)S(1)}, u32[]{:S(2)}, u32[]{:S(2)}) %all-to-all-start.2) | async-done | bytes 393248 | tf_op jit(solution)/shard_map/all_to_all | solution.py:97
  95.9 0.2 copy.20
  96.1 0.4 fusion.16
  96.5 0.4 convolution_add_fusion.3
  96.9 0.4 convolution_add_fusion.2
  97.3 0.4 convolution_add_fusion.1
  97.7 0.0 copy-start.4
  97.7 0.9 copy-done.4
  98.6 0.8 fusion.2
  (12 shorter events, 0.2 us)
Async XLA Ops:
  0.0 47.6 %copy-start = (bf16[1,2048,256]{2,1,0:T(8,128)(2,1)S(1)}, bf16[1,2048,256]{2,1,0:T(8,128)(2,1)}, u32[]{:S(2)}) copy-start(bf16[1,2048,256]{2,1,0:T(8,128)(2,1)} %param.14) | copy-start | bytes 3145732
  0.0 2.2 %copy-start.2 = (bf16[128,2048]{1,0:T(8,128)(2,1)S(1)}, bf16[128,2048]{1,0:T(8,128)(2,1)}, u32[]{:S(2)}) copy-start(bf16[128,2048]{1,0:T(8,128)(2,1)} %param.10) | copy-start | bytes 1572868
  0.9 1.3 %copy-start.6 = (s32[128]{0:T(128)}, s32[128]{0:T(128)S(1)}, u32[]{:S(2)}) copy-start(s32[128]{0:T(128)S(1)} %get-tuple-element.21) | copy-start | bytes 1540
  0.9 1.3 %copy-start.8 = (s32[128]{0:T(128)}, s32[128]{0:T(128)S(1)}, u32[]{:S(2)}) copy-start(s32[128]{0:T(128)S(1)} %get-tuple-element.22) | copy-start | bytes 1540
  2.2 0.7 copy-start.13
  4.7 42.7 %all-to-all-start = ((bf16[64,2,2048]{2,1,0:T(2,128)(2,1)}), bf16[64,2,2048]{2,1,0:T(2,128)(2,1)S(1)}, u32[]{:S(2)}, u32[]{:S(2)}) async-start(bf16[64,2,2048]{2,1,0:T(2,128)(2,1)} %reshape.111), calls=%async_computation | async-start | bytes 1048576 | tf_op jit(solution)/shard_map/all_to_all | solution.py:57
  47.6 1.2 %copy-start.10 = (bf16[1,2048,256]{2,1,0:T(8,128)(2,1)S(1)}, bf16[1,2048,256]{2,1,0:T(8,128)(2,1)}, u32[]{:S(2)}) copy-start(bf16[1,2048,256]{2,1,0:T(8,128)(2,1)} %param.15) | copy-start | bytes 3145732
  48.8 1.0 %copy-start.1 = (bf16[256,8,1,128]{0,3,2,1:T(8,128)(2,1)S(1)}, bf16[256,8,1,128]{0,3,2,1:T(8,128)(2,1)}, u32[]{:S(2)}) copy-start(bf16[256,8,1,128]{0,3,2,1:T(8,128)(2,1)} %get-tuple-element.5) | copy-start | bytes 1572868
  50.2 3.4 %collective-permute-start = (bf16[128,1024]{1,0:T(8,128)(2,1)S(1)}, bf16[128,1024]{1,0:T(8,128)(2,1)S(1)}, u32[]{:S(2)}, u32[]{:S(2)}) collective-permute-start(bf16[128,1024]{1,0:T(8,128)(2,1)S(1)} %convolution_convert_fusion.1), channel_id=1, source_target_pairs={{0,1},{1,0},{2,3},{3,2},{4,5},{5,4},{6,7},{7,6},{8,9},{9,8},{10,11... | collective-permute-start | bytes 786440 | tf_op jit(solution)/shard_map/ppermute | solution.py:87
  53.9 6.2 %copy-start.3 = (bf16[128,2048]{1,0:T(8,128)(2,1)S(1)}, bf16[128,2048]{1,0:T(8,128)(2,1)}, u32[]{:S(2)}) copy-start(bf16[128,2048]{1,0:T(8,128)(2,1)} %param.10) | copy-start | bytes 1572868
  54.7 5.4 %copy-start.11 = (bf16[2048,32]{0,1:T(8,128)(2,1)S(1)}, bf16[2048,32]{0,1:T(8,128)(2,1)}, u32[]{:S(2)}) copy-start(bf16[2048,32]{0,1:T(8,128)(2,1)} %param.17) | copy-start | bytes 393220
  54.7 20.1 %all-to-all-start.1 = ((bf16[64,2,1024]{2,1,0:T(2,128)(2,1)}), bf16[64,2,1024]{2,1,0:T(2,128)(2,1)S(1)}, u32[]{:S(2)}, u32[]{:S(2)}) async-start(bf16[64,2,1024]{2,1,0:T(2,128)(2,1)} %reshape.115), calls=%async_computation.1 | async-start | bytes 524288 | tf_op jit(solution)/shard_map/all_to_all | solution.py:90
  60.2 0.9 copy-start.12
  61.4 3.1 %collective-permute-start.1 = (bf16[32,128]{1,0:T(8,128)(2,1)S(1)}, bf16[32,128]{1,0:T(8,128)(2,1)S(1)}, u32[]{:S(2)}, u32[]{:S(2)}) collective-permute-start(bf16[32,128]{1,0:T(8,128)(2,1)S(1)} %fusion.5), channel_id=1, source_target_pairs={{0,1},{1,0},{2,3},{3,2},{4,5},{5,4},{6,7},{7,6},{8,9},{9,8},{10,11... | collective-permute-start | bytes 24584 | tf_op jit(solution)/shard_map/ppermute | solution.py:62
  75.8 6.9 %copy-start.5 = (f32[128,6]{0,1:T(8,128)S(1)}, f32[128,6]{0,1:T(8,128)}, u32[]{:S(2)}) copy-start(f32[128,6]{0,1:T(8,128)} %param.13) | copy-start | bytes 9220
  75.8 20.0 %all-to-all-start.2 = ((bf16[8,192,128]{2,1,0:T(8,128)(2,1)}), bf16[8,192,128]{2,1,0:T(8,128)(2,1)S(1)}, u32[]{:S(2)}, u32[]{:S(2)}) async-start(bf16[8,192,128]{2,1,0:T(8,128)(2,1)} %copy.16), calls=%async_computation.2 | async-start | bytes 786432 | tf_op jit(solution)/shard_map/all_to_all | solution.py:97
  82.7 0.7 copy-start.7
  82.8 0.6 copy-start.9
  97.7 0.9 copy-start.4

commit v2 on v1

v2 whole, which is shorter than its diff:
```python
import jax
import jax.numpy as jnp
from jax import lax
from jax.sharding import Mesh
from jax.sharding import PartitionSpec as P

TP = ("x", "core")
EP = ("z", "y")
ALL = ("z", "y", "x", "core")

NORM_EPSILON = 1e-06


def dot(a, b, dims=((1,), (0,))):
    return lax.dot_general(a, b, (dims, ((), ())), preferred_element_type=jnp.float32)


def local(
    tokens,
    norm_gain,
    expert_ids,
    route_weights,
    expert_gate,
    expert_up,
    expert_down,
    shared_gate,
    shared_up,
    shared_down,
):
    groups = lax.axis_size(EP)
    columns = lax.axis_size("x")
    cores = lax.axis_size("core")
    column = lax.axis_index("x")
    core = lax.axis_index("core")
    rows, width = tokens.shape
    top_count = expert_ids.shape[1]
    tp_count = columns * cores
    block = width // tp_count

    as_float = tokens.astype(jnp.float32)
    inverse_rms = lax.rsqrt(jnp.mean(as_float * as_float, axis=-1, keepdims=True) + NORM_EPSILON)
    normed = (as_float * inverse_rms * norm_gain).astype(jnp.bfloat16)

    token_iota = jnp.arange(rows, dtype=jnp.int32)
    strict_lower = (token_iota[:, None] > token_iota[None, :]).astype(jnp.bfloat16)

    own_expert = jnp.arange(groups, dtype=jnp.int32) * columns + column
    own = jnp.zeros((rows, groups), jnp.bool_)
    for k in range(top_count):
        own = own | (expert_ids[:, k : k + 1] == own_expert[None, :])
    before = dot(strict_lower, own.astype(jnp.bfloat16))
    chosen = own & (before == core.astype(jnp.float32))
    buffer = dot(chosen.astype(jnp.bfloat16), normed, ((0,), (0,))).astype(jnp.bfloat16)
    with jax.named_scope("dispatch"):
        received = lax.all_to_all(
            buffer.reshape(groups, tp_count, block), EP, split_axis=0, concat_axis=0, tiled=True
        )

    swap = [(0, 1), (1, 0)]
    with jax.named_scope("weights"):
        gates = [expert_gate[0], lax.ppermute(expert_gate[0], "core", swap)]
        ups = [expert_up[0], lax.ppermute(expert_up[0], "core", swap)]
        downs = [expert_down[0], lax.ppermute(expert_down[0], "core", swap)]

    shared_act = (
        jax.nn.silu(dot(shared_gate, normed, ((0,), (1,)))) * dot(shared_up, normed, ((0,), (1,)))
    ).astype(jnp.bfloat16)

    slot_iota = jnp.arange(tp_count * groups, dtype=jnp.int32)
    slot_expert = (slot_iota % groups) * columns + slot_iota // (groups * cores)
    slot_number = (slot_iota // groups) % cores
    weight = jnp.zeros((rows, tp_count * groups), jnp.float32)
    taken = jnp.zeros((rows, tp_count * groups), jnp.bool_)
    for k in range(top_count):
        hit = expert_ids[:, k : k + 1] == slot_expert[None, :]
        taken = taken | hit
        weight = jnp.where(hit, route_weights[:, k : k + 1], weight)
    ahead = dot(strict_lower, taken.astype(jnp.bfloat16))
    weight = jnp.where(ahead == slot_number.astype(jnp.float32)[None, :], weight, 0.0)
    high = lax.reduce_precision(weight, 8, 7)
    parts = (high.astype(jnp.bfloat16), (weight - high).astype(jnp.bfloat16))

    flat_rows = lax.optimization_barrier(received.reshape(groups, width))
    expert_out = jnp.zeros((groups, width), jnp.float32)
    for gate, up, down in zip(gates, ups, downs):
        hidden = (jax.nn.silu(dot(flat_rows, gate)) * dot(flat_rows, up)).astype(jnp.bfloat16)
        expert_out = expert_out + dot(hidden, down)
    expert_out = expert_out.astype(jnp.bfloat16)
    with jax.named_scope("back"):
        returned = lax.all_to_all(
            expert_out.reshape(groups, tp_count, block), EP, split_axis=0, concat_axis=0, tiled=True
        )
    payload = jnp.concatenate(
        [
            jnp.swapaxes(returned, 0, 1),
            jnp.broadcast_to(shared_act[None], (tp_count,) + shared_act.shape),
        ],
        axis=1,
    )
    payload, *parts = lax.optimization_barrier((payload, *parts))
    with jax.named_scope("share"):
        gathered = lax.all_to_all(payload, TP, split_axis=0, concat_axis=0, tiled=True)
    values = gathered[:, :groups].reshape(tp_count * groups, block)
    act = gathered[:, groups:].reshape(-1, rows)
    mixed = dot(parts[0], values) + dot(parts[1], values) + dot(act, shared_down, ((0,), (0,)))
    return mixed.astype(jnp.bfloat16)


def solution(mesh):
    ep = mesh.shape["ep"]
    tp = mesh.shape["tp"]
    finer = Mesh(mesh.devices.reshape(8, ep // 8, tp // 2, 2), ALL)
    in_specs = (
        P(EP, None),
        P(),
        P(EP, None),
        P(EP, None),
        P(ALL, None, None),
        P(ALL, None, None),
        P(ALL, None, None),
        P(None, TP),
        P(None, TP),
        P(None, TP),
    )
    out_specs = P(EP, TP)
    return jax.shard_map(local, mesh=finer, in_specs=in_specs, out_specs=out_specs, check_vma=False)
```

time: 100 us -> 94.1 us (0.941)
  the two profiles are of different devices: /device:TPU:16 before, /device:TPU:1 now
where the time goes in v2:
time: 94.1 us; the launch traced here: 93.5 us
  starting transfers between devices  38 us (40%)
  blocking collectives  24 us (26%)
  waiting for transfers between devices  16.2 us (17%)
  matrix products  10.4 us (11%)
  local copies, waits for them, and re-layouts  3.3 us (4%)
  other arithmetic  1.36 us (1%)
    all_to_all x1, blocking collectives, local(): lax.all_to_all(payload, TP, split_axis=0, concat_axis=0, tiled=True)  24 us
    all_to_all x1, starting transfers between devices, local(): lax.all_to_all(buffer.reshape(groups, tp_count, block), EP, split_axis=0,...  23.9 us
    all_to_all x1, waiting for transfers between devices, local(): lax.all_to_all(expert_out.reshape(groups, tp_count, block), EP, split_axi...  10.6 us
    dot_general x11, matrix products, dot(): lax.dot_general(a, b, (dims, ((), ())), preferred_element_type=jnp.float32)  10.4 us
    all_to_all x1, starting transfers between devices, local(): lax.all_to_all(expert_out.reshape(groups, tp_count, block), EP, split_axi...  6.88 us
    all_to_all x1, waiting for transfers between devices, local(): lax.all_to_all(buffer.reshape(groups, tp_count, block), EP, split_axis=0,...  5.55 us
    unnamed x21, local copies, waits for them, and re-layouts  3.18 us
    ppermute x1, starting transfers between devices, local(): gates = [expert_gate[0], lax.ppermute(expert_gate[0], 'core', swap)]  2.87 us
  transfers between devices with their start and end apart: 5, of which 2 were waited for; matrix products, arithmetic and copies ran while one was open for 6% of the time, Pallas kernels for 0%

profile of v2, /device:TPU:1, one launch (start us, length us, event | category | flops | bytes accessed | tf_op | source)
XLA Modules:
  0.0 93.5 jit_solution(4609253883861135704)
XLA Ops:
  0.0 0.0 copy-start
  0.0 0.0 copy-start.4
  0.0 0.7 copy-done.4
  0.7 0.0 copy-start.8
  0.7 0.0 copy-start.2
  0.7 1.3 %fusion.10 = f32[128]{0:T(128)S(1)} fusion(bf16[128,2048]{1,0:T(8,128)(2,1)} %param.10), kind=kLoop, calls=%fused_computation.21 | loop fusion | flops 786304 | bytes 524800 | tf_op jit(solution)/shard_map/reduce_sum | solution.py:41
  2.1 0.0 copy-start.1
  2.1 0.0 copy-done.8
  2.1 1.5 %fusion.2 = bf16[8,8,16,128]{3,1,2,0:T(8,128)(2,1)S(1)} fusion(f32[]{:T(128)S(6)} %convert_element_type.44, s32[128]{0:T(128)S(1)} %get-tuple-element.23, s32[128]{0:T(128)S(1)} %get-tuple-element.24, s32[128]{0:T(128)S(1)} %get-tuple-element.20, s32[128]{0:T(128)S(1)} %get-tuple-element.21, s32[128]{0:T(128)S(1)} %get-tuple-element.22, ...), kind=kOutput, calls=%fused_computation.7 | convolution fusion | flops 37044224 | bytes 798468 | tf_op jit(solution)/shard_map/dot_general | solution.py:15
  3.6 0.7 copy.13
  4.4 23.9 %all-to-all-start = ((bf16[64,16,128]{2,1,0:T(8,128)(2,1)}), bf16[64,16,128]{2,1,0:T(8,128)(2,1)S(1)}, u32[]{:S(2)}, u32[]{:S(2)}) async-start(bf16[64,16,128]{2,1,0:T(8,128)(2,1)} %bitcast.21), calls=%async_computation | async-start | bytes 524288 | tf_op jit(solution)/shard_map/dispatch/all_to_all | solution.py:55
  28.3 2.9 %collective-permute-start = (bf16[2048,256]{1,0:T(8,128)(2,1)}, bf16[2048,256]{1,0:T(8,128)(2,1)}, u32[]{:S(2)}, u32[]{:S(2)}) collective-permute-start(bf16[2048,256]{1,0:T(8,128)(2,1)} %bitcast.81), channel_id=1, source_target_pairs={{0,1},{1,0},{2,3},{3,2},{4,5},{5,4},{6,7},{7,6},{8,9},{9,8},{10,11... | collective-permute-start | bytes 3145736 | tf_op jit(solution)/shard_map/weights/ppermute | solution.py:61
  31.2 0.0 copy-done.1
  31.2 1.9 %collective-permute-start.1 = (bf16[2048,256]{1,0:T(8,128)(2,1)S(1)}, bf16[2048,256]{1,0:T(8,128)(2,1)}, u32[]{:S(2)}, u32[]{:S(2)}) collective-permute-start(bf16[2048,256]{1,0:T(8,128)(2,1)S(1)} %bitcast.78), channel_id=1, source_target_pairs={{0,1},{1,0},{2,3},{3,2},{4,5},{5,4},{6,7},{7,6},{8,9},{9,8},{10,11... | collective-permute-start | bytes 3145736 | tf_op jit(solution)/shard_map/weights/ppermute | solution.py:62
  33.2 0.0 copy-done.2
  33.2 0.0 copy-start.5
  33.2 2.4 %collective-permute-start.2 = (bf16[256,2048]{1,0:T(8,128)(2,1)S(1)}, bf16[256,2048]{1,0:T(8,128)(2,1)}, u32[]{:S(2)}, u32[]{:S(2)}) collective-permute-start(bf16[256,2048]{1,0:T(8,128)(2,1)S(1)} %bitcast.79), channel_id=1, source_target_pairs={{0,1},{1,0},{2,3},{3,2},{4,5},{5,4},{6,7},{7,6},{8,9},{9,8},{10,11... | collective-permute-start | bytes 3145736 | tf_op jit(solution)/shard_map/weights/ppermute | solution.py:63
  35.6 0.0 copy-done.5
  35.6 5.5 %all-to-all-done = bf16[64,16,128]{2,1,0:T(8,128)(2,1)S(1)} async-done(((bf16[64,16,128]{2,1,0:T(8,128)(2,1)}), bf16[64,16,128]{2,1,0:T(8,128)(2,1)S(1)}, u32[]{:S(2)}, u32[]{:S(2)}) %all-to-all-start) | async-done | bytes 262176 | tf_op jit(solution)/shard_map/dispatch/all_to_all | solution.py:55
  41.2 0.1 copy.18
  41.3 1.5 %fusion.81 = f32[64,256]{1,0:T(8,128)S(1)} fusion(bf16[64,2048]{1,0:T(8,128)(2,1)S(1)} %bitcast.72, bf16[1,2048,256]{2,1,0:T(8,128)(2,1)} %param.14), kind=kOutput, calls=%fused_computation.114 | convolution fusion | flops 67108864 | bytes 1376256 | tf_op jit(solution)/shard_map/dot_general | solution.py:15
  42.8 0.8 fusion.6
  43.6 0.0 collective-permute-done
  43.6 1.5 %fusion.90 = f32[64,256]{1,0:T(8,128)S(1)} fusion(bf16[64,2048]{1,0:T(8,128)(2,1)S(1)} %bitcast.74, bf16[2048,256]{1,0:T(8,128)(2,1)} %collective-permute-done), kind=kOutput, calls=%fused_computation.119 | convolution fusion | flops 67108864 | bytes 1376256 | tf_op jit(solution)/shard_map/dot_general | solution.py:15
  45.1 0.0 collective-permute-done.1
  45.1 0.0 collective-permute-done.2
  45.1 2.3 %fusion.3 = bf16[8,8,16,128]{3,1,2,0:T(8,128)(2,1)S(1)} fusion(f32[64,2048]{1,0:T(8,128)S(1)} %fusion.6, bf16[256,2048]{1,0:T(8,128)(2,1)} %collective-permute-done.2, f32[64,256]{1,0:T(8,128)S(1)} %fusion.90, bf16[64,2048]{1,0:T(8,128)(2,1)S(1)} %bitcast.75, bf16[2048,256]{1,0:T(8,128)(2,1)} %collective-permute-done.1), kind=kOutput, calls=%fused_computation.8 | convolution fusion | flops 134578176 | bytes 3211264 | tf_op jit(solution)/shard_map/dot_general | solution.py:15
  47.5 0.7 copy.15
  48.2 6.9 %all-to-all-start.1 = ((bf16[64,16,128]{2,1,0:T(8,128)(2,1)}), bf16[64,16,128]{2,1,0:T(8,128)(2,1)S(1)}, u32[]{:S(2)}, u32[]{:S(2)}) async-start(bf16[64,16,128]{2,1,0:T(8,128)(2,1)} %bitcast.25), calls=%async_computation.1 | async-start | bytes 524288 | tf_op jit(solution)/shard_map/back/all_to_all | solution.py:90
  55.1 0.0 copy-start.3
  55.1 0.0 copy-start.6
  55.1 0.7 fusion.13
  55.9 0.3 copy-done.3
  56.2 0.0 copy-done.6
  56.2 0.0 copy-start.7
  56.2 0.3 convolution_bitcast_fusion.1
  56.5 0.6 copy-done.7
  57.1 0.4 fusion.8
  57.4 10.6 %all-to-all-done.1 = bf16[64,16,128]{2,1,0:T(8,128)(2,1)S(1)} async-done(((bf16[64,16,128]{2,1,0:T(8,128)(2,1)}), bf16[64,16,128]{2,1,0:T(8,128)(2,1)S(1)}, u32[]{:S(2)}, u32[]{:S(2)}) %all-to-all-start.1) | async-done | bytes 262176 | tf_op jit(solution)/shard_map/back/all_to_all | solution.py:90
  68.1 0.1 copy.19
  68.2 24.0 %all_to_all.15 = bf16[16,96,128]{2,1,0:T(8,128)(2,1)S(1)} all-to-all(bf16[16,96,128]{2,1,0:T(8,128)(2,1)S(1)} %pad_maximum_fusion), channel_id=1, replica_groups=mesh['z'=8,'y'=8,'x'=8,'core'=2] {'x','core'}, dimensions={0} | all-to-all | bytes 786432 | tf_op jit(solution)/shard_map/share/all_to_all | solution.py:102
  92.2 0.2 fusion.91
  92.4 0.2 convolution_add_fusion.2
  92.7 0.0 copy-done
  92.7 0.8 fusion.5
  (9 shorter events, 0.1 us)
Async XLA Ops:
  0.0 92.7 %copy-start = (bf16[512,128]{1,0:T(8,128)(2,1)S(1)}, bf16[512,128]{1,0:T(8,128)(2,1)}, u32[]{:S(2)}) copy-start(bf16[512,128]{1,0:T(8,128)(2,1)} %param.19) | copy-start | bytes 393220
  0.0 0.7 copy-start.4
  0.7 1.4 %copy-start.8 = (f32[2048]{0:T(1024)S(1)}, f32[2048]{0:T(1024)}, u32[]{:S(2)}) copy-start(f32[2048]{0:T(1024)} %param.11) | copy-start | bytes 24580
  0.7 32.4 %copy-start.2 = (bf16[1,256,2048]{2,1,0:T(8,128)(2,1)S(1)}, bf16[1,256,2048]{2,1,0:T(8,128)(2,1)}, u32[]{:S(2)}) copy-start(bf16[1,256,2048]{2,1,0:T(8,128)(2,1)} %param.16) | copy-start | bytes 3145732
  2.1 29.2 %copy-start.1 = (bf16[1,2048,256]{2,1,0:T(8,128)(2,1)S(1)}, bf16[1,2048,256]{2,1,0:T(8,128)(2,1)}, u32[]{:S(2)}) copy-start(bf16[1,2048,256]{2,1,0:T(8,128)(2,1)} %param.15) | copy-start | bytes 3145732
  4.4 36.8 %all-to-all-start = ((bf16[64,16,128]{2,1,0:T(8,128)(2,1)}), bf16[64,16,128]{2,1,0:T(8,128)(2,1)S(1)}, u32[]{:S(2)}, u32[]{:S(2)}) async-start(bf16[64,16,128]{2,1,0:T(8,128)(2,1)} %bitcast.21), calls=%async_computation | async-start | bytes 524288 | tf_op jit(solution)/shard_map/dispatch/all_to_all | solution.py:55
  28.3 15.2 %collective-permute-start = (bf16[2048,256]{1,0:T(8,128)(2,1)}, bf16[2048,256]{1,0:T(8,128)(2,1)}, u32[]{:S(2)}, u32[]{:S(2)}) collective-permute-start(bf16[2048,256]{1,0:T(8,128)(2,1)} %bitcast.81), channel_id=1, source_target_pairs={{0,1},{1,0},{2,3},{3,2},{4,5},{5,4},{6,7},{7,6},{8,9},{9,8},{10,11... | collective-permute-start | bytes 3145736 | tf_op jit(solution)/shard_map/weights/ppermute | solution.py:61
  31.2 13.9 %collective-permute-start.1 = (bf16[2048,256]{1,0:T(8,128)(2,1)S(1)}, bf16[2048,256]{1,0:T(8,128)(2,1)}, u32[]{:S(2)}, u32[]{:S(2)}) collective-permute-start(bf16[2048,256]{1,0:T(8,128)(2,1)S(1)} %bitcast.78), channel_id=1, source_target_pairs={{0,1},{1,0},{2,3},{3,2},{4,5},{5,4},{6,7},{7,6},{8,9},{9,8},{10,11... | collective-permute-start | bytes 3145736 | tf_op jit(solution)/shard_map/weights/ppermute | solution.py:62
  33.2 2.4 %copy-start.5 = (f32[128,6]{0,1:T(8,128)S(1)}, f32[128,6]{0,1:T(8,128)}, u32[]{:S(2)}) copy-start(f32[128,6]{0,1:T(8,128)} %param.13) | copy-start | bytes 9220
  33.2 11.9 %collective-permute-start.2 = (bf16[256,2048]{1,0:T(8,128)(2,1)S(1)}, bf16[256,2048]{1,0:T(8,128)(2,1)}, u32[]{:S(2)}, u32[]{:S(2)}) collective-permute-start(bf16[256,2048]{1,0:T(8,128)(2,1)S(1)} %bitcast.79), channel_id=1, source_target_pairs={{0,1},{1,0},{2,3},{3,2},{4,5},{5,4},{6,7},{7,6},{8,9},{9,8},{10,11... | collective-permute-start | bytes 3145736 | tf_op jit(solution)/shard_map/weights/ppermute | solution.py:63
  48.2 19.9 %all-to-all-start.1 = ((bf16[64,16,128]{2,1,0:T(8,128)(2,1)}), bf16[64,16,128]{2,1,0:T(8,128)(2,1)S(1)}, u32[]{:S(2)}, u32[]{:S(2)}) async-start(bf16[64,16,128]{2,1,0:T(8,128)(2,1)} %bitcast.25), calls=%async_computation.1 | async-start | bytes 524288 | tf_op jit(solution)/shard_map/back/all_to_all | solution.py:90
  55.1 1.0 %copy-start.3 = (bf16[128,2048]{1,0:T(8,128)(2,1)S(1)}, bf16[128,2048]{1,0:T(8,128)(2,1)}, u32[]{:S(2)}) copy-start(bf16[128,2048]{1,0:T(8,128)(2,1)} %param.10) | copy-start | bytes 1572868
  55.1 1.1 %copy-start.6 = (bf16[2048,32]{0,1:T(8,128)(2,1)S(1)}, bf16[2048,32]{0,1:T(8,128)(2,1)}, u32[]{:S(2)}) copy-start(bf16[2048,32]{0,1:T(8,128)(2,1)} %param.17) | copy-start | bytes 393220
  56.2 0.9 copy-start.7

commit v3 on v2

v3 whole, which is shorter than its diff:
```python
import jax
import jax.numpy as jnp
from jax import lax
from jax.experimental import pallas as pl
from jax.experimental.pallas import tpu as pltpu
from jax.sharding import Mesh
from jax.sharding import PartitionSpec as P


TP = ("x", "core")
EP = ("z", "y")
ALL = ("z", "y", "x", "core")

NORM_EPSILON = 1e-06
INTERPRET = False


def dot(a, b, dims=((1,), (0,))):
    return lax.dot_general(a, b, (dims, ((), ())), preferred_element_type=jnp.float32)


def pick_rows(place, far_ids, far_tokens, far_gain, out, ids, tokens, gain, sems):
    pairs = ((far_ids, ids), (far_tokens, tokens), (far_gain, gain))
    copies = [pltpu.make_async_copy(*pairs[i], sems.at[i]) for i in range(len(pairs))]
    for copy in copies:
        copy.start()
    columns = place[1]
    column, core = place[0] // place[2], place[0] % place[2]
    top_count, rows = ids.shape
    groups, width = out.shape
    expert = lax.broadcasted_iota(jnp.int32, (groups, rows), 0) * columns + column
    copies[0].wait()
    own = ids[0:1, :] == expert
    for k in range(1, top_count):
        own = own | (ids[k : k + 1, :] == expert)
    own = jnp.where(own, 1.0, 0.0)
    sooner = lax.broadcasted_iota(jnp.int32, (rows, rows), 0) < lax.broadcasted_iota(
        jnp.int32, (rows, rows), 1
    )
    before = dot(own.astype(jnp.bfloat16), jnp.where(sooner, 1.0, 0.0).astype(jnp.bfloat16))
    chosen = jnp.where(before == core.astype(jnp.float32), own, 0.0).astype(jnp.bfloat16)
    copies[1].wait()
    as_float = tokens[...].astype(jnp.float32)
    square = jnp.sum(as_float * as_float, axis=1, keepdims=True) * (1.0 / width)
    copies[2].wait()
    normed = (as_float * lax.rsqrt(square + NORM_EPSILON) * gain[...]).astype(jnp.bfloat16)
    out[...] = dot(chosen, normed).astype(jnp.bfloat16)


def expert_body(x, near, up_a, down_a, gate_b, up_b, down_b, out, wide, tall, sems):
    sources = (up_a, down_a, gate_b, up_b, down_b)
    targets = (wide.at[0], tall.at[0], wide.at[1], wide.at[2], tall.at[1])
    copies = [
        pltpu.make_async_copy(sources[i], targets[i], sems.at[i]) for i in range(len(sources))
    ]
    for copy in copies:
        copy.start()

    def hidden(gated, lifted):
        return (gated / (1.0 + jnp.exp(-gated)) * lifted).astype(jnp.bfloat16)

    gated = dot(x[...], near[...])
    copies[0].wait()
    acts = hidden(gated, dot(x[...], wide[0]))
    copies[1].wait()
    total = dot(acts, tall[0])
    copies[2].wait()
    gated = dot(x[...], wide[1])
    copies[3].wait()
    acts = hidden(gated, dot(x[...], wide[2]))
    copies[4].wait()
    out[...] = (total + dot(acts, tall[1])).astype(jnp.bfloat16)


def finish(gathered, high, low, down, out):
    tp_count = gathered.shape[0]
    groups = high.shape[1] // tp_count
    values = jnp.concatenate([gathered[s, :groups] for s in range(tp_count)], axis=0)
    act = jnp.concatenate([gathered[s, groups:] for s in range(tp_count)], axis=0)
    mixed = dot(high[...], values) + dot(low[...], values)
    out[...] = (mixed + dot(act, down[...], ((0,), (0,)))).astype(jnp.bfloat16)


def in_vmem(body, shape, *args, smem=0, anywhere=(), scratch=(), onward=False):
    specs = []
    args = list(args)
    for i in range(len(args)):
        space = pltpu.SMEM if i < smem else pltpu.HBM if i in anywhere else pltpu.VMEM
        specs.append(pl.BlockSpec(memory_space=space))
        if i >= smem and not INTERPRET:
            args[i] = pltpu.with_memory_space_constraint(args[i], space)
    out = jax.ShapeDtypeStruct(shape, jnp.bfloat16)
    return pl.pallas_call(
        body,
        out_shape=pltpu.VMEM(shape, jnp.bfloat16) if onward and not INTERPRET else out,
        in_specs=specs,
        out_specs=pl.BlockSpec(memory_space=pltpu.VMEM),
        scratch_shapes=list(scratch),
        interpret=INTERPRET,
    )(*args)


def local(
    tokens,
    norm_gain,
    expert_ids,
    route_weights,
    expert_gate,
    expert_up,
    expert_down,
    shared_gate,
    shared_up,
    shared_down,
):
    groups = lax.axis_size(EP)
    columns = lax.axis_size("x")
    cores = lax.axis_size("core")
    rows, width = tokens.shape
    top_count = expert_ids.shape[1]
    tp_count = columns * cores
    block = width // tp_count

    as_float = tokens.astype(jnp.float32)
    inverse_rms = lax.rsqrt(jnp.mean(as_float * as_float, axis=-1, keepdims=True) + NORM_EPSILON)
    normed = (as_float * inverse_rms * norm_gain).astype(jnp.bfloat16)

    token_iota = jnp.arange(rows, dtype=jnp.int32)
    strict_lower = (token_iota[:, None] > token_iota[None, :]).astype(jnp.bfloat16)

    place = jnp.stack([lax.axis_index(TP), jnp.int32(columns), jnp.int32(cores)])
    buffer = in_vmem(
        pick_rows,
        (groups, width),
        place,
        expert_ids.T,
        tokens,
        norm_gain[None],
        smem=1,
        anywhere=range(1, 4),
        onward=True,
        scratch=(
            pltpu.VMEM((top_count, rows), jnp.int32),
            pltpu.VMEM((rows, width), jnp.bfloat16),
            pltpu.VMEM((1, width), jnp.float32),
            pltpu.SemaphoreType.DMA((3,)),
        ),
    )
    received = lax.all_to_all(
        buffer.reshape(groups, tp_count, block), EP, split_axis=0, concat_axis=0, tiled=True
    )

    swap = [(0, 1), (1, 0)]
    halves = []
    for half in (expert_gate, expert_up, expert_down):
        halves.append((half[0], lax.ppermute(half[0], "core", swap)))
    gates, ups, downs = halves

    shared_act = (
        jax.nn.silu(dot(shared_gate, normed, ((0,), (1,)))) * dot(shared_up, normed, ((0,), (1,)))
    ).astype(jnp.bfloat16)

    slot_iota = jnp.arange(tp_count * groups, dtype=jnp.int32)
    slot_expert = (slot_iota % groups) * columns + slot_iota // (groups * cores)
    slot_number = (slot_iota // groups) % cores
    weight = jnp.zeros((rows, tp_count * groups), jnp.float32)
    taken = jnp.zeros((rows, tp_count * groups), jnp.bool_)
    for k in range(top_count):
        hit = expert_ids[:, k : k + 1] == slot_expert[None, :]
        taken = taken | hit
        weight = jnp.where(hit, route_weights[:, k : k + 1], weight)
    ahead = dot(strict_lower, taken.astype(jnp.bfloat16))
    weight = jnp.where(ahead == slot_number.astype(jnp.float32)[None, :], weight, 0.0)
    high = lax.reduce_precision(weight, 8, 7)
    parts = (high.astype(jnp.bfloat16), (weight - high).astype(jnp.bfloat16))

    inner = expert_gate.shape[2]
    expert_out = in_vmem(
        expert_body,
        (groups, width),
        received.reshape(groups, width),
        gates[1],
        ups[1],
        downs[1],
        gates[0],
        ups[0],
        downs[0],
        anywhere=range(2, 7),
        onward=True,
        scratch=(
            pltpu.VMEM((3, width, inner), jnp.bfloat16),
            pltpu.VMEM((2, inner, width), jnp.bfloat16),
            pltpu.SemaphoreType.DMA((5,)),
        ),
    )
    returned = lax.all_to_all(
        expert_out.reshape(groups, tp_count, block), EP, split_axis=0, concat_axis=0, tiled=True
    )
    payload = jnp.concatenate(
        [
            jnp.swapaxes(returned, 0, 1),
            jnp.broadcast_to(shared_act[None], (tp_count,) + shared_act.shape),
        ],
        axis=1,
    )
    payload, *parts = lax.optimization_barrier((payload, *parts))
    gathered = lax.all_to_all(payload, TP, split_axis=0, concat_axis=0, tiled=True)
    return in_vmem(finish, (rows, block), gathered, *parts, shared_down)


def solution(mesh):
    ep = mesh.shape["ep"]
    tp = mesh.shape["tp"]
    finer = Mesh(mesh.devices.reshape(8, ep // 8, tp // 2, 2), ALL)
    in_specs = (
        P(EP, None),
        P(),
        P(EP, None),
        P(EP, None),
        P(ALL, None, None),
        P(ALL, None, None),
        P(ALL, None, None),
        P(None, TP),
        P(None, TP),
        P(None, TP),
    )
    out_specs = P(EP, TP)

    return jax.shard_map(local, mesh=finer, in_specs=in_specs, out_specs=out_specs, check_vma=False)
```

time: 94.1 us -> 96.2 us (1.022)
  matrix products: 10.4 us -> 1.41 us
  waiting for transfers between devices: 16.2 us -> 22.7 us
  Pallas kernels: 0 us -> 6.34 us
  starting transfers between devices: 38 us -> 36.2 us
    all_to_all x1, starting transfers between devices: 23.9 us -> 10.5 us  [local(): lax.all_to_all(buffer.reshape(groups, tp_count, block), EP, split_axis=0,...]
    ppermute x3, starting transfers between devices: 7.2 us -> 20.5 us  [local(): halves.append((half[0], lax.ppermute(half[0], 'core', swap)))]
    dot_general x11 -> x3, matrix products: 10.4 us -> 1.41 us  [dot(): lax.dot_general(a, b, (dims, ((), ())), preferred_element_type=jnp.float32)]
    pallas_call x0 -> x3, Pallas kernels: none -> 6.34 us  [in_vmem(): pl.pallas_call(body, out_shape=pltpu.VMEM(shape, jnp.bfloat16) if onward...]
    all_to_all x1, waiting for transfers between devices: 5.55 us -> 11.5 us  [local(): lax.all_to_all(buffer.reshape(groups, tp_count, block), EP, split_axis=0,...]
    all_to_all x1, starting transfers between devices: 6.88 us -> 5.18 us  [local(): lax.all_to_all(expert_out.reshape(groups, tp_count, block), EP, split_axi...]
    reduce_sum x1, other arithmetic: 1.32 us -> 0.19 us  [local(): jnp.mean(as_float * as_float, axis=-1, keepdims=True) + NORM_EPSILON]
    unnamed x21 -> x17, local copies, waits for them, and re-layouts: 3.18 us -> 3.31 us
  transfers between devices with their start and end apart: 5 -> 5, of which waited for: 2 -> 2; matrix products, arithmetic and copies ran while one was open for 6% -> 3% of each run, Pallas kernels for 0% -> 2%
where the time goes in v3:
time: 96.2 us; the launch traced here: 95.7 us
  starting transfers between devices  36.2 us (38%)
  blocking collectives  24.7 us (26%)
  waiting for transfers between devices  22.7 us (24%)
  Pallas kernels  6.34 us (7%)
  local copies, waits for them, and re-layouts  3.4 us (4%)
  matrix products  1.41 us (1%)
    all_to_all x1, blocking collectives, local(): lax.all_to_all(payload, TP, split_axis=0, concat_axis=0, tiled=True)  24.7 us
    ppermute x3, starting transfers between devices, local(): halves.append((half[0], lax.ppermute(half[0], 'core', swap)))  20.5 us
    all_to_all x1, waiting for transfers between devices, local(): lax.all_to_all(buffer.reshape(groups, tp_count, block), EP, split_axis=0,...  11.5 us
    all_to_all x1, waiting for transfers between devices, local(): lax.all_to_all(expert_out.reshape(groups, tp_count, block), EP, split_axi...  11.2 us
    all_to_all x1, starting transfers between devices, local(): lax.all_to_all(buffer.reshape(groups, tp_count, block), EP, split_axis=0,...  10.5 us
    pallas_call x3, Pallas kernels, in_vmem(): pl.pallas_call(body, out_shape=pltpu.VMEM(shape, jnp.bfloat16) if onward...  6.34 us
    all_to_all x1, starting transfers between devices, local(): lax.all_to_all(expert_out.reshape(groups, tp_count, block), EP, split_axi...  5.18 us
    unnamed x17, local copies, waits for them, and re-layouts  3.31 us
  transfers between devices with their start and end apart: 5, of which 2 were waited for; matrix products, arithmetic and copies ran while one was open for 3% of the time, Pallas kernels for 2%

profile of v3, /device:TPU:1, one launch (start us, length us, event | category | flops | bytes accessed | tf_op | source)
XLA Modules:
  0.0 95.7 jit_solution(15631035185420459265)
XLA Ops:
  0.0 0.0 copy-start
  0.0 16.1 %collective-permute-start = (bf16[2048,256]{1,0:T(8,128)(2,1)}, bf16[2048,256]{1,0:T(8,128)(2,1)S(1)}, u32[]{:S(2)}, u32[]{:S(2)}) collective-permute-start(bf16[2048,256]{1,0:T(8,128)(2,1)} %bitcast.56), channel_id=1, source_target_pairs={{0,1},{1,0},{2,3},{3,2},{4,5},{5,4},{6,7},{7,6},{8,9},{9,8},{10,11... | collective-permute-start | bytes 3145736 | tf_op jit(solution)/shard_map/ppermute | solution.py:155
  16.2 1.9 %collective-permute-start.1 = (bf16[2048,256]{1,0:T(8,128)(2,1)}, bf16[2048,256]{1,0:T(8,128)(2,1)}, u32[]{:S(2)}, u32[]{:S(2)}) collective-permute-start(bf16[2048,256]{1,0:T(8,128)(2,1)} %bitcast.58), channel_id=1, source_target_pairs={{0,1},{1,0},{2,3},{3,2},{4,5},{5,4},{6,7},{7,6},{8,9},{9,8},{10,11... | collective-permute-start | bytes 3145736 | tf_op jit(solution)/shard_map/ppermute | solution.py:155
  18.1 2.4 %collective-permute-start.2 = (bf16[256,2048]{1,0:T(8,128)(2,1)}, bf16[256,2048]{1,0:T(8,128)(2,1)}, u32[]{:S(2)}, u32[]{:S(2)}) collective-permute-start(bf16[256,2048]{1,0:T(8,128)(2,1)} %bitcast.60), channel_id=1, source_target_pairs={{0,1},{1,0},{2,3},{3,2},{4,5},{5,4},{6,7},{7,6},{8,9},{9,8},{10,11... | collective-permute-start | bytes 3145736 | tf_op jit(solution)/shard_map/ppermute | solution.py:155
  20.5 0.6 pad_add_fusion.place
  21.1 2.2 %shard_map.100 = bf16[64,2048]{1,0:T(8,128)(2,1)S(1)} custom-call(s32[3]{0:T(128)} %pad_add_fusion.place, s32[6,128]{1,0:T(8,128)} %bitcast.62, bf16[128,2048]{1,0:T(8,128)(2,1)} %far_tokens.1, f32[1,2048]{1,0:T(1,128)} %bitcast.63), custom_call_target="tpu_custom_call" | custom-call | tf_op jit(solution)/shard_map/pallas_call | solution.py:93
  23.3 0.0 copy-start.2
  23.3 0.7 copy.13
  24.0 10.5 %all-to-all-start = ((bf16[64,16,128]{2,1,0:T(8,128)(2,1)}), bf16[64,16,128]{2,1,0:T(8,128)(2,1)S(1)}, u32[]{:S(2)}, u32[]{:S(2)}) async-start(bf16[64,16,128]{2,1,0:T(8,128)(2,1)} %bitcast.22), calls=%async_computation | async-start | bytes 524288 | tf_op jit(solution)/shard_map/all_to_all | solution.py:148
  34.5 0.0 copy-done.2
  34.5 0.0 copy-start.3
  34.6 0.2 fusion.3
  34.7 0.5 copy-done.3
  35.2 0.0 copy-start.5
  35.3 0.7 copy-done.5
  35.9 0.7 fusion.6
  36.7 11.5 %all-to-all-done = bf16[64,16,128]{2,1,0:T(8,128)(2,1)S(1)} async-done(((bf16[64,16,128]{2,1,0:T(8,128)(2,1)}), bf16[64,16,128]{2,1,0:T(8,128)(2,1)S(1)}, u32[]{:S(2)}, u32[]{:S(2)}) %all-to-all-start) | async-done | bytes 262176 | tf_op jit(solution)/shard_map/all_to_all | solution.py:148
  48.1 0.1 copy.18
  48.2 0.0 collective-permute-done.near
  48.2 0.0 collective-permute-done.1.up_a
  48.2 0.0 collective-permute-done.2.down_a
  48.2 3.2 %shard_map.101 = bf16[64,2048]{1,0:T(8,128)(2,1)S(1)} custom-call(bf16[64,2048]{1,0:T(8,128)(2,1)S(1)} %bitcast.52, bf16[2048,256]{1,0:T(8,128)(2,1)S(1)} %collective-permute-done.near, bf16[2048,256]{1,0:T(8,128)(2,1)} %collective-permute-done.1.up_a, bf16[256,2048]{1,0:T(8,128)(2,1)} %collective-permute-done.2.down_a, bf16[2048,256]{1,0:T(8,128)(2,1)} %bitcast.57, ...), custom_call_target="tpu_custom_call" | custom-call | tf_op jit(solution)/shard_map/pallas_call | solution.py:93
  51.5 0.7 copy.15
  52.2 0.0 copy-start.4
  52.2 5.2 %all-to-all-start.1 = ((bf16[64,16,128]{2,1,0:T(8,128)(2,1)}), bf16[64,16,128]{2,1,0:T(8,128)(2,1)S(1)}, u32[]{:S(2)}, u32[]{:S(2)}) async-start(bf16[64,16,128]{2,1,0:T(8,128)(2,1)} %bitcast.26), calls=%async_computation.1 | async-start | bytes 524288 | tf_op jit(solution)/shard_map/all_to_all | solution.py:195
  57.4 0.0 copy-done
  57.4 0.0 copy-done.4
  57.4 0.0 copy-start.6
  57.4 0.3 convolution_bitcast_fusion.1
  57.8 0.5 copy-done.6
  58.3 0.4 fusion.2
  58.7 11.2 %all-to-all-done.1 = bf16[64,16,128]{2,1,0:T(8,128)(2,1)S(1)} async-done(((bf16[64,16,128]{2,1,0:T(8,128)(2,1)}), bf16[64,16,128]{2,1,0:T(8,128)(2,1)S(1)}, u32[]{:S(2)}, u32[]{:S(2)}) %all-to-all-start.1) | async-done | bytes 262176 | tf_op jit(solution)/shard_map/all_to_all | solution.py:195
  69.9 0.1 copy.19
  70.0 0.0 copy-start.1
  70.0 24.7 %all_to_all.15.gathered = bf16[16,96,128]{2,1,0:T(8,128)(2,1)S(1)} all-to-all(bf16[16,96,128]{2,1,0:T(8,128)(2,1)S(1)} %pad_maximum_fusion), channel_id=1, replica_groups=mesh['z'=8,'y'=8,'x'=8,'core'=2] {'x','core'}, dimensions={0} | all-to-all | bytes 786432 | tf_op jit(solution)/shard_map/all_to_all | solution.py:206
  94.7 0.0 copy-done.1
  94.7 0.9 shard_map.102
  (6 shorter events, 0.1 us)
Async XLA Ops:
  0.0 57.4 %copy-start = (bf16[2048,32]{0,1:T(8,128)(2,1)S(1)}, bf16[2048,32]{0,1:T(8,128)(2,1)}, u32[]{:S(2)}) copy-start(bf16[2048,32]{0,1:T(8,128)(2,1)} %param.17) | copy-start | bytes 393220
  0.0 48.2 %collective-permute-start = (bf16[2048,256]{1,0:T(8,128)(2,1)}, bf16[2048,256]{1,0:T(8,128)(2,1)S(1)}, u32[]{:S(2)}, u32[]{:S(2)}) collective-permute-start(bf16[2048,256]{1,0:T(8,128)(2,1)} %bitcast.56), channel_id=1, source_target_pairs={{0,1},{1,0},{2,3},{3,2},{4,5},{5,4},{6,7},{7,6},{8,9},{9,8},{10,11... | collective-permute-start | bytes 3145736 | tf_op jit(solution)/shard_map/ppermute | solution.py:155
  16.2 32.1 %collective-permute-start.1 = (bf16[2048,256]{1,0:T(8,128)(2,1)}, bf16[2048,256]{1,0:T(8,128)(2,1)}, u32[]{:S(2)}, u32[]{:S(2)}) collective-permute-start(bf16[2048,256]{1,0:T(8,128)(2,1)} %bitcast.58), channel_id=1, source_target_pairs={{0,1},{1,0},{2,3},{3,2},{4,5},{5,4},{6,7},{7,6},{8,9},{9,8},{10,11... | collective-permute-start | bytes 3145736 | tf_op jit(solution)/shard_map/ppermute | solution.py:155
  18.1 30.1 %collective-permute-start.2 = (bf16[256,2048]{1,0:T(8,128)(2,1)}, bf16[256,2048]{1,0:T(8,128)(2,1)}, u32[]{:S(2)}, u32[]{:S(2)}) collective-permute-start(bf16[256,2048]{1,0:T(8,128)(2,1)} %bitcast.60), channel_id=1, source_target_pairs={{0,1},{1,0},{2,3},{3,2},{4,5},{5,4},{6,7},{7,6},{8,9},{9,8},{10,11... | collective-permute-start | bytes 3145736 | tf_op jit(solution)/shard_map/ppermute | solution.py:155
  23.3 11.3 %copy-start.2 = (bf16[128,2048]{1,0:T(8,128)(2,1)S(1)}, bf16[128,2048]{1,0:T(8,128)(2,1)}, u32[]{:S(2)}) copy-start(bf16[128,2048]{1,0:T(8,128)(2,1)} %far_tokens.1) | copy-start | bytes 1572868
  24.0 24.1 %all-to-all-start = ((bf16[64,16,128]{2,1,0:T(8,128)(2,1)}), bf16[64,16,128]{2,1,0:T(8,128)(2,1)S(1)}, u32[]{:S(2)}, u32[]{:S(2)}) async-start(bf16[64,16,128]{2,1,0:T(8,128)(2,1)} %bitcast.22), calls=%async_computation | async-start | bytes 524288 | tf_op jit(solution)/shard_map/all_to_all | solution.py:148
  34.5 0.7 copy-start.3
  35.2 0.7 copy-start.5
  52.2 5.2 %copy-start.4 = (f32[2048]{0:T(1024)S(1)}, f32[2048]{0:T(1024)}, u32[]{:S(2)}) copy-start(f32[2048]{0:T(1024)} %param.11) | copy-start | bytes 24580
  52.2 17.7 %all-to-all-start.1 = ((bf16[64,16,128]{2,1,0:T(8,128)(2,1)}), bf16[64,16,128]{2,1,0:T(8,128)(2,1)S(1)}, u32[]{:S(2)}, u32[]{:S(2)}) async-start(bf16[64,16,128]{2,1,0:T(8,128)(2,1)} %bitcast.26), calls=%async_computation.1 | async-start | bytes 524288 | tf_op jit(solution)/shard_map/all_to_all | solution.py:195
  57.4 0.9 copy-start.6
  70.0 24.7 %copy-start.1 = (bf16[512,128]{1,0:T(8,128)(2,1)S(1)}, bf16[512,128]{1,0:T(8,128)(2,1)}, u32[]{:S(2)}) copy-start(bf16[512,128]{1,0:T(8,128)(2,1)} %down.1) | copy-start | bytes 393220

commit v4 on v3

--- a/solution.py
+++ b/solution.py
@@ -1,3 +1,5 @@
+import functools
+
 import jax
 import jax.numpy as jnp
 from jax import lax
@@ -19,15 +21,24 @@
     return lax.dot_general(a, b, (dims, ((), ())), preferred_element_type=jnp.float32)
 
 
-def pick_rows(place, far_ids, far_tokens, far_gain, out, ids, tokens, gain, sems):
+def row_major(value, scratch, out):
+    rows, width = value.shape
+    block = out.shape[1]
+    count = width // block
+    for b in range(count):
+        scratch[pl.ds(b, rows, stride=count), :] = value[:, b * block : (b + 1) * block]
+    out[...] = scratch[...].astype(jnp.bfloat16)
+
+
+def pick_rows(columns, cores, place, far_ids, far_tokens, far_gain, out, ids, tokens, gain, wide, sems):
     pairs = ((far_ids, ids), (far_tokens, tokens), (far_gain, gain))
     copies = [pltpu.make_async_copy(*pairs[i], sems.at[i]) for i in range(len(pairs))]
     for copy in copies:
         copy.start()
-    columns = place[1]
-    column, core = place[0] // place[2], place[0] % place[2]
+    column, core = place[0] // cores, place[0] % cores
     top_count, rows = ids.shape
-    groups, width = out.shape
+    width = tokens.shape[1]
+    groups = out.shape[0] * out.shape[1] // width
     expert = lax.broadcasted_iota(jnp.int32, (groups, rows), 0) * columns + column
     copies[0].wait()
     own = ids[0:1, :] == expert
@@ -44,10 +55,10 @@
     square = jnp.sum(as_float * as_float, axis=1, keepdims=True) * (1.0 / width)
     copies[2].wait()
     normed = (as_float * lax.rsqrt(square + NORM_EPSILON) * gain[...]).astype(jnp.bfloat16)
-    out[...] = dot(chosen, normed).astype(jnp.bfloat16)
-
-
-def expert_body(x, near, up_a, down_a, gate_b, up_b, down_b, out, wide, tall, sems):
+    row_major(dot(chosen, normed), wide, out)
+
+
+def expert_body(x, near, up_a, down_a, gate_b, up_b, down_b, out, wide, tall, flat, sems):
     sources = (up_a, down_a, gate_b, up_b, down_b)
     targets = (wide.at[0], tall.at[0], wide.at[1], wide.at[2], tall.at[1])
     copies = [
@@ -69,7 +80,7 @@
     copies[3].wait()
     acts = hidden(gated, dot(x[...], wide[2]))
     copies[4].wait()
-    out[...] = (total + dot(acts, tall[1])).astype(jnp.bfloat16)
+    row_major(total + dot(acts, tall[1]), flat, out)
 
 
 def finish(gathered, high, low, down, out):
@@ -98,6 +109,38 @@
         scratch_shapes=list(scratch),
         interpret=INTERPRET,
     )(*args)
+
+
+def late_work(tokens, norm_gain, expert_ids, route_weights, shared_gate, shared_up, groups):
+    columns = lax.axis_size("x")
+    cores = lax.axis_size("core")
+    tp_count = columns * cores
+    rows, top_count = expert_ids.shape
+    as_float = tokens.astype(jnp.float32)
+    inverse_rms = lax.rsqrt(jnp.mean(as_float * as_float, axis=-1, keepdims=True) + NORM_EPSILON)
+    normed = (as_float * inverse_rms * norm_gain).astype(jnp.bfloat16)
+
+    shared_act = (
+        jax.nn.silu(dot(shared_gate, normed, ((0,), (1,)))) * dot(shared_up, normed, ((0,), (1,)))
+    ).astype(jnp.bfloat16)
+
+    token_iota = jnp.arange(rows, dtype=jnp.int32)
+    strict_lower = (token_iota[:, None] > token_iota[None, :]).astype(jnp.bfloat16)
+
+    slot_iota = jnp.arange(tp_count * groups, dtype=jnp.int32)
+    slot_expert = (slot_iota % groups) * columns + slot_iota // (groups * cores)
+    slot_number = (slot_iota // groups) % cores
+    weight = jnp.zeros((rows, tp_count * groups), jnp.float32)
+    taken = jnp.zeros((rows, tp_count * groups), jnp.bool_)
+    for k in range(top_count):
+        hit = expert_ids[:, k : k + 1] == slot_expert[None, :]
+        taken = taken | hit
+        weight = jnp.where(hit, route_weights[:, k : k + 1], weight)
+    ahead = dot(strict_lower, taken.astype(jnp.bfloat16))
+    weight = jnp.where(ahead == slot_number.astype(jnp.float32)[None, :], weight, 0.0)
+    high = lax.reduce_precision(weight, 8, 7)
+    parts = (high.astype(jnp.bfloat16), (weight - high).astype(jnp.bfloat16))
+    return shared_act, parts
 
 
 def local(
@@ -120,18 +163,11 @@
     tp_count = columns * cores
     block = width // tp_count
 
-    as_float = tokens.astype(jnp.float32)
-    inverse_rms = lax.rsqrt(jnp.mean(as_float * as_float, axis=-1, keepdims=True) + NORM_EPSILON)
-    normed = (as_float * inverse_rms * norm_gain).astype(jnp.bfloat16)
-
-    token_iota = jnp.arange(rows, dtype=jnp.int32)
-    strict_lower = (token_iota[:, None] > token_iota[None, :]).astype(jnp.bfloat16)
-
-    place = jnp.stack([lax.axis_index(TP), jnp.int32(columns), jnp.int32(cores)])
+    flat = (groups * tp_count, block)
     buffer = in_vmem(
-        pick_rows,
-        (groups, width),
-        place,
+        functools.partial(pick_rows, columns, cores),
+        flat,
+        lax.axis_index(TP)[None],
         expert_ids.T,
         tokens,
         norm_gain[None],
@@ -142,6 +178,7 @@
             pltpu.VMEM((top_count, rows), jnp.int32),
             pltpu.VMEM((rows, width), jnp.bfloat16),
             pltpu.VMEM((1, width), jnp.float32),
+            pltpu.VMEM(flat, jnp.float32),
             pltpu.SemaphoreType.DMA((3,)),
         ),
     )
@@ -155,28 +192,10 @@
         halves.append((half[0], lax.ppermute(half[0], "core", swap)))
     gates, ups, downs = halves
 
-    shared_act = (
-        jax.nn.silu(dot(shared_gate, normed, ((0,), (1,)))) * dot(shared_up, normed, ((0,), (1,)))
-    ).astype(jnp.bfloat16)
-
-    slot_iota = jnp.arange(tp_count * groups, dtype=jnp.int32)
-    slot_expert = (slot_iota % groups) * columns + slot_iota // (groups * cores)
-    slot_number = (slot_iota // groups) % cores
-    weight = jnp.zeros((rows, tp_count * groups), jnp.float32)
-    taken = jnp.zeros((rows, tp_count * groups), jnp.bool_)
-    for k in range(top_count):
-        hit = expert_ids[:, k : k + 1] == slot_expert[None, :]
-        taken = taken | hit
-        weight = jnp.where(hit, route_weights[:, k : k + 1], weight)
-    ahead = dot(strict_lower, taken.astype(jnp.bfloat16))
-    weight = jnp.where(ahead == slot_number.astype(jnp.float32)[None, :], weight, 0.0)
-    high = lax.reduce_precision(weight, 8, 7)
-    parts = (high.astype(jnp.bfloat16), (weight - high).astype(jnp.bfloat16))
-
     inner = expert_gate.shape[2]
     expert_out = in_vmem(
         expert_body,
-        (groups, width),
+        flat,
         received.reshape(groups, width),
         gates[1],
         ups[1],
@@ -189,11 +208,15 @@
         scratch=(
             pltpu.VMEM((3, width, inner), jnp.bfloat16),
             pltpu.VMEM((2, inner, width), jnp.bfloat16),
+            pltpu.VMEM(flat, jnp.float32),
             pltpu.SemaphoreType.DMA((5,)),
         ),
     )
     returned = lax.all_to_all(
         expert_out.reshape(groups, tp_count, block), EP, split_axis=0, concat_axis=0, tiled=True
+    )
+    shared_act, parts = late_work(
+        tokens, norm_gain, expert_ids, route_weights, shared_gate, shared_up, groups
     )
     payload = jnp.concatenate(
         [

time: 96.2 us -> 95 us (0.988)
  local copies, waits for them, and re-layouts: 3.4 us -> 1.91 us
  Pallas kernels: 6.34 us -> 7.37 us
    unnamed x17 -> x15, local copies, waits for them, and re-layouts: 3.31 us -> 1.82 us
    pallas_call x3, Pallas kernels: 6.34 us -> 7.37 us  [in_vmem(): pl.pallas_call(body, out_shape=pltpu.VMEM(shape, jnp.bfloat16) if onward...]
  transfers between devices with their start and end apart: 5 -> 5, of which waited for: 2 -> 2; matrix products, arithmetic and copies ran while one was open for 3% -> 2% of each run, Pallas kernels for 2% -> 2%
where the time goes in v4:
time: 95 us; the launch traced here: 94.5 us
  starting transfers between devices  36 us (38%)
  blocking collectives  24.7 us (26%)
  waiting for transfers between devices  22.7 us (24%)
  Pallas kernels  7.37 us (8%)
  local copies, waits for them, and re-layouts  1.91 us (2%)
  matrix products  1.41 us (1%)
    all_to_all x1, blocking collectives, local(): lax.all_to_all(payload, TP, split_axis=0, concat_axis=0, tiled=True)  24.7 us
    ppermute x3, starting transfers between devices, local(): halves.append((half[0], lax.ppermute(half[0], 'core', swap)))  20.5 us
    all_to_all x1, waiting for transfers between devices, local(): lax.all_to_all(buffer.reshape(groups, tp_count, block), EP, split_axis=0,...  11.5 us
    all_to_all x1, waiting for transfers between devices, local(): lax.all_to_all(expert_out.reshape(groups, tp_count, block), EP, split_axi...  11.2 us
    all_to_all x1, starting transfers between devices, local(): lax.all_to_all(buffer.reshape(groups, tp_count, block), EP, split_axis=0,...  10.5 us
    pallas_call x3, Pallas kernels, in_vmem(): pl.pallas_call(body, out_shape=pltpu.VMEM(shape, jnp.bfloat16) if onward...  7.37 us
    all_to_all x1, starting transfers between devices, local(): lax.all_to_all(expert_out.reshape(groups, tp_count, block), EP, split_axi...  5.05 us
  transfers between devices with their start and end apart: 5, of which 2 were waited for; matrix products, arithmetic and copies ran while one was open for 2% of the time, Pallas kernels for 2%

profile of v4, /device:TPU:1, one launch (start us, length us, event | category | flops | bytes accessed | tf_op | source)
XLA Modules:
  0.0 94.5 jit_solution(253484156429453477)
XLA Ops:
  0.0 0.0 copy-start
  0.0 16.1 %collective-permute-start = (bf16[2048,256]{1,0:T(8,128)(2,1)}, bf16[2048,256]{1,0:T(8,128)(2,1)S(1)}, u32[]{:S(2)}, u32[]{:S(2)}) collective-permute-start(bf16[2048,256]{1,0:T(8,128)(2,1)} %bitcast.52), channel_id=1, source_target_pairs={{0,1},{1,0},{2,3},{3,2},{4,5},{5,4},{6,7},{7,6},{8,9},{9,8},{10,11... | collective-permute-start | bytes 3145736 | tf_op jit(solution)/shard_map/ppermute | solution.py:192
  16.2 1.9 %collective-permute-start.1 = (bf16[2048,256]{1,0:T(8,128)(2,1)}, bf16[2048,256]{1,0:T(8,128)(2,1)}, u32[]{:S(2)}, u32[]{:S(2)}) collective-permute-start(bf16[2048,256]{1,0:T(8,128)(2,1)} %bitcast.54), channel_id=1, source_target_pairs={{0,1},{1,0},{2,3},{3,2},{4,5},{5,4},{6,7},{7,6},{8,9},{9,8},{10,11... | collective-permute-start | bytes 3145736 | tf_op jit(solution)/shard_map/ppermute | solution.py:192
  18.1 2.4 %collective-permute-start.2 = (bf16[256,2048]{1,0:T(8,128)(2,1)}, bf16[256,2048]{1,0:T(8,128)(2,1)}, u32[]{:S(2)}, u32[]{:S(2)}) collective-permute-start(bf16[256,2048]{1,0:T(8,128)(2,1)} %bitcast.56), channel_id=1, source_target_pairs={{0,1},{1,0},{2,3},{3,2},{4,5},{5,4},{6,7},{7,6},{8,9},{9,8},{10,11... | collective-permute-start | bytes 3145736 | tf_op jit(solution)/shard_map/ppermute | solution.py:192
  20.5 0.0 copy-start.2
  20.5 2.4 %shard_map.100 = bf16[1024,128]{1,0:T(8,128)(2,1)} custom-call(s32[1]{0:T(128)} %bitcast.place, s32[6,128]{1,0:T(8,128)} %bitcast.58, bf16[128,2048]{1,0:T(8,128)(2,1)} %far_tokens.1, f32[1,2048]{1,0:T(1,128)} %bitcast.59), custom_call_target="tpu_custom_call" | custom-call | tf_op jit(solution)/shard_map/pallas_call | solution.py:104
  22.9 10.5 %all-to-all-start = ((bf16[64,16,128]{2,1,0:T(8,128)(2,1)}), bf16[64,16,128]{2,1,0:T(8,128)(2,1)S(1)}, u32[]{:S(2)}, u32[]{:S(2)}) async-start(bf16[64,16,128]{2,1,0:T(8,128)(2,1)} %bitcast.3), calls=%async_computation | async-start | bytes 524288 | tf_op jit(solution)/shard_map/all_to_all | solution.py:185
  33.4 0.0 copy-done.2
  33.4 0.0 copy-start.3
  33.4 0.2 fusion.3
  33.6 0.5 copy-done.3
  34.1 0.0 copy-start.5
  34.1 0.7 copy-done.5
  34.8 0.7 fusion.6
  35.5 11.5 %all-to-all-done = bf16[64,16,128]{2,1,0:T(8,128)(2,1)S(1)} async-done(((bf16[64,16,128]{2,1,0:T(8,128)(2,1)}), bf16[64,16,128]{2,1,0:T(8,128)(2,1)S(1)}, u32[]{:S(2)}, u32[]{:S(2)}) %all-to-all-start) | async-done | bytes 262176 | tf_op jit(solution)/shard_map/all_to_all | solution.py:185
  47.0 0.1 copy.16
  47.1 0.0 collective-permute-done.near
  47.1 0.0 collective-permute-done.1.up_a
  47.1 0.0 collective-permute-done.2.down_a
  47.1 4.1 %shard_map.101 = bf16[1024,128]{1,0:T(8,128)(2,1)} custom-call(bf16[64,2048]{1,0:T(8,128)(2,1)S(1)} %bitcast.49, bf16[2048,256]{1,0:T(8,128)(2,1)S(1)} %collective-permute-done.near, bf16[2048,256]{1,0:T(8,128)(2,1)} %collective-permute-done.1.up_a, bf16[256,2048]{1,0:T(8,128)(2,1)} %collective-permute-done.2.down_a, bf16[2048,256]{1,0:T(8,128)(2,1)} %bitcast.53, ...), custom_call_target="tpu_custom_call" | custom-call | tf_op jit(solution)/shard_map/pallas_call | solution.py:104
  51.2 0.0 copy-start.4
  51.2 5.0 %all-to-all-start.1 = ((bf16[64,16,128]{2,1,0:T(8,128)(2,1)}), bf16[64,16,128]{2,1,0:T(8,128)(2,1)S(1)}, u32[]{:S(2)}, u32[]{:S(2)}) async-start(bf16[64,16,128]{2,1,0:T(8,128)(2,1)} %bitcast.7), calls=%async_computation.1 | async-start | bytes 524288 | tf_op jit(solution)/shard_map/all_to_all | solution.py:215
  56.3 0.0 copy-done
  56.3 0.0 copy-done.4
  56.3 0.0 copy-start.6
  56.3 0.3 convolution_bitcast_fusion.1
  56.6 0.5 copy-done.6
  57.2 0.4 fusion.2
  57.5 11.2 %all-to-all-done.1 = bf16[64,16,128]{2,1,0:T(8,128)(2,1)S(1)} async-done(((bf16[64,16,128]{2,1,0:T(8,128)(2,1)}), bf16[64,16,128]{2,1,0:T(8,128)(2,1)S(1)}, u32[]{:S(2)}, u32[]{:S(2)}) %all-to-all-start.1) | async-done | bytes 262176 | tf_op jit(solution)/shard_map/all_to_all | solution.py:215
  68.8 0.1 copy.17
  68.9 0.0 copy-start.1
  68.9 24.7 %all_to_all.15.gathered = bf16[16,96,128]{2,1,0:T(8,128)(2,1)S(1)} all-to-all(bf16[16,96,128]{2,1,0:T(8,128)(2,1)S(1)} %pad_maximum_fusion), channel_id=1, replica_groups=mesh['z'=8,'y'=8,'x'=8,'core'=2] {'x','core'}, dimensions={0} | all-to-all | bytes 786432 | tf_op jit(solution)/shard_map/all_to_all | solution.py:229
  93.6 0.0 copy-done.1
  93.6 0.9 shard_map.102
  (6 shorter events, 0.1 us)
Async XLA Ops:
  0.0 56.3 %copy-start = (bf16[2048,32]{0,1:T(8,128)(2,1)S(1)}, bf16[2048,32]{0,1:T(8,128)(2,1)}, u32[]{:S(2)}) copy-start(bf16[2048,32]{0,1:T(8,128)(2,1)} %param.17) | copy-start | bytes 393220
  0.0 47.1 %collective-permute-start = (bf16[2048,256]{1,0:T(8,128)(2,1)}, bf16[2048,256]{1,0:T(8,128)(2,1)S(1)}, u32[]{:S(2)}, u32[]{:S(2)}) collective-permute-start(bf16[2048,256]{1,0:T(8,128)(2,1)} %bitcast.52), channel_id=1, source_target_pairs={{0,1},{1,0},{2,3},{3,2},{4,5},{5,4},{6,7},{7,6},{8,9},{9,8},{10,11... | collective-permute-start | bytes 3145736 | tf_op jit(solution)/shard_map/ppermute | solution.py:192
  16.2 30.9 %collective-permute-start.1 = (bf16[2048,256]{1,0:T(8,128)(2,1)}, bf16[2048,256]{1,0:T(8,128)(2,1)}, u32[]{:S(2)}, u32[]{:S(2)}) collective-permute-start(bf16[2048,256]{1,0:T(8,128)(2,1)} %bitcast.54), channel_id=1, source_target_pairs={{0,1},{1,0},{2,3},{3,2},{4,5},{5,4},{6,7},{7,6},{8,9},{9,8},{10,11... | collective-permute-start | bytes 3145736 | tf_op jit(solution)/shard_map/ppermute | solution.py:192
  18.1 29.0 %collective-permute-start.2 = (bf16[256,2048]{1,0:T(8,128)(2,1)}, bf16[256,2048]{1,0:T(8,128)(2,1)}, u32[]{:S(2)}, u32[]{:S(2)}) collective-permute-start(bf16[256,2048]{1,0:T(8,128)(2,1)} %bitcast.56), channel_id=1, source_target_pairs={{0,1},{1,0},{2,3},{3,2},{4,5},{5,4},{6,7},{7,6},{8,9},{9,8},{10,11... | collective-permute-start | bytes 3145736 | tf_op jit(solution)/shard_map/ppermute | solution.py:192
  20.5 12.9 %copy-start.2 = (bf16[128,2048]{1,0:T(8,128)(2,1)S(1)}, bf16[128,2048]{1,0:T(8,128)(2,1)}, u32[]{:S(2)}) copy-start(bf16[128,2048]{1,0:T(8,128)(2,1)} %far_tokens.1) | copy-start | bytes 1572868
  22.9 24.1 %all-to-all-start = ((bf16[64,16,128]{2,1,0:T(8,128)(2,1)}), bf16[64,16,128]{2,1,0:T(8,128)(2,1)S(1)}, u32[]{:S(2)}, u32[]{:S(2)}) async-start(bf16[64,16,128]{2,1,0:T(8,128)(2,1)} %bitcast.3), calls=%async_computation | async-start | bytes 524288 | tf_op jit(solution)/shard_map/all_to_all | solution.py:185
  33.4 0.7 copy-start.3
  34.1 0.7 copy-start.5
  51.2 5.1 %copy-start.4 = (f32[2048]{0:T(1024)S(1)}, f32[2048]{0:T(1024)}, u32[]{:S(2)}) copy-start(f32[2048]{0:T(1024)} %param.11) | copy-start | bytes 24580
  51.2 17.6 %all-to-all-start.1 = ((bf16[64,16,128]{2,1,0:T(8,128)(2,1)}), bf16[64,16,128]{2,1,0:T(8,128)(2,1)S(1)}, u32[]{:S(2)}, u32[]{:S(2)}) async-start(bf16[64,16,128]{2,1,0:T(8,128)(2,1)} %bitcast.7), calls=%async_computation.1 | async-start | bytes 524288 | tf_op jit(solution)/shard_map/all_to_all | solution.py:215
  56.3 0.9 copy-start.6
  68.9 24.7 %copy-start.1 = (bf16[512,128]{1,0:T(8,128)(2,1)S(1)}, bf16[512,128]{1,0:T(8,128)(2,1)}, u32[]{:S(2)}) copy-start(bf16[512,128]{1,0:T(8,128)(2,1)} %down.1) | copy-start | bytes 393220

commit v5 on v4

--- a/solution.py
+++ b/solution.py
@@ -21,12 +21,15 @@
     return lax.dot_general(a, b, (dims, ((), ())), preferred_element_type=jnp.float32)
 
 
-def row_major(value, scratch, out):
-    rows, width = value.shape
+def row_major(piece, width, scratch, out):
     block = out.shape[1]
     count = width // block
-    for b in range(count):
-        scratch[pl.ds(b, rows, stride=count), :] = value[:, b * block : (b + 1) * block]
+    rows = out.shape[0] // count
+    for first in range(0, count, 2):
+        value = piece(slice(first * block, (first + 2) * block))
+        for b in range(2):
+            here = value[:, b * block : (b + 1) * block]
+            scratch[pl.ds(first + b, rows, stride=count), :] = here
     out[...] = scratch[...].astype(jnp.bfloat16)
 
 
@@ -55,32 +58,37 @@
     square = jnp.sum(as_float * as_float, axis=1, keepdims=True) * (1.0 / width)
     copies[2].wait()
     normed = (as_float * lax.rsqrt(square + NORM_EPSILON) * gain[...]).astype(jnp.bfloat16)
-    row_major(dot(chosen, normed), wide, out)
-
-
-def expert_body(x, near, up_a, down_a, gate_b, up_b, down_b, out, wide, tall, flat, sems):
-    sources = (up_a, down_a, gate_b, up_b, down_b)
-    targets = (wide.at[0], tall.at[0], wide.at[1], wide.at[2], tall.at[1])
+    row_major(lambda span: dot(chosen, normed[:, span]), width, wide, out)
+
+
+def hidden_units(x, gate_a, up_a, gate_b, up_b, out, wide, sems):
+    sources = (up_a, gate_b, up_b)
     copies = [
-        pltpu.make_async_copy(sources[i], targets[i], sems.at[i]) for i in range(len(sources))
+        pltpu.make_async_copy(sources[i], wide.at[i], sems.at[i]) for i in range(len(sources))
     ]
     for copy in copies:
         copy.start()
-
-    def hidden(gated, lifted):
+    inner = wide.shape[2]
+
+    def acts(gated, lifted):
         return (gated / (1.0 + jnp.exp(-gated)) * lifted).astype(jnp.bfloat16)
 
-    gated = dot(x[...], near[...])
+    gated = dot(x[...], gate_a[...])
     copies[0].wait()
-    acts = hidden(gated, dot(x[...], wide[0]))
+    out[:, inner:] = acts(gated, dot(x[...], wide[0]))
     copies[1].wait()
-    total = dot(acts, tall[0])
+    gated = dot(x[...], wide[1])
     copies[2].wait()
-    gated = dot(x[...], wide[1])
-    copies[3].wait()
-    acts = hidden(gated, dot(x[...], wide[2]))
-    copies[4].wait()
-    row_major(total + dot(acts, tall[1]), flat, out)
+    out[:, :inner] = acts(gated, dot(x[...], wide[2]))
+
+
+def products(acts, down_a, down_b, out, flat):
+    inner = down_a.shape[0]
+
+    def piece(span):
+        return dot(acts[:, :inner], down_b[:, span]) + dot(acts[:, inner:], down_a[:, span])
+
+    row_major(piece, down_a.shape[1], flat, out)
 
 
 def finish(gathered, high, low, down, out):
@@ -88,11 +96,12 @@
     groups = high.shape[1] // tp_count
     values = jnp.concatenate([gathered[s, :groups] for s in range(tp_count)], axis=0)
     act = jnp.concatenate([gathered[s, groups:] for s in range(tp_count)], axis=0)
-    mixed = dot(high[...], values) + dot(low[...], values)
+    mixed = dot(jnp.concatenate([high[...], low[...]], axis=0), values)
+    mixed = mixed[: high.shape[0]] + mixed[high.shape[0] :]
     out[...] = (mixed + dot(act, down[...], ((0,), (0,)))).astype(jnp.bfloat16)
 
 
-def in_vmem(body, shape, *args, smem=0, anywhere=(), scratch=(), onward=False):
+def in_vmem(body, shape, *args, smem=0, anywhere=(), scratch=(), onward=False, room=12):
     specs = []
     args = list(args)
     for i in range(len(args)):
@@ -108,6 +117,7 @@
         out_specs=pl.BlockSpec(memory_space=pltpu.VMEM),
         scratch_shapes=list(scratch),
         interpret=INTERPRET,
+        compiler_params=pltpu.CompilerParams(vmem_limit_bytes=room << 20),
     )(*args)
 
 
@@ -193,24 +203,26 @@
     gates, ups, downs = halves
 
     inner = expert_gate.shape[2]
-    expert_out = in_vmem(
-        expert_body,
-        flat,
+    acts = in_vmem(
+        hidden_units,
+        (groups, 2 * inner),
         received.reshape(groups, width),
         gates[1],
         ups[1],
-        downs[1],
         gates[0],
         ups[0],
+        anywhere=range(2, 5),
+        onward=True,
+        scratch=(pltpu.VMEM((3, width, inner), jnp.bfloat16), pltpu.SemaphoreType.DMA((3,))),
+    )
+    expert_out = in_vmem(
+        products,
+        flat,
+        acts,
+        downs[1],
         downs[0],
-        anywhere=range(2, 7),
         onward=True,
-        scratch=(
-            pltpu.VMEM((3, width, inner), jnp.bfloat16),
-            pltpu.VMEM((2, inner, width), jnp.bfloat16),
-            pltpu.VMEM(flat, jnp.float32),
-            pltpu.SemaphoreType.DMA((5,)),
-        ),
+        scratch=(pltpu.VMEM(flat, jnp.float32),),
     )
     returned = lax.all_to_all(
         expert_out.reshape(groups, tp_count, block), EP, split_axis=0, concat_axis=0, tiled=True

time: 95 us -> 94.9 us (level)
    pallas_call x3 -> x4, Pallas kernels: 7.37 us -> 7.16 us  [in_vmem(): pl.pallas_call(body, out_shape=pltpu.VMEM(shape, jnp.bfloat16) if onward...]
  transfers between devices with their start and end apart: 5 -> 5, of which waited for: 2 -> 2; matrix products, arithmetic and copies ran while one was open for 2% -> 2% of each run, Pallas kernels for 2% -> 5%
where the time goes in v5:
time: 94.9 us; the launch traced here: 94.4 us
  starting transfers between devices  36.2 us (38%)
  blocking collectives  24.7 us (26%)
  waiting for transfers between devices  22.7 us (24%)
  Pallas kernels  7.16 us (8%)
  local copies, waits for them, and re-layouts  1.92 us (2%)
  matrix products  1.41 us (1%)
    all_to_all x1, blocking collectives, local(): lax.all_to_all(payload, TP, split_axis=0, concat_axis=0, tiled=True)  24.7 us
    ppermute x3, starting transfers between devices, local(): halves.append((half[0], lax.ppermute(half[0], 'core', swap)))  20.5 us
    all_to_all x1, waiting for transfers between devices, local(): lax.all_to_all(buffer.reshape(groups, tp_count, block), EP, split_axis=0,...  11.5 us
    all_to_all x1, waiting for transfers between devices, local(): lax.all_to_all(expert_out.reshape(groups, tp_count, block), EP, split_axi...  11.2 us
    all_to_all x1, starting transfers between devices, local(): lax.all_to_all(buffer.reshape(groups, tp_count, block), EP, split_axis=0,...  10.5 us
    pallas_call x4, Pallas kernels, in_vmem(): pl.pallas_call(body, out_shape=pltpu.VMEM(shape, jnp.bfloat16) if onward...  7.16 us
    all_to_all x1, starting transfers between devices, local(): lax.all_to_all(expert_out.reshape(groups, tp_count, block), EP, split_axi...  5.17 us
  transfers between devices with their start and end apart: 5, of which 2 were waited for; matrix products, arithmetic and copies ran while one was open for 2% of the time, Pallas kernels for 5%

profile of v5, /device:TPU:1, one launch (start us, length us, event | category | flops | bytes accessed | tf_op | source)
XLA Modules:
  0.0 94.4 jit_solution(1534870009445805263)
XLA Ops:
  0.0 0.0 copy-start
  0.0 16.1 %collective-permute-start = (bf16[2048,256]{1,0:T(8,128)(2,1)}, bf16[2048,256]{1,0:T(8,128)(2,1)S(1)}, u32[]{:S(2)}, u32[]{:S(2)}) collective-permute-start(bf16[2048,256]{1,0:T(8,128)(2,1)} %bitcast.52), channel_id=1, source_target_pairs={{0,1},{1,0},{2,3},{3,2},{4,5},{5,4},{6,7},{7,6},{8,9},{9,8},{10,11... | collective-permute-start | bytes 3145736 | tf_op jit(solution)/shard_map/ppermute | solution.py:202
  16.2 1.9 %collective-permute-start.1 = (bf16[2048,256]{1,0:T(8,128)(2,1)}, bf16[2048,256]{1,0:T(8,128)(2,1)}, u32[]{:S(2)}, u32[]{:S(2)}) collective-permute-start(bf16[2048,256]{1,0:T(8,128)(2,1)} %bitcast.54), channel_id=1, source_target_pairs={{0,1},{1,0},{2,3},{3,2},{4,5},{5,4},{6,7},{7,6},{8,9},{9,8},{10,11... | collective-permute-start | bytes 3145736 | tf_op jit(solution)/shard_map/ppermute | solution.py:202
  18.1 2.4 %collective-permute-start.2 = (bf16[256,2048]{1,0:T(8,128)(2,1)}, bf16[256,2048]{1,0:T(8,128)(2,1)S(1)}, u32[]{:S(2)}, u32[]{:S(2)}) collective-permute-start(bf16[256,2048]{1,0:T(8,128)(2,1)} %bitcast.49), channel_id=1, source_target_pairs={{0,1},{1,0},{2,3},{3,2},{4,5},{5,4},{6,7},{7,6},{8,9},{9,8},{10,11... | collective-permute-start | bytes 3145736 | tf_op jit(solution)/shard_map/ppermute | solution.py:202
  20.5 0.0 copy-start.3
  20.5 2.4 %shard_map.100 = bf16[1024,128]{1,0:T(8,128)(2,1)} custom-call(s32[1]{0:T(128)} %bitcast.place, s32[6,128]{1,0:T(8,128)} %bitcast.58, bf16[128,2048]{1,0:T(8,128)(2,1)} %far_tokens.1, f32[1,2048]{1,0:T(1,128)} %bitcast.59), custom_call_target="tpu_custom_call" | custom-call | tf_op jit(solution)/shard_map/pallas_call | solution.py:113
  22.9 10.5 %all-to-all-start = ((bf16[64,16,128]{2,1,0:T(8,128)(2,1)}), bf16[64,16,128]{2,1,0:T(8,128)(2,1)S(1)}, u32[]{:S(2)}, u32[]{:S(2)}) async-start(bf16[64,16,128]{2,1,0:T(8,128)(2,1)} %bitcast.3), calls=%async_computation | async-start | bytes 524288 | tf_op jit(solution)/shard_map/all_to_all | solution.py:195
  33.4 0.0 copy-done.3
  33.4 0.0 copy-start.4
  33.5 0.2 fusion.3
  33.6 0.5 copy-done.4
  34.1 0.0 copy-start.6
  34.1 0.7 copy-done.6
  34.8 0.7 fusion.6
  35.5 11.5 %all-to-all-done = bf16[64,16,128]{2,1,0:T(8,128)(2,1)S(1)} async-done(((bf16[64,16,128]{2,1,0:T(8,128)(2,1)}), bf16[64,16,128]{2,1,0:T(8,128)(2,1)S(1)}, u32[]{:S(2)}, u32[]{:S(2)}) %all-to-all-start) | async-done | bytes 262176 | tf_op jit(solution)/shard_map/all_to_all | solution.py:195
  47.0 0.1 copy.16
  47.1 0.0 collective-permute-done.gate_a
  47.1 0.0 collective-permute-done.1.up_a
  47.1 0.0 copy-start.1
  47.1 2.6 %shard_map.101.acts = bf16[64,512]{1,0:T(8,128)(2,1)S(1)} custom-call(bf16[64,2048]{1,0:T(8,128)(2,1)S(1)} %bitcast.51, bf16[2048,256]{1,0:T(8,128)(2,1)S(1)} %collective-permute-done.gate_a, bf16[2048,256]{1,0:T(8,128)(2,1)} %collective-permute-done.1.up_a, bf16[2048,256]{1,0:T(8,128)(2,1)} %bitcast.53, bf16[2048,256]{1,0:T(8,128)(2,1)} %bitcast.55), custom_call_target="tpu_custom_call" | custom-call | tf_op jit(solution)/shard_map/pallas_call | solution.py:113
  49.7 0.0 collective-permute-done.2.down_a
  49.8 0.0 copy-done.1
  49.8 1.2 %shard_map.102 = bf16[1024,128]{1,0:T(8,128)(2,1)} custom-call(bf16[64,512]{1,0:T(8,128)(2,1)S(1)} %shard_map.101.acts, bf16[256,2048]{1,0:T(8,128)(2,1)S(1)} %collective-permute-done.2.down_a, bf16[256,2048]{1,0:T(8,128)(2,1)S(1)} %bitcast.50), custom_call_target="tpu_custom_call" | custom-call | tf_op jit(solution)/shard_map/pallas_call | solution.py:113
  51.0 0.0 copy-start.5
  51.0 5.2 %all-to-all-start.1 = ((bf16[64,16,128]{2,1,0:T(8,128)(2,1)}), bf16[64,16,128]{2,1,0:T(8,128)(2,1)S(1)}, u32[]{:S(2)}, u32[]{:S(2)}) async-start(bf16[64,16,128]{2,1,0:T(8,128)(2,1)} %bitcast.7), calls=%async_computation.1 | async-start | bytes 524288 | tf_op jit(solution)/shard_map/all_to_all | solution.py:227
  56.2 0.0 copy-done
  56.2 0.0 copy-done.5
  56.2 0.0 copy-start.7
  56.2 0.3 convolution_bitcast_fusion.1
  56.6 0.5 copy-done.7
  57.1 0.4 fusion.2
  57.5 11.2 %all-to-all-done.1 = bf16[64,16,128]{2,1,0:T(8,128)(2,1)S(1)} async-done(((bf16[64,16,128]{2,1,0:T(8,128)(2,1)}), bf16[64,16,128]{2,1,0:T(8,128)(2,1)S(1)}, u32[]{:S(2)}, u32[]{:S(2)}) %all-to-all-start.1) | async-done | bytes 262176 | tf_op jit(solution)/shard_map/all_to_all | solution.py:227
  68.7 0.1 copy.17
  68.8 0.0 copy-start.2
  68.8 24.7 %all_to_all.15.gathered = bf16[16,96,128]{2,1,0:T(8,128)(2,1)S(1)} all-to-all(bf16[16,96,128]{2,1,0:T(8,128)(2,1)S(1)} %pad_maximum_fusion), channel_id=1, replica_groups=mesh['z'=8,'y'=8,'x'=8,'core'=2] {'x','core'}, dimensions={0} | all-to-all | bytes 786432 | tf_op jit(solution)/shard_map/all_to_all | solution.py:241
  93.5 0.0 copy-done.2
  93.5 0.9 shard_map.103
  (6 shorter events, 0.1 us)
Async XLA Ops:
  0.0 56.2 %copy-start = (bf16[2048,32]{0,1:T(8,128)(2,1)S(1)}, bf16[2048,32]{0,1:T(8,128)(2,1)}, u32[]{:S(2)}) copy-start(bf16[2048,32]{0,1:T(8,128)(2,1)} %param.17) | copy-start | bytes 393220
  0.0 47.1 %collective-permute-start = (bf16[2048,256]{1,0:T(8,128)(2,1)}, bf16[2048,256]{1,0:T(8,128)(2,1)S(1)}, u32[]{:S(2)}, u32[]{:S(2)}) collective-permute-start(bf16[2048,256]{1,0:T(8,128)(2,1)} %bitcast.52), channel_id=1, source_target_pairs={{0,1},{1,0},{2,3},{3,2},{4,5},{5,4},{6,7},{7,6},{8,9},{9,8},{10,11... | collective-permute-start | bytes 3145736 | tf_op jit(solution)/shard_map/ppermute | solution.py:202
  16.2 30.9 %collective-permute-start.1 = (bf16[2048,256]{1,0:T(8,128)(2,1)}, bf16[2048,256]{1,0:T(8,128)(2,1)}, u32[]{:S(2)}, u32[]{:S(2)}) collective-permute-start(bf16[2048,256]{1,0:T(8,128)(2,1)} %bitcast.54), channel_id=1, source_target_pairs={{0,1},{1,0},{2,3},{3,2},{4,5},{5,4},{6,7},{7,6},{8,9},{9,8},{10,11... | collective-permute-start | bytes 3145736 | tf_op jit(solution)/shard_map/ppermute | solution.py:202
  18.1 31.7 %collective-permute-start.2 = (bf16[256,2048]{1,0:T(8,128)(2,1)}, bf16[256,2048]{1,0:T(8,128)(2,1)S(1)}, u32[]{:S(2)}, u32[]{:S(2)}) collective-permute-start(bf16[256,2048]{1,0:T(8,128)(2,1)} %bitcast.49), channel_id=1, source_target_pairs={{0,1},{1,0},{2,3},{3,2},{4,5},{5,4},{6,7},{7,6},{8,9},{9,8},{10,11... | collective-permute-start | bytes 3145736 | tf_op jit(solution)/shard_map/ppermute | solution.py:202
  20.5 12.9 %copy-start.3 = (bf16[128,2048]{1,0:T(8,128)(2,1)S(1)}, bf16[128,2048]{1,0:T(8,128)(2,1)}, u32[]{:S(2)}) copy-start(bf16[128,2048]{1,0:T(8,128)(2,1)} %far_tokens.1) | copy-start | bytes 1572868
  22.9 24.1 %all-to-all-start = ((bf16[64,16,128]{2,1,0:T(8,128)(2,1)}), bf16[64,16,128]{2,1,0:T(8,128)(2,1)S(1)}, u32[]{:S(2)}, u32[]{:S(2)}) async-start(bf16[64,16,128]{2,1,0:T(8,128)(2,1)} %bitcast.3), calls=%async_computation | async-start | bytes 524288 | tf_op jit(solution)/shard_map/all_to_all | solution.py:195
  33.4 0.7 copy-start.4
  34.1 0.7 copy-start.6
  47.1 2.6 %copy-start.1 = (bf16[1,256,2048]{2,1,0:T(8,128)(2,1)S(1)}, bf16[1,256,2048]{2,1,0:T(8,128)(2,1)}, u32[]{:S(2)}) copy-start(bf16[1,256,2048]{2,1,0:T(8,128)(2,1)} %param.16) | copy-start | bytes 3145732
  51.0 5.2 %copy-start.5 = (f32[2048]{0:T(1024)S(1)}, f32[2048]{0:T(1024)}, u32[]{:S(2)}) copy-start(f32[2048]{0:T(1024)} %param.11) | copy-start | bytes 24580
  51.0 17.7 %all-to-all-start.1 = ((bf16[64,16,128]{2,1,0:T(8,128)(2,1)}), bf16[64,16,128]{2,1,0:T(8,128)(2,1)S(1)}, u32[]{:S(2)}, u32[]{:S(2)}) async-start(bf16[64,16,128]{2,1,0:T(8,128)(2,1)} %bitcast.7), calls=%async_computation.1 | async-start | bytes 524288 | tf_op jit(solution)/shard_map/all_to_all | solution.py:227
  56.2 0.9 copy-start.7
  68.8 24.7 %copy-start.2 = (bf16[512,128]{1,0:T(8,128)(2,1)S(1)}, bf16[512,128]{1,0:T(8,128)(2,1)}, u32[]{:S(2)}) copy-start(bf16[512,128]{1,0:T(8,128)(2,1)} %down.1) | copy-start | bytes 393220

commit v6 on v5

--- a/solution.py
+++ b/solution.py
@@ -91,17 +91,20 @@
     row_major(piece, down_a.shape[1], flat, out)
 
 
-def finish(gathered, high, low, down, out):
-    tp_count = gathered.shape[0]
-    groups = high.shape[1] // tp_count
-    values = jnp.concatenate([gathered[s, :groups] for s in range(tp_count)], axis=0)
-    act = jnp.concatenate([gathered[s, groups:] for s in range(tp_count)], axis=0)
+def share(partner, place, gathered, high, low, down, out):
+    core = place[0]
+    half = 1 - core if partner else core
+    columns = gathered.shape[0]
+    groups = high.shape[1] // columns
+    here = pl.ds(pl.multiple_of(half * groups, groups), groups)
+    values = jnp.concatenate([gathered[c, here] for c in range(columns)], axis=0)
+    act = jnp.concatenate([gathered[c, 2 * groups :] for c in range(columns)], axis=0)
     mixed = dot(jnp.concatenate([high[...], low[...]], axis=0), values)
     mixed = mixed[: high.shape[0]] + mixed[high.shape[0] :]
-    out[...] = (mixed + dot(act, down[...], ((0,), (0,)))).astype(jnp.bfloat16)
-
-
-def in_vmem(body, shape, *args, smem=0, anywhere=(), scratch=(), onward=False, room=12):
+    out[...] = mixed + dot(act, down[...], ((0,), (0,)))
+
+
+def in_vmem(body, shape, *args, dtype=jnp.bfloat16, smem=0, anywhere=(), scratch=(), onward=False, room=12):
     specs = []
     args = list(args)
     for i in range(len(args)):
@@ -109,10 +112,10 @@
         specs.append(pl.BlockSpec(memory_space=space))
         if i >= smem and not INTERPRET:
             args[i] = pltpu.with_memory_space_constraint(args[i], space)
-    out = jax.ShapeDtypeStruct(shape, jnp.bfloat16)
+    out = jax.ShapeDtypeStruct(shape, dtype)
     return pl.pallas_call(
         body,
-        out_shape=pltpu.VMEM(shape, jnp.bfloat16) if onward and not INTERPRET else out,
+        out_shape=pltpu.VMEM(shape, dtype) if onward and not INTERPRET else out,
         in_specs=specs,
         out_specs=pl.BlockSpec(memory_space=pltpu.VMEM),
         scratch_shapes=list(scratch),
@@ -123,8 +126,6 @@
 
 def late_work(tokens, norm_gain, expert_ids, route_weights, shared_gate, shared_up, groups):
     columns = lax.axis_size("x")
-    cores = lax.axis_size("core")
-    tp_count = columns * cores
     rows, top_count = expert_ids.shape
     as_float = tokens.astype(jnp.float32)
     inverse_rms = lax.rsqrt(jnp.mean(as_float * as_float, axis=-1, keepdims=True) + NORM_EPSILON)
@@ -137,17 +138,17 @@
     token_iota = jnp.arange(rows, dtype=jnp.int32)
     strict_lower = (token_iota[:, None] > token_iota[None, :]).astype(jnp.bfloat16)
 
-    slot_iota = jnp.arange(tp_count * groups, dtype=jnp.int32)
-    slot_expert = (slot_iota % groups) * columns + slot_iota // (groups * cores)
-    slot_number = (slot_iota // groups) % cores
-    weight = jnp.zeros((rows, tp_count * groups), jnp.float32)
-    taken = jnp.zeros((rows, tp_count * groups), jnp.bool_)
+    slot_iota = jnp.arange(columns * groups, dtype=jnp.int32)
+    slot_expert = (slot_iota % groups) * columns + slot_iota // groups
+    slot_number = lax.axis_index("core").astype(jnp.float32)
+    weight = jnp.zeros((rows, columns * groups), jnp.float32)
+    taken = jnp.zeros((rows, columns * groups), jnp.bool_)
     for k in range(top_count):
         hit = expert_ids[:, k : k + 1] == slot_expert[None, :]
         taken = taken | hit
         weight = jnp.where(hit, route_weights[:, k : k + 1], weight)
     ahead = dot(strict_lower, taken.astype(jnp.bfloat16))
-    weight = jnp.where(ahead == slot_number.astype(jnp.float32)[None, :], weight, 0.0)
+    weight = jnp.where(ahead == slot_number, weight, 0.0)
     high = lax.reduce_precision(weight, 8, 7)
     parts = (high.astype(jnp.bfloat16), (weight - high).astype(jnp.bfloat16))
     return shared_act, parts
@@ -168,6 +169,7 @@
     groups = lax.axis_size(EP)
     columns = lax.axis_size("x")
     cores = lax.axis_size("core")
+    core = lax.axis_index("core")
     rows, width = tokens.shape
     top_count = expert_ids.shape[1]
     tp_count = columns * cores
@@ -230,16 +232,40 @@
     shared_act, parts = late_work(
         tokens, norm_gain, expert_ids, route_weights, shared_gate, shared_up, groups
     )
+    by_core = shared_down.reshape(columns, cores, -1, block)
+    down_own, down_lent = (
+        lax.dynamic_index_in_dim(by_core, half, 1, keepdims=False).reshape(-1, block)
+        for half in (core, 1 - core)
+    )
+    down_borrowed = lax.ppermute(down_lent, "core", swap)
+
     payload = jnp.concatenate(
         [
-            jnp.swapaxes(returned, 0, 1),
-            jnp.broadcast_to(shared_act[None], (tp_count,) + shared_act.shape),
+            jnp.swapaxes(returned, 0, 1).reshape(columns, cores * groups, block),
+            jnp.broadcast_to(shared_act[None], (columns,) + shared_act.shape),
         ],
         axis=1,
     )
-    payload, *parts = lax.optimization_barrier((payload, *parts))
-    gathered = lax.all_to_all(payload, TP, split_axis=0, concat_axis=0, tiled=True)
-    return in_vmem(finish, (rows, block), gathered, *parts, shared_down)
+    payload, down_borrowed, *parts = lax.optimization_barrier((payload, down_borrowed, *parts))
+    gathered = lax.all_to_all(payload, "x", split_axis=0, concat_axis=0, tiled=True)
+    place = core[None]
+    halves = []
+    for partner, down in ((True, down_borrowed), (False, down_own)):
+        halves.append(
+            in_vmem(
+                functools.partial(share, partner),
+                (rows, block),
+                place,
+                gathered,
+                *parts,
+                down,
+                dtype=jnp.float32,
+                smem=1,
+                onward=True,
+            )
+        )
+    from_partner = lax.ppermute(halves[0], "core", swap)
+    return (halves[1] + from_partner).astype(jnp.bfloat16)
 
 
 def solution(mesh):

time: 94.9 us -> 95.2 us (level)
  starting transfers between devices: 36.2 us -> 51.7 us
  waiting for transfers between devices: 22.7 us -> 12.8 us
  blocking collectives: 24.7 us -> 16.3 us
  other arithmetic: 0.23 us -> 1.89 us
  local copies, waits for them, and re-layouts: 1.92 us -> 3.02 us
    all_to_all x1, starting transfers between devices: 10.5 us -> 24.4 us  [local(): lax.all_to_all(buffer.reshape(groups, tp_count, block), EP, split_axis=0,...]
    ppermute x3, starting transfers between devices: 20.5 us -> 7.2 us  [local(): halves.append((half[0], lax.ppermute(half[0], 'core', swap)))]
    all_to_all x1, waiting for transfers between devices: 11.5 us -> 0.46 us  [local(): lax.all_to_all(buffer.reshape(groups, tp_count, block), EP, split_axis=0,...]
    all_to_all x1, blocking collectives: 24.7 us -> 16.3 us  [local(): lax.all_to_all(payload, 'x', split_axis=0, concat_axis=0, tiled=True)]
    ppermute x0 -> x2, starting transfers between devices: none -> 8.15 us  [the longest x1 6.24 us: local(): from_partner = lax.ppermute(halves[0], 'core', swap)]
    all_to_all x1, starting transfers between devices: 5.17 us -> 12 us  [local(): lax.all_to_all(expert_out.reshape(groups, tp_count, block), EP, split_axi...]
    reduce_sum x1, other arithmetic: 0.19 us -> 1.23 us  [late_work(): jnp.mean(as_float * as_float, axis=-1, keepdims=True) + NORM_EPSILON]
    unnamed x17 -> x19, local copies, waits for them, and re-layouts: 1.82 us -> 2.26 us
  transfers between devices with their start and end apart: 5 -> 7, of which waited for: 2 -> 3; matrix products, arithmetic and copies ran while one was open for 2% -> 4% of each run, Pallas kernels for 5% -> 4%
where the time goes in v6:
time: 95.2 us; the launch traced here: 94.6 us
  starting transfers between devices  51.7 us (54%)
  blocking collectives  16.3 us (17%)
  waiting for transfers between devices  12.8 us (13%)
  Pallas kernels  7.5 us (8%)
  local copies, waits for them, and re-layouts  3.02 us (3%)
  other arithmetic  1.89 us (2%)
  matrix products  1.14 us (1%)
    all_to_all x1, starting transfers between devices, local(): lax.all_to_all(buffer.reshape(groups, tp_count, block), EP, split_axis=0,...  24.4 us
    all_to_all x1, blocking collectives, local(): lax.all_to_all(payload, 'x', split_axis=0, concat_axis=0, tiled=True)  16.3 us
    all_to_all x1, starting transfers between devices, local(): lax.all_to_all(expert_out.reshape(groups, tp_count, block), EP, split_axi...  12 us
    all_to_all x1, waiting for transfers between devices, local(): lax.all_to_all(expert_out.reshape(groups, tp_count, block), EP, split_axi...  11.7 us
    pallas_call x5, Pallas kernels, in_vmem(): pl.pallas_call(body, out_shape=pltpu.VMEM(shape, dtype) if onward and (no...  7.5 us
    ppermute x3, starting transfers between devices, local(): halves.append((half[0], lax.ppermute(half[0], 'core', swap)))  7.2 us
    ppermute x1, starting transfers between devices, local(): from_partner = lax.ppermute(halves[0], 'core', swap)  6.24 us
    unnamed x19, local copies, waits for them, and re-layouts  2.26 us
  transfers between devices with their start and end apart: 7, of which 3 were waited for; matrix products, arithmetic and copies ran while one was open for 4% of the time, Pallas kernels for 4%

profile of v6, /device:TPU:1, one launch (start us, length us, event | category | flops | bytes accessed | tf_op | source)
XLA Modules:
  0.0 94.6 jit_solution(16372179089075131985)
XLA Ops:
  0.0 0.0 copy-start
  0.0 0.0 copy-start.1
  0.0 2.4 %shard_map.100 = bf16[1024,128]{1,0:T(8,128)(2,1)} custom-call(s32[1]{0:T(128)} %bitcast.1.place, s32[6,128]{1,0:T(8,128)} %bitcast.67, bf16[128,2048]{1,0:T(8,128)(2,1)} %far_tokens.1, f32[1,2048]{1,0:T(1,128)} %bitcast.68), custom_call_target="tpu_custom_call" | custom-call | tf_op jit(solution)/shard_map/pallas_call | solution.py:116
  2.4 0.0 copy-start.4
  2.4 24.4 %all-to-all-start = ((bf16[64,16,128]{2,1,0:T(8,128)(2,1)}), bf16[64,16,128]{2,1,0:T(8,128)(2,1)}, u32[]{:S(2)}, u32[]{:S(2)}) async-start(bf16[64,16,128]{2,1,0:T(8,128)(2,1)} %bitcast.4), calls=%async_computation | async-start | bytes 524288 | tf_op jit(solution)/shard_map/all_to_all | solution.py:197
  26.8 2.9 %collective-permute-start = (bf16[2048,256]{1,0:T(8,128)(2,1)}, bf16[2048,256]{1,0:T(8,128)(2,1)S(1)}, u32[]{:S(2)}, u32[]{:S(2)}) collective-permute-start(bf16[2048,256]{1,0:T(8,128)(2,1)} %bitcast.60), channel_id=1, source_target_pairs={{0,1},{1,0},{2,3},{3,2},{4,5},{5,4},{6,7},{7,6},{8,9},{9,8},{10,11... | collective-permute-start | bytes 3145736 | tf_op jit(solution)/shard_map/ppermute | solution.py:204
  29.7 1.9 %collective-permute-start.1 = (bf16[2048,256]{1,0:T(8,128)(2,1)}, bf16[2048,256]{1,0:T(8,128)(2,1)}, u32[]{:S(2)}, u32[]{:S(2)}) collective-permute-start(bf16[2048,256]{1,0:T(8,128)(2,1)} %bitcast.62), channel_id=1, source_target_pairs={{0,1},{1,0},{2,3},{3,2},{4,5},{5,4},{6,7},{7,6},{8,9},{9,8},{10,11... | collective-permute-start | bytes 3145736 | tf_op jit(solution)/shard_map/ppermute | solution.py:204
  31.6 0.0 copy-done.1
  31.6 2.4 %collective-permute-start.2 = (bf16[256,2048]{1,0:T(8,128)(2,1)S(1)}, bf16[256,2048]{1,0:T(8,128)(2,1)S(1)}, u32[]{:S(2)}, u32[]{:S(2)}) collective-permute-start(bf16[256,2048]{1,0:T(8,128)(2,1)S(1)} %bitcast.56), channel_id=1, source_target_pairs={{0,1},{1,0},{2,3},{3,2},{4,5},{5,4},{6,7},{7,6},{8,9},{9,8},{10,11... | collective-permute-start | bytes 3145736 | tf_op jit(solution)/shard_map/ppermute | solution.py:204
  34.0 0.0 copy-done.4
  34.0 0.7 constant_dynamic-slice_fusion
  34.7 1.9 %collective-permute-start.3 = (bf16[256,128]{1,0:T(8,128)(2,1)}, bf16[256,128]{1,0:T(8,128)(2,1)}, u32[]{:S(2)}, u32[]{:S(2)}) collective-permute-start(bf16[256,128]{1,0:T(8,128)(2,1)} %bitcast.14), channel_id=1, source_target_pairs={{0,1},{1,0},{2,3},{3,2},{4,5},{5,4},{6,7},{7,6},{8,9},{9,8},{10,11... | collective-permute-start | bytes 196616 | tf_op jit(solution)/shard_map/ppermute | solution.py:240
  36.6 0.0 copy-start.5
  36.6 1.2 %fusion.3 = f32[128]{0:T(128)S(1)} fusion(bf16[128,2048]{1,0:T(8,128)(2,1)} %far_tokens.1), kind=kLoop, calls=%fused_computation.8 | loop fusion | flops 786304 | bytes 524800 | tf_op jit(solution)/shard_map/reduce_sum | solution.py:131
  37.9 0.0 copy-done.5
  37.9 0.0 copy-start.7
  37.9 0.7 copy-done.7
  38.6 0.4 fusion.6
  39.0 0.5 all-to-all-done
  39.5 1.0 %copy.21 = bf16[8,8,16,128]{3,1,2,0:T(8,128)(2,1)S(1)} copy(bf16[8,8,16,128]{3,2,1,0:T(8,128)(2,1)} %bitcast.32) | data formatting | bytes 524288
  40.5 0.0 collective-permute-done.gate_a
  40.5 0.0 collective-permute-done.1.up_a
  40.5 2.5 %shard_map.101.acts = bf16[64,512]{1,0:T(8,128)(2,1)S(1)} custom-call(bf16[64,2048]{1,0:T(8,128)(2,1)S(1)} %bitcast.58, bf16[2048,256]{1,0:T(8,128)(2,1)S(1)} %collective-permute-done.gate_a, bf16[2048,256]{1,0:T(8,128)(2,1)} %collective-permute-done.1.up_a, bf16[2048,256]{1,0:T(8,128)(2,1)} %bitcast.61, bf16[2048,256]{1,0:T(8,128)(2,1)} %bitcast.63), custom_call_target="tpu_custom_call" | custom-call | tf_op jit(solution)/shard_map/pallas_call | solution.py:116
  43.1 0.0 collective-permute-done.2.down_a
  43.1 0.0 copy-start.6
  43.1 1.2 %shard_map.102 = bf16[1024,128]{1,0:T(8,128)(2,1)} custom-call(bf16[64,512]{1,0:T(8,128)(2,1)S(1)} %shard_map.101.acts, bf16[256,2048]{1,0:T(8,128)(2,1)S(1)} %collective-permute-done.2.down_a, bf16[256,2048]{1,0:T(8,128)(2,1)S(1)} %bitcast.57), custom_call_target="tpu_custom_call" | custom-call | tf_op jit(solution)/shard_map/pallas_call | solution.py:116
  44.3 0.0 copy-start.3
  44.3 12.0 %all-to-all-start.1 = ((bf16[64,16,128]{2,1,0:T(8,128)(2,1)}), bf16[64,16,128]{2,1,0:T(8,128)(2,1)S(1)}, u32[]{:S(2)}, u32[]{:S(2)}) async-start(bf16[64,16,128]{2,1,0:T(8,128)(2,1)} %bitcast.8), calls=%async_computation.1 | async-start | bytes 524288 | tf_op jit(solution)/shard_map/all_to_all | solution.py:229
  56.3 0.0 copy-done
  56.4 0.0 copy-done.6
  56.4 0.0 copy-done.3
  56.4 0.0 copy-start.8
  56.4 0.3 convolution_bitcast_fusion.1
  56.7 0.5 copy-done.8
  57.3 0.4 fusion.2
  57.6 11.7 %all-to-all-done.1 = bf16[64,16,128]{2,1,0:T(8,128)(2,1)S(1)} async-done(((bf16[64,16,128]{2,1,0:T(8,128)(2,1)}), bf16[64,16,128]{2,1,0:T(8,128)(2,1)S(1)}, u32[]{:S(2)}, u32[]{:S(2)}) %all-to-all-start.1) | async-done | bytes 262176 | tf_op jit(solution)/shard_map/all_to_all | solution.py:229
  69.3 0.1 copy.14
  69.4 0.0 collective-permute-done.3.down
  69.4 16.3 %all_to_all.15.gathered = bf16[8,160,128]{2,1,0:T(8,128)(2,1)S(1)} all-to-all(bf16[8,160,128]{2,1,0:T(8,128)(2,1)S(1)} %pad_maximum_fusion), channel_id=1, replica_groups=mesh['z'=8,'y'=8,'x'=8,'core'=2] {'x'}, dimensions={0} | all-to-all | bytes 655360 | tf_op jit(solution)/shard_map/all_to_all | solution.py:250
  85.7 0.0 copy-start.2
  85.7 1.1 %shard_map.104 = f32[128,128]{1,0:T(8,128)S(1)} custom-call(s32[1]{0:T(128)} %bitcast.place, bf16[8,160,128]{2,1,0:T(8,128)(2,1)S(1)} %all_to_all.15.gathered, bf16[128,512]{1,0:T(8,128)(2,1)S(1)} %get-tuple-element.10.high, bf16[128,512]{1,0:T(8,128)(2,1)S(1)} %get-tuple-element.11.low, bf16[256,128]{1,0:T(8,128)(2,1)} %collective-permute-done.3.down), custom_call_target="tpu_custom_call" | custom-call | tf_op jit(solution)/shard_map/pallas_call | solution.py:116
  86.9 6.2 %collective-permute-start.4 = (f32[128,128]{1,0:T(8,128)S(1)}, f32[128,128]{1,0:T(8,128)S(1)}, u32[]{:S(2)}, u32[]{:S(2)}) collective-permute-start(f32[128,128]{1,0:T(8,128)S(1)} %shard_map.104), channel_id=1, source_target_pairs={{0,1},{1,0},{2,3},{3,2},{4,5},{5,4},{6,7},{7,6},{8,9},{9,8},{10,11... | collective-permute-start | bytes 196616 | tf_op jit(solution)/shard_map/ppermute | solution.py:267
  93.1 0.0 copy-done.2
  93.1 0.2 shard_map.103
  93.4 0.6 collective-permute-done.4
  94.0 0.6 add_convert_fusion
  (6 shorter events, 0.1 us)
Async XLA Ops:
  0.0 56.3 %copy-start = (bf16[2048,32]{0,1:T(8,128)(2,1)S(1)}, bf16[2048,32]{0,1:T(8,128)(2,1)}, u32[]{:S(2)}) copy-start(bf16[2048,32]{0,1:T(8,128)(2,1)} %param.17) | copy-start | bytes 393220
  0.0 31.6 %copy-start.1 = (bf16[1,256,2048]{2,1,0:T(8,128)(2,1)S(1)}, bf16[1,256,2048]{2,1,0:T(8,128)(2,1)}, u32[]{:S(2)}) copy-start(bf16[1,256,2048]{2,1,0:T(8,128)(2,1)} %param.16) | copy-start | bytes 3145732
  2.4 31.6 %copy-start.4 = (bf16[512,128]{1,0:T(8,128)(2,1)S(1)}, bf16[512,128]{1,0:T(8,128)(2,1)}, u32[]{:S(2)}) copy-start(bf16[512,128]{1,0:T(8,128)(2,1)} %param.19) | copy-start | bytes 393220
  2.4 37.0 %all-to-all-start = ((bf16[64,16,128]{2,1,0:T(8,128)(2,1)}), bf16[64,16,128]{2,1,0:T(8,128)(2,1)}, u32[]{:S(2)}, u32[]{:S(2)}) async-start(bf16[64,16,128]{2,1,0:T(8,128)(2,1)} %bitcast.4), calls=%async_computation | async-start | bytes 524288 | tf_op jit(solution)/shard_map/all_to_all | solution.py:197
  26.8 13.7 %collective-permute-start = (bf16[2048,256]{1,0:T(8,128)(2,1)}, bf16[2048,256]{1,0:T(8,128)(2,1)S(1)}, u32[]{:S(2)}, u32[]{:S(2)}) collective-permute-start(bf16[2048,256]{1,0:T(8,128)(2,1)} %bitcast.60), channel_id=1, source_target_pairs={{0,1},{1,0},{2,3},{3,2},{4,5},{5,4},{6,7},{7,6},{8,9},{9,8},{10,11... | collective-permute-start | bytes 3145736 | tf_op jit(solution)/shard_map/ppermute | solution.py:204
  29.7 10.8 %collective-permute-start.1 = (bf16[2048,256]{1,0:T(8,128)(2,1)}, bf16[2048,256]{1,0:T(8,128)(2,1)}, u32[]{:S(2)}, u32[]{:S(2)}) collective-permute-start(bf16[2048,256]{1,0:T(8,128)(2,1)} %bitcast.62), channel_id=1, source_target_pairs={{0,1},{1,0},{2,3},{3,2},{4,5},{5,4},{6,7},{7,6},{8,9},{9,8},{10,11... | collective-permute-start | bytes 3145736 | tf_op jit(solution)/shard_map/ppermute | solution.py:204
  31.6 11.4 %collective-permute-start.2 = (bf16[256,2048]{1,0:T(8,128)(2,1)S(1)}, bf16[256,2048]{1,0:T(8,128)(2,1)S(1)}, u32[]{:S(2)}, u32[]{:S(2)}) collective-permute-start(bf16[256,2048]{1,0:T(8,128)(2,1)S(1)} %bitcast.56), channel_id=1, source_target_pairs={{0,1},{1,0},{2,3},{3,2},{4,5},{5,4},{6,7},{7,6},{8,9},{9,8},{10,11... | collective-permute-start | bytes 3145736 | tf_op jit(solution)/shard_map/ppermute | solution.py:204
  34.7 34.7 %collective-permute-start.3 = (bf16[256,128]{1,0:T(8,128)(2,1)}, bf16[256,128]{1,0:T(8,128)(2,1)}, u32[]{:S(2)}, u32[]{:S(2)}) collective-permute-start(bf16[256,128]{1,0:T(8,128)(2,1)} %bitcast.14), channel_id=1, source_target_pairs={{0,1},{1,0},{2,3},{3,2},{4,5},{5,4},{6,7},{7,6},{8,9},{9,8},{10,11... | collective-permute-start | bytes 196616 | tf_op jit(solution)/shard_map/ppermute | solution.py:240
  36.6 1.2 %copy-start.5 = (s32[128,6]{0,1:T(8,128)S(1)}, s32[128,6]{0,1:T(8,128)}, u32[]{:S(2)}) copy-start(s32[128,6]{0,1:T(8,128)} %param.12) | copy-start | bytes 9220
  37.9 0.7 copy-start.7
  43.1 13.3 %copy-start.6 = (f32[2048]{0:T(1024)S(1)}, f32[2048]{0:T(1024)}, u32[]{:S(2)}) copy-start(f32[2048]{0:T(1024)} %param.11) | copy-start | bytes 24580
  44.3 12.1 %copy-start.3 = (bf16[128,2048]{1,0:T(8,128)(2,1)S(1)}, bf16[128,2048]{1,0:T(8,128)(2,1)}, u32[]{:S(2)}) copy-start(bf16[128,2048]{1,0:T(8,128)(2,1)} %far_tokens.1) | copy-start | bytes 1572868
  44.3 25.0 %all-to-all-start.1 = ((bf16[64,16,128]{2,1,0:T(8,128)(2,1)}), bf16[64,16,128]{2,1,0:T(8,128)(2,1)S(1)}, u32[]{:S(2)}, u32[]{:S(2)}) async-start(bf16[64,16,128]{2,1,0:T(8,128)(2,1)} %bitcast.8), calls=%async_computation.1 | async-start | bytes 524288 | tf_op jit(solution)/shard_map/all_to_all | solution.py:229
  56.4 0.9 copy-start.8
  85.7 7.4 %copy-start.2 = (bf16[8,1,32,128]{3,2,1,0:T(8,128)(2,1)S(1)}, bf16[8,1,32,128]{3,2,1,0:T(8,128)(2,1)}, u32[]{:S(2)}) copy-start(bf16[8,1,32,128]{3,2,1,0:T(8,128)(2,1)} %get-tuple-element.15) | copy-start | bytes 196612
  86.9 7.1 %collective-permute-start.4 = (f32[128,128]{1,0:T(8,128)S(1)}, f32[128,128]{1,0:T(8,128)S(1)}, u32[]{:S(2)}, u32[]{:S(2)}) collective-permute-start(f32[128,128]{1,0:T(8,128)S(1)} %shard_map.104), channel_id=1, source_target_pairs={{0,1},{1,0},{2,3},{3,2},{4,5},{5,4},{6,7},{7,6},{8,9},{9,8},{10,11... | collective-permute-start | bytes 196616 | tf_op jit(solution)/shard_map/ppermute | solution.py:267

commit v7 on v6

--- a/solution.py
+++ b/solution.py
@@ -33,7 +33,7 @@
     out[...] = scratch[...].astype(jnp.bfloat16)
 
 
-def pick_rows(columns, cores, place, far_ids, far_tokens, far_gain, out, ids, tokens, gain, wide, sems):
+def pick_rows(columns, cores, place, far_ids, far_tokens, far_gain, out, ids, tokens, gain, picked, wide, sems):
     pairs = ((far_ids, ids), (far_tokens, tokens), (far_gain, gain))
     copies = [pltpu.make_async_copy(*pairs[i], sems.at[i]) for i in range(len(pairs))]
     for copy in copies:
@@ -54,18 +54,22 @@
     before = dot(own.astype(jnp.bfloat16), jnp.where(sooner, 1.0, 0.0).astype(jnp.bfloat16))
     chosen = jnp.where(before == core.astype(jnp.float32), own, 0.0).astype(jnp.bfloat16)
     copies[1].wait()
-    as_float = tokens[...].astype(jnp.float32)
-    square = jnp.sum(as_float * as_float, axis=1, keepdims=True) * (1.0 / width)
+    step = 2 * out.shape[1]
+    spans = [slice(first, first + step) for first in range(0, width, step)]
+    squares = jnp.zeros((groups, step), jnp.float32)
+    for span in spans:
+        row = dot(chosen, tokens[:, span])
+        picked[:, span] = row
+        squares = squares + row * row
+    mean = jnp.sum(squares, axis=1, keepdims=True) * (1.0 / width)
+    scale = lax.rsqrt(mean + NORM_EPSILON)
     copies[2].wait()
-    normed = (as_float * lax.rsqrt(square + NORM_EPSILON) * gain[...]).astype(jnp.bfloat16)
-    row_major(lambda span: dot(chosen, normed[:, span]), width, wide, out)
-
-
-def hidden_units(x, gate_a, up_a, gate_b, up_b, out, wide, sems):
-    sources = (up_a, gate_b, up_b)
-    copies = [
-        pltpu.make_async_copy(sources[i], wide.at[i], sems.at[i]) for i in range(len(sources))
-    ]
+    row_major(lambda span: picked[:, span] * scale * gain[:, span], width, wide, out)
+
+
+def hidden_units(x, gate_a, up_a, gate_b, up_b, down_b, out, kept, wide, sems):
+    pairs = ((gate_b, wide.at[0]), (up_b, wide.at[1]), (down_b, kept))
+    copies = [pltpu.make_async_copy(*pairs[i], sems.at[i]) for i in range(len(pairs))]
     for copy in copies:
         copy.start()
     inner = wide.shape[2]
@@ -73,13 +77,12 @@
     def acts(gated, lifted):
         return (gated / (1.0 + jnp.exp(-gated)) * lifted).astype(jnp.bfloat16)
 
-    gated = dot(x[...], gate_a[...])
+    out[:, inner:] = acts(dot(x[...], gate_a[...]), dot(x[...], up_a[...]))
     copies[0].wait()
-    out[:, inner:] = acts(gated, dot(x[...], wide[0]))
+    gated = dot(x[...], wide[0])
     copies[1].wait()
-    gated = dot(x[...], wide[1])
+    out[:, :inner] = acts(gated, dot(x[...], wide[1]))
     copies[2].wait()
-    out[:, :inner] = acts(gated, dot(x[...], wide[2]))
 
 
 def products(acts, down_a, down_b, out, flat):
@@ -104,7 +107,7 @@
     out[...] = mixed + dot(act, down[...], ((0,), (0,)))
 
 
-def in_vmem(body, shape, *args, dtype=jnp.bfloat16, smem=0, anywhere=(), scratch=(), onward=False, room=12):
+def in_vmem(body, shape, *args, dtype=jnp.bfloat16, second=None, smem=0, anywhere=(), scratch=(), onward=False, room=12):
     specs = []
     args = list(args)
     for i in range(len(args)):
@@ -113,11 +116,16 @@
         if i >= smem and not INTERPRET:
             args[i] = pltpu.with_memory_space_constraint(args[i], space)
     out = jax.ShapeDtypeStruct(shape, dtype)
+    shapes = pltpu.VMEM(shape, dtype) if onward and not INTERPRET else out
+    out_specs = pl.BlockSpec(memory_space=pltpu.VMEM)
+    if second is not None:
+        more = jax.ShapeDtypeStruct(second, dtype) if INTERPRET else pltpu.VMEM(second, dtype)
+        shapes, out_specs = (shapes, more), (out_specs, out_specs)
     return pl.pallas_call(
         body,
-        out_shape=pltpu.VMEM(shape, dtype) if onward and not INTERPRET else out,
+        out_shape=shapes,
         in_specs=specs,
-        out_specs=pl.BlockSpec(memory_space=pltpu.VMEM),
+        out_specs=out_specs,
         scratch_shapes=list(scratch),
         interpret=INTERPRET,
         compiler_params=pltpu.CompilerParams(vmem_limit_bytes=room << 20),
@@ -190,6 +198,7 @@
             pltpu.VMEM((top_count, rows), jnp.int32),
             pltpu.VMEM((rows, width), jnp.bfloat16),
             pltpu.VMEM((1, width), jnp.float32),
+            pltpu.VMEM((groups, width), jnp.float32),
             pltpu.VMEM(flat, jnp.float32),
             pltpu.SemaphoreType.DMA((3,)),
         ),
@@ -205,7 +214,7 @@
     gates, ups, downs = halves
 
     inner = expert_gate.shape[2]
-    acts = in_vmem(
+    acts, down_kept = in_vmem(
         hidden_units,
         (groups, 2 * inner),
         received.reshape(groups, width),
@@ -213,22 +222,16 @@
         ups[1],
         gates[0],
         ups[0],
-        anywhere=range(2, 5),
+        downs[0],
+        second=(inner, width),
+        anywhere=range(3, 6),
         onward=True,
-        scratch=(pltpu.VMEM((3, width, inner), jnp.bfloat16), pltpu.SemaphoreType.DMA((3,))),
+        scratch=(pltpu.VMEM((2, width, inner), jnp.bfloat16), pltpu.SemaphoreType.DMA((3,))),
     )
     expert_out = in_vmem(
-        products,
-        flat,
-        acts,
-        downs[1],
-        downs[0],
-        onward=True,
-        scratch=(pltpu.VMEM(flat, jnp.float32),),
-    )
-    returned = lax.all_to_all(
-        expert_out.reshape(groups, tp_count, block), EP, split_axis=0, concat_axis=0, tiled=True
-    )
+        products, flat, acts, downs[1], down_kept, onward=True, scratch=(pltpu.VMEM(flat, jnp.float32),)
+    )
+    returned = lax.all_to_all(expert_out.reshape(groups, tp_count, block), EP, split_axis=0, concat_axis=0, tiled=True)
     shared_act, parts = late_work(
         tokens, norm_gain, expert_ids, route_weights, shared_gate, shared_up, groups
     )

time: 95.2 us -> 94.7 us (level)
    unnamed x19 -> x17, local copies, waits for them, and re-layouts: 2.26 us -> 2.26 us
where the time goes in v7:
time: 94.7 us; the launch traced here: 94.1 us
  starting transfers between devices  51.7 us (55%)
  blocking collectives  16.3 us (17%)
  waiting for transfers between devices  12.8 us (14%)
  Pallas kernels  7.02 us (7%)
  local copies, waits for them, and re-layouts  3.01 us (3%)
  other arithmetic  1.89 us (2%)
  matrix products  1.14 us (1%)
    all_to_all x1, starting transfers between devices, local(): lax.all_to_all(buffer.reshape(groups, tp_count, block), EP, split_axis=0,...  24.4 us
    all_to_all x1, blocking collectives, local(): lax.all_to_all(payload, 'x', split_axis=0, concat_axis=0, tiled=True)  16.3 us
    all_to_all x1, starting transfers between devices, local(): lax.all_to_all(expert_out.reshape(groups, tp_count, block), EP, split_axi...  12 us
    all_to_all x1, waiting for transfers between devices, local(): lax.all_to_all(expert_out.reshape(groups, tp_count, block), EP, split_axi...  11.7 us
    ppermute x3, starting transfers between devices, local(): halves.append((half[0], lax.ppermute(half[0], 'core', swap)))  7.2 us
    pallas_call x5, Pallas kernels, in_vmem(): pl.pallas_call(body, out_shape=shapes, in_specs=specs, out_specs=out_spec...  7.02 us
    ppermute x1, starting transfers between devices, local(): from_partner = lax.ppermute(halves[0], 'core', swap)  6.24 us
    unnamed x17, local copies, waits for them, and re-layouts  2.26 us
  transfers between devices with their start and end apart: 7, of which 3 were waited for; matrix products, arithmetic and copies ran while one was open for 4% of the time, Pallas kernels for 4%

profile of v7, /device:TPU:1, one launch (start us, length us, event | category | flops | bytes accessed | tf_op | source)
XLA Modules:
  0.0 94.1 jit_solution(11206874131045202446)
XLA Ops:
  0.0 0.0 copy-start
  0.0 2.3 %shard_map.100 = bf16[1024,128]{1,0:T(8,128)(2,1)} custom-call(s32[1]{0:T(128)} %bitcast.1.place, s32[6,128]{1,0:T(8,128)} %bitcast.63, bf16[128,2048]{1,0:T(8,128)(2,1)} %far_tokens.1, f32[1,2048]{1,0:T(1,128)} %bitcast.64), custom_call_target="tpu_custom_call" | custom-call | tf_op jit(solution)/shard_map/pallas_call | solution.py:124
  2.4 0.0 copy-start.3
  2.4 24.4 %all-to-all-start = ((bf16[64,16,128]{2,1,0:T(8,128)(2,1)}), bf16[64,16,128]{2,1,0:T(8,128)(2,1)}, u32[]{:S(2)}, u32[]{:S(2)}) async-start(bf16[64,16,128]{2,1,0:T(8,128)(2,1)} %bitcast.4), calls=%async_computation | async-start | bytes 524288 | tf_op jit(solution)/shard_map/all_to_all | solution.py:206
  26.7 2.9 %collective-permute-start = (bf16[2048,256]{1,0:T(8,128)(2,1)}, bf16[2048,256]{1,0:T(8,128)(2,1)S(1)}, u32[]{:S(2)}, u32[]{:S(2)}) collective-permute-start(bf16[2048,256]{1,0:T(8,128)(2,1)} %bitcast.5.gate_b), channel_id=1, source_target_pairs={{0,1},{1,0},{2,3},{3,2},{4,5},{5,4},{6,7},{7,6},{8,9},{9,8},{10,11... | collective-permute-start | bytes 3145736 | tf_op jit(solution)/shard_map/ppermute | solution.py:213
  29.6 1.9 %collective-permute-start.1 = (bf16[2048,256]{1,0:T(8,128)(2,1)}, bf16[2048,256]{1,0:T(8,128)(2,1)S(1)}, u32[]{:S(2)}, u32[]{:S(2)}) collective-permute-start(bf16[2048,256]{1,0:T(8,128)(2,1)} %bitcast.6.up_b), channel_id=1, source_target_pairs={{0,1},{1,0},{2,3},{3,2},{4,5},{5,4},{6,7},{7,6},{8,9},{9,8},{10,11... | collective-permute-start | bytes 3145736 | tf_op jit(solution)/shard_map/ppermute | solution.py:213
  31.5 2.4 %collective-permute-start.2 = (bf16[256,2048]{1,0:T(8,128)(2,1)}, bf16[256,2048]{1,0:T(8,128)(2,1)S(1)}, u32[]{:S(2)}, u32[]{:S(2)}) collective-permute-start(bf16[256,2048]{1,0:T(8,128)(2,1)} %bitcast.60), channel_id=1, source_target_pairs={{0,1},{1,0},{2,3},{3,2},{4,5},{5,4},{6,7},{7,6},{8,9},{9,8},{10,11... | collective-permute-start | bytes 3145736 | tf_op jit(solution)/shard_map/ppermute | solution.py:213
  34.0 0.0 copy-done.3
  34.0 0.7 constant_dynamic-slice_fusion
  34.6 1.9 %collective-permute-start.3 = (bf16[256,128]{1,0:T(8,128)(2,1)}, bf16[256,128]{1,0:T(8,128)(2,1)}, u32[]{:S(2)}, u32[]{:S(2)}) collective-permute-start(bf16[256,128]{1,0:T(8,128)(2,1)} %bitcast.14), channel_id=1, source_target_pairs={{0,1},{1,0},{2,3},{3,2},{4,5},{5,4},{6,7},{7,6},{8,9},{9,8},{10,11... | collective-permute-start | bytes 196616 | tf_op jit(solution)/shard_map/ppermute | solution.py:243
  36.5 0.0 copy-start.4
  36.6 1.2 %fusion.3 = f32[128]{0:T(128)S(1)} fusion(bf16[128,2048]{1,0:T(8,128)(2,1)} %far_tokens.1), kind=kLoop, calls=%fused_computation.8 | loop fusion | flops 786304 | bytes 524800 | tf_op jit(solution)/shard_map/reduce_sum | solution.py:139
  37.8 0.0 copy-done.4
  37.8 0.0 copy-start.6
  37.8 0.7 copy-done.6
  38.5 0.4 fusion.6
  38.9 0.5 all-to-all-done
  39.4 1.0 %copy.21 = bf16[8,8,16,128]{3,1,2,0:T(8,128)(2,1)S(1)} copy(bf16[8,8,16,128]{3,2,1,0:T(8,128)(2,1)} %bitcast.32) | data formatting | bytes 524288
  40.4 0.0 collective-permute-done.gate_a
  40.4 0.0 collective-permute-done.1.up_a
  40.4 2.1 %shard_map.101 = (bf16[64,512]{1,0:T(8,128)(2,1)S(1)}, bf16[256,2048]{1,0:T(8,128)(2,1)S(1)}) custom-call(bf16[64,2048]{1,0:T(8,128)(2,1)S(1)} %bitcast.56, bf16[2048,256]{1,0:T(8,128)(2,1)S(1)} %collective-permute-done.gate_a, bf16[2048,256]{1,0:T(8,128)(2,1)S(1)} %collective-permute-done.1.up_a, bf16[2048,256]{1,0:T(8,128)(2,1)} %bitcast.5.gate_b, ...), custom_call_target="tpu_custom_call" | custom-call | tf_op jit(solution)/shard_map/pallas_call | solution.py:124
  42.6 0.0 collective-permute-done.2.down_a
  42.6 0.0 copy-start.5
  42.6 1.2 %shard_map.102 = bf16[1024,128]{1,0:T(8,128)(2,1)} custom-call(bf16[64,512]{1,0:T(8,128)(2,1)S(1)} %get-tuple-element.11.acts, bf16[256,2048]{1,0:T(8,128)(2,1)S(1)} %collective-permute-done.2.down_a, bf16[256,2048]{1,0:T(8,128)(2,1)S(1)} %get-tuple-element.12.down_b), custom_call_target="tpu_custom_call" | custom-call | tf_op jit(solution)/shard_map/pallas_call | solution.py:124
  43.8 0.0 copy-start.2
  43.8 12.0 %all-to-all-start.1 = ((bf16[64,16,128]{2,1,0:T(8,128)(2,1)}), bf16[64,16,128]{2,1,0:T(8,128)(2,1)S(1)}, u32[]{:S(2)}, u32[]{:S(2)}) async-start(bf16[64,16,128]{2,1,0:T(8,128)(2,1)} %bitcast.8), calls=%async_computation.1 | async-start | bytes 524288 | tf_op jit(solution)/shard_map/all_to_all | solution.py:234
  55.8 0.0 copy-done
  55.9 0.0 copy-done.5
  55.9 0.0 copy-done.2
  55.9 0.0 copy-start.7
  55.9 0.3 convolution_bitcast_fusion.1
  56.2 0.5 copy-done.7
  56.8 0.4 fusion.2
  57.1 11.7 %all-to-all-done.1 = bf16[64,16,128]{2,1,0:T(8,128)(2,1)S(1)} async-done(((bf16[64,16,128]{2,1,0:T(8,128)(2,1)}), bf16[64,16,128]{2,1,0:T(8,128)(2,1)S(1)}, u32[]{:S(2)}, u32[]{:S(2)}) %all-to-all-start.1) | async-done | bytes 262176 | tf_op jit(solution)/shard_map/all_to_all | solution.py:234
  68.8 0.1 copy.14
  68.9 0.0 collective-permute-done.3.down
  68.9 16.3 %all_to_all.15.gathered = bf16[8,160,128]{2,1,0:T(8,128)(2,1)S(1)} all-to-all(bf16[8,160,128]{2,1,0:T(8,128)(2,1)S(1)} %pad_maximum_fusion), channel_id=1, replica_groups=mesh['z'=8,'y'=8,'x'=8,'core'=2] {'x'}, dimensions={0} | all-to-all | bytes 655360 | tf_op jit(solution)/shard_map/all_to_all | solution.py:253
  85.2 0.0 copy-start.1
  85.2 1.1 %shard_map.104 = f32[128,128]{1,0:T(8,128)S(1)} custom-call(s32[1]{0:T(128)} %bitcast.place, bf16[8,160,128]{2,1,0:T(8,128)(2,1)S(1)} %all_to_all.15.gathered, bf16[128,512]{1,0:T(8,128)(2,1)S(1)} %get-tuple-element.14.high, bf16[128,512]{1,0:T(8,128)(2,1)S(1)} %get-tuple-element.15.low, bf16[256,128]{1,0:T(8,128)(2,1)} %collective-permute-done.3.down), custom_call_target="tpu_custom_call" | custom-call | tf_op jit(solution)/shard_map/pallas_call | solution.py:124
  86.4 6.2 %collective-permute-start.4 = (f32[128,128]{1,0:T(8,128)S(1)}, f32[128,128]{1,0:T(8,128)S(1)}, u32[]{:S(2)}, u32[]{:S(2)}) collective-permute-start(f32[128,128]{1,0:T(8,128)S(1)} %shard_map.104), channel_id=1, source_target_pairs={{0,1},{1,0},{2,3},{3,2},{4,5},{5,4},{6,7},{7,6},{8,9},{9,8},{10,11... | collective-permute-start | bytes 196616 | tf_op jit(solution)/shard_map/ppermute | solution.py:270
  92.6 0.0 copy-done.1
  92.6 0.2 shard_map.103
  92.9 0.6 collective-permute-done.4
  93.5 0.6 add_convert_fusion
  (6 shorter events, 0.1 us)
Async XLA Ops:
  0.0 55.8 %copy-start = (bf16[2048,32]{0,1:T(8,128)(2,1)S(1)}, bf16[2048,32]{0,1:T(8,128)(2,1)}, u32[]{:S(2)}) copy-start(bf16[2048,32]{0,1:T(8,128)(2,1)} %param.17) | copy-start | bytes 393220
  2.4 31.6 %copy-start.3 = (bf16[512,128]{1,0:T(8,128)(2,1)S(1)}, bf16[512,128]{1,0:T(8,128)(2,1)}, u32[]{:S(2)}) copy-start(bf16[512,128]{1,0:T(8,128)(2,1)} %param.19) | copy-start | bytes 393220
  2.4 37.0 %all-to-all-start = ((bf16[64,16,128]{2,1,0:T(8,128)(2,1)}), bf16[64,16,128]{2,1,0:T(8,128)(2,1)}, u32[]{:S(2)}, u32[]{:S(2)}) async-start(bf16[64,16,128]{2,1,0:T(8,128)(2,1)} %bitcast.4), calls=%async_computation | async-start | bytes 524288 | tf_op jit(solution)/shard_map/all_to_all | solution.py:206
  26.7 13.7 %collective-permute-start = (bf16[2048,256]{1,0:T(8,128)(2,1)}, bf16[2048,256]{1,0:T(8,128)(2,1)S(1)}, u32[]{:S(2)}, u32[]{:S(2)}) collective-permute-start(bf16[2048,256]{1,0:T(8,128)(2,1)} %bitcast.5.gate_b), channel_id=1, source_target_pairs={{0,1},{1,0},{2,3},{3,2},{4,5},{5,4},{6,7},{7,6},{8,9},{9,8},{10,11... | collective-permute-start | bytes 3145736 | tf_op jit(solution)/shard_map/ppermute | solution.py:213
  29.6 10.8 %collective-permute-start.1 = (bf16[2048,256]{1,0:T(8,128)(2,1)}, bf16[2048,256]{1,0:T(8,128)(2,1)S(1)}, u32[]{:S(2)}, u32[]{:S(2)}) collective-permute-start(bf16[2048,256]{1,0:T(8,128)(2,1)} %bitcast.6.up_b), channel_id=1, source_target_pairs={{0,1},{1,0},{2,3},{3,2},{4,5},{5,4},{6,7},{7,6},{8,9},{9,8},{10,11... | collective-permute-start | bytes 3145736 | tf_op jit(solution)/shard_map/ppermute | solution.py:213
  31.5 11.0 %collective-permute-start.2 = (bf16[256,2048]{1,0:T(8,128)(2,1)}, bf16[256,2048]{1,0:T(8,128)(2,1)S(1)}, u32[]{:S(2)}, u32[]{:S(2)}) collective-permute-start(bf16[256,2048]{1,0:T(8,128)(2,1)} %bitcast.60), channel_id=1, source_target_pairs={{0,1},{1,0},{2,3},{3,2},{4,5},{5,4},{6,7},{7,6},{8,9},{9,8},{10,11... | collective-permute-start | bytes 3145736 | tf_op jit(solution)/shard_map/ppermute | solution.py:213
  34.6 34.3 %collective-permute-start.3 = (bf16[256,128]{1,0:T(8,128)(2,1)}, bf16[256,128]{1,0:T(8,128)(2,1)}, u32[]{:S(2)}, u32[]{:S(2)}) collective-permute-start(bf16[256,128]{1,0:T(8,128)(2,1)} %bitcast.14), channel_id=1, source_target_pairs={{0,1},{1,0},{2,3},{3,2},{4,5},{5,4},{6,7},{7,6},{8,9},{9,8},{10,11... | collective-permute-start | bytes 196616 | tf_op jit(solution)/shard_map/ppermute | solution.py:243
  36.5 1.2 %copy-start.4 = (s32[128,6]{0,1:T(8,128)S(1)}, s32[128,6]{0,1:T(8,128)}, u32[]{:S(2)}) copy-start(s32[128,6]{0,1:T(8,128)} %param.12) | copy-start | bytes 9220
  37.8 0.7 copy-start.6
  42.6 13.3 %copy-start.5 = (f32[2048]{0:T(1024)S(1)}, f32[2048]{0:T(1024)}, u32[]{:S(2)}) copy-start(f32[2048]{0:T(1024)} %param.11) | copy-start | bytes 24580
  43.8 12.1 %copy-start.2 = (bf16[128,2048]{1,0:T(8,128)(2,1)S(1)}, bf16[128,2048]{1,0:T(8,128)(2,1)}, u32[]{:S(2)}) copy-start(bf16[128,2048]{1,0:T(8,128)(2,1)} %far_tokens.1) | copy-start | bytes 1572868
  43.8 25.0 %all-to-all-start.1 = ((bf16[64,16,128]{2,1,0:T(8,128)(2,1)}), bf16[64,16,128]{2,1,0:T(8,128)(2,1)S(1)}, u32[]{:S(2)}, u32[]{:S(2)}) async-start(bf16[64,16,128]{2,1,0:T(8,128)(2,1)} %bitcast.8), calls=%async_computation.1 | async-start | bytes 524288 | tf_op jit(solution)/shard_map/all_to_all | solution.py:234
  55.9 0.9 copy-start.7
  85.2 7.4 %copy-start.1 = (bf16[8,1,32,128]{3,2,1,0:T(8,128)(2,1)S(1)}, bf16[8,1,32,128]{3,2,1,0:T(8,128)(2,1)}, u32[]{:S(2)}) copy-start(bf16[8,1,32,128]{3,2,1,0:T(8,128)(2,1)} %get-tuple-element.19) | copy-start | bytes 196612
  86.4 7.1 %collective-permute-start.4 = (f32[128,128]{1,0:T(8,128)S(1)}, f32[128,128]{1,0:T(8,128)S(1)}, u32[]{:S(2)}, u32[]{:S(2)}) collective-permute-start(f32[128,128]{1,0:T(8,128)S(1)} %shard_map.104), channel_id=1, source_target_pairs={{0,1},{1,0},{2,3},{3,2},{4,5},{5,4},{6,7},{7,6},{8,9},{9,8},{10,11... | collective-permute-start | bytes 196616 | tf_op jit(solution)/shard_map/ppermute | solution.py:270

commit v8 on v7

--- a/solution.py
+++ b/solution.py
@@ -21,7 +21,7 @@
     return lax.dot_general(a, b, (dims, ((), ())), preferred_element_type=jnp.float32)
 
 
-def row_major(piece, width, scratch, out):
+def row_major(piece, width, scratch, packed, out, sems):
     block = out.shape[1]
     count = width // block
     rows = out.shape[0] // count
@@ -30,10 +30,19 @@
         for b in range(2):
             here = value[:, b * block : (b + 1) * block]
             scratch[pl.ds(first + b, rows, stride=count), :] = here
-    out[...] = scratch[...].astype(jnp.bfloat16)
-
-
-def pick_rows(columns, cores, place, far_ids, far_tokens, far_gain, out, ids, tokens, gain, picked, wide, sems):
+    parts = sems.shape[0]
+    size = out.shape[0] // parts
+    copies = []
+    for i in range(parts):
+        span = pl.ds(i * size, size)
+        packed[span, :] = scratch[span, :].astype(jnp.bfloat16)
+        copies.append(pltpu.make_async_copy(packed.at[span], out.at[span], sems.at[i]))
+        copies[-1].start()
+    for copy in copies:
+        copy.wait()
+
+
+def pick_rows(columns, cores, place, far_ids, far_tokens, far_gain, out, ids, tokens, gain, picked, wide, packed, sems, out_sems):
     pairs = ((far_ids, ids), (far_tokens, tokens), (far_gain, gain))
     copies = [pltpu.make_async_copy(*pairs[i], sems.at[i]) for i in range(len(pairs))]
     for copy in copies:
@@ -64,7 +73,7 @@
     mean = jnp.sum(squares, axis=1, keepdims=True) * (1.0 / width)
     scale = lax.rsqrt(mean + NORM_EPSILON)
     copies[2].wait()
-    row_major(lambda span: picked[:, span] * scale * gain[:, span], width, wide, out)
+    row_major(lambda span: picked[:, span] * scale * gain[:, span], width, wide, packed, out, out_sems)
 
 
 def hidden_units(x, gate_a, up_a, gate_b, up_b, down_b, out, kept, wide, sems):
@@ -85,13 +94,13 @@
     copies[2].wait()
 
 
-def products(acts, down_a, down_b, out, flat):
+def products(acts, down_a, down_b, out, flat, packed, out_sems):
     inner = down_a.shape[0]
 
     def piece(span):
         return dot(acts[:, :inner], down_b[:, span]) + dot(acts[:, inner:], down_a[:, span])
 
-    row_major(piece, down_a.shape[1], flat, out)
+    row_major(piece, down_a.shape[1], flat, packed, out, out_sems)
 
 
 def share(partner, place, gathered, high, low, down, out):
@@ -107,7 +116,7 @@
     out[...] = mixed + dot(act, down[...], ((0,), (0,)))
 
 
-def in_vmem(body, shape, *args, dtype=jnp.bfloat16, second=None, smem=0, anywhere=(), scratch=(), onward=False, room=12):
+def in_vmem(body, shape, *args, dtype=jnp.bfloat16, second=None, smem=0, anywhere=(), scratch=(), onward=False, far=False, room=12):
     specs = []
     args = list(args)
     for i in range(len(args)):
@@ -117,7 +126,7 @@
             args[i] = pltpu.with_memory_space_constraint(args[i], space)
     out = jax.ShapeDtypeStruct(shape, dtype)
     shapes = pltpu.VMEM(shape, dtype) if onward and not INTERPRET else out
-    out_specs = pl.BlockSpec(memory_space=pltpu.VMEM)
+    out_specs = pl.BlockSpec(memory_space=pltpu.HBM if far else pltpu.VMEM)
     if second is not None:
         more = jax.ShapeDtypeStruct(second, dtype) if INTERPRET else pltpu.VMEM(second, dtype)
         shapes, out_specs = (shapes, more), (out_specs, out_specs)
@@ -193,14 +202,16 @@
         norm_gain[None],
         smem=1,
         anywhere=range(1, 4),
-        onward=True,
+        far=True,
         scratch=(
             pltpu.VMEM((top_count, rows), jnp.int32),
             pltpu.VMEM((rows, width), jnp.bfloat16),
             pltpu.VMEM((1, width), jnp.float32),
             pltpu.VMEM((groups, width), jnp.float32),
             pltpu.VMEM(flat, jnp.float32),
+            pltpu.VMEM(flat, jnp.bfloat16),
             pltpu.SemaphoreType.DMA((3,)),
+            pltpu.SemaphoreType.DMA((4,)),
         ),
     )
     received = lax.all_to_all(
@@ -229,7 +240,17 @@
         scratch=(pltpu.VMEM((2, width, inner), jnp.bfloat16), pltpu.SemaphoreType.DMA((3,))),
     )
     expert_out = in_vmem(
-        products, flat, acts, downs[1], down_kept, onward=True, scratch=(pltpu.VMEM(flat, jnp.float32),)
+        products,
+        flat,
+        acts,
+        downs[1],
+        down_kept,
+        far=True,
+        scratch=(
+            pltpu.VMEM(flat, jnp.float32),
+            pltpu.VMEM(flat, jnp.bfloat16),
+            pltpu.SemaphoreType.DMA((4,)),
+        ),
     )
     returned = lax.all_to_all(expert_out.reshape(groups, tp_count, block), EP, split_axis=0, concat_axis=0, tiled=True)
     shared_act, parts = late_work(

time: 94.7 us -> 94.8 us (level)
  no operation moved by 1% of the time
where the time goes in v8:
time: 94.8 us; the launch traced here: 94.2 us
  starting transfers between devices  51.7 us (55%)
  blocking collectives  16.3 us (17%)
  waiting for transfers between devices  12.8 us (14%)
  Pallas kernels  7.04 us (7%)
  local copies, waits for them, and re-layouts  3.01 us (3%)
  other arithmetic  1.89 us (2%)
  matrix products  1.14 us (1%)
    all_to_all x1, starting transfers between devices, local(): lax.all_to_all(buffer.reshape(groups, tp_count, block), EP, split_axis=0,...  24.4 us
    all_to_all x1, blocking collectives, local(): lax.all_to_all(payload, 'x', split_axis=0, concat_axis=0, tiled=True)  16.3 us
    all_to_all x1, starting transfers between devices, local(): lax.all_to_all(expert_out.reshape(groups, tp_count, block), EP, split_axi...  12 us
    all_to_all x1, waiting for transfers between devices, local(): lax.all_to_all(expert_out.reshape(groups, tp_count, block), EP, split_axi...  11.7 us
    ppermute x3, starting transfers between devices, local(): halves.append((half[0], lax.ppermute(half[0], 'core', swap)))  7.2 us
    pallas_call x5, Pallas kernels, in_vmem(): pl.pallas_call(body, out_shape=shapes, in_specs=specs, out_specs=out_spec...  7.04 us
    ppermute x1, starting transfers between devices, local(): from_partner = lax.ppermute(halves[0], 'core', swap)  6.24 us
    unnamed x17, local copies, waits for them, and re-layouts  2.26 us
  transfers between devices with their start and end apart: 7, of which 3 were waited for; matrix products, arithmetic and copies ran while one was open for 4% of the time, Pallas kernels for 4%

profile of v8, /device:TPU:1, one launch (start us, length us, event | category | flops | bytes accessed | tf_op | source)
XLA Modules:
  0.0 94.2 jit_solution(6226405852928353775)
XLA Ops:
  0.0 0.0 copy-start
  0.0 2.4 %shard_map.100 = bf16[1024,128]{1,0:T(8,128)(2,1)} custom-call(s32[1]{0:T(128)} %bitcast.1.place, s32[6,128]{1,0:T(8,128)} %bitcast.63, bf16[128,2048]{1,0:T(8,128)(2,1)} %far_tokens.1, f32[1,2048]{1,0:T(1,128)} %bitcast.64), custom_call_target="tpu_custom_call" | custom-call | tf_op jit(solution)/shard_map/pallas_call | solution.py:133
  2.4 0.0 copy-start.3
  2.4 24.4 %all-to-all-start = ((bf16[64,16,128]{2,1,0:T(8,128)(2,1)}), bf16[64,16,128]{2,1,0:T(8,128)(2,1)}, u32[]{:S(2)}, u32[]{:S(2)}) async-start(bf16[64,16,128]{2,1,0:T(8,128)(2,1)} %bitcast.4), calls=%async_computation | async-start | bytes 524288 | tf_op jit(solution)/shard_map/all_to_all | solution.py:217
  26.7 2.9 %collective-permute-start = (bf16[2048,256]{1,0:T(8,128)(2,1)}, bf16[2048,256]{1,0:T(8,128)(2,1)S(1)}, u32[]{:S(2)}, u32[]{:S(2)}) collective-permute-start(bf16[2048,256]{1,0:T(8,128)(2,1)} %bitcast.5.gate_b), channel_id=1, source_target_pairs={{0,1},{1,0},{2,3},{3,2},{4,5},{5,4},{6,7},{7,6},{8,9},{9,8},{10,11... | collective-permute-start | bytes 3145736 | tf_op jit(solution)/shard_map/ppermute | solution.py:224
  29.6 1.9 %collective-permute-start.1 = (bf16[2048,256]{1,0:T(8,128)(2,1)}, bf16[2048,256]{1,0:T(8,128)(2,1)S(1)}, u32[]{:S(2)}, u32[]{:S(2)}) collective-permute-start(bf16[2048,256]{1,0:T(8,128)(2,1)} %bitcast.6.up_b), channel_id=1, source_target_pairs={{0,1},{1,0},{2,3},{3,2},{4,5},{5,4},{6,7},{7,6},{8,9},{9,8},{10,11... | collective-permute-start | bytes 3145736 | tf_op jit(solution)/shard_map/ppermute | solution.py:224
  31.6 2.4 %collective-permute-start.2 = (bf16[256,2048]{1,0:T(8,128)(2,1)}, bf16[256,2048]{1,0:T(8,128)(2,1)S(1)}, u32[]{:S(2)}, u32[]{:S(2)}) collective-permute-start(bf16[256,2048]{1,0:T(8,128)(2,1)} %bitcast.60), channel_id=1, source_target_pairs={{0,1},{1,0},{2,3},{3,2},{4,5},{5,4},{6,7},{7,6},{8,9},{9,8},{10,11... | collective-permute-start | bytes 3145736 | tf_op jit(solution)/shard_map/ppermute | solution.py:224
  34.0 0.0 copy-done.3
  34.0 0.7 constant_dynamic-slice_fusion
  34.6 1.9 %collective-permute-start.3 = (bf16[256,128]{1,0:T(8,128)(2,1)}, bf16[256,128]{1,0:T(8,128)(2,1)}, u32[]{:S(2)}, u32[]{:S(2)}) collective-permute-start(bf16[256,128]{1,0:T(8,128)(2,1)} %bitcast.14), channel_id=1, source_target_pairs={{0,1},{1,0},{2,3},{3,2},{4,5},{5,4},{6,7},{7,6},{8,9},{9,8},{10,11... | collective-permute-start | bytes 196616 | tf_op jit(solution)/shard_map/ppermute | solution.py:264
  36.6 0.0 copy-start.4
  36.6 1.2 %fusion.3 = f32[128]{0:T(128)S(1)} fusion(bf16[128,2048]{1,0:T(8,128)(2,1)} %far_tokens.1), kind=kLoop, calls=%fused_computation.8 | loop fusion | flops 786304 | bytes 524800 | tf_op jit(solution)/shard_map/reduce_sum | solution.py:148
  37.8 0.0 copy-done.4
  37.8 0.0 copy-start.6
  37.8 0.7 copy-done.6
  38.5 0.4 fusion.6
  38.9 0.5 all-to-all-done
  39.4 1.0 %copy.21 = bf16[8,8,16,128]{3,1,2,0:T(8,128)(2,1)S(1)} copy(bf16[8,8,16,128]{3,2,1,0:T(8,128)(2,1)} %bitcast.32) | data formatting | bytes 524288
  40.4 0.0 collective-permute-done.gate_a
  40.5 0.0 collective-permute-done.1.up_a
  40.5 2.1 %shard_map.101 = (bf16[64,512]{1,0:T(8,128)(2,1)S(1)}, bf16[256,2048]{1,0:T(8,128)(2,1)S(1)}) custom-call(bf16[64,2048]{1,0:T(8,128)(2,1)S(1)} %bitcast.56, bf16[2048,256]{1,0:T(8,128)(2,1)S(1)} %collective-permute-done.gate_a, bf16[2048,256]{1,0:T(8,128)(2,1)S(1)} %collective-permute-done.1.up_a, bf16[2048,256]{1,0:T(8,128)(2,1)} %bitcast.5.gate_b, ...), custom_call_target="tpu_custom_call" | custom-call | tf_op jit(solution)/shard_map/pallas_call | solution.py:133
  42.6 0.0 collective-permute-done.2.down_a
  42.6 0.0 copy-start.5
  42.6 1.2 %shard_map.102 = bf16[1024,128]{1,0:T(8,128)(2,1)} custom-call(bf16[64,512]{1,0:T(8,128)(2,1)S(1)} %get-tuple-element.11.acts, bf16[256,2048]{1,0:T(8,128)(2,1)S(1)} %collective-permute-done.2.down_a, bf16[256,2048]{1,0:T(8,128)(2,1)S(1)} %get-tuple-element.12.down_b), custom_call_target="tpu_custom_call" | custom-call | tf_op jit(solution)/shard_map/pallas_call | solution.py:133
  43.8 0.0 copy-start.2
  43.9 12.0 %all-to-all-start.1 = ((bf16[64,16,128]{2,1,0:T(8,128)(2,1)}), bf16[64,16,128]{2,1,0:T(8,128)(2,1)S(1)}, u32[]{:S(2)}, u32[]{:S(2)}) async-start(bf16[64,16,128]{2,1,0:T(8,128)(2,1)} %bitcast.8), calls=%async_computation.1 | async-start | bytes 524288 | tf_op jit(solution)/shard_map/all_to_all | solution.py:255
  55.9 0.0 copy-done
  55.9 0.0 copy-done.5
  55.9 0.0 copy-done.2
  55.9 0.0 copy-start.7
  55.9 0.3 convolution_bitcast_fusion.1
  56.3 0.5 copy-done.7
  56.8 0.4 fusion.2
  57.2 11.7 %all-to-all-done.1 = bf16[64,16,128]{2,1,0:T(8,128)(2,1)S(1)} async-done(((bf16[64,16,128]{2,1,0:T(8,128)(2,1)}), bf16[64,16,128]{2,1,0:T(8,128)(2,1)S(1)}, u32[]{:S(2)}, u32[]{:S(2)}) %all-to-all-start.1) | async-done | bytes 262176 | tf_op jit(solution)/shard_map/all_to_all | solution.py:255
  68.8 0.1 copy.14
  69.0 0.0 collective-permute-done.3.down
  69.0 16.3 %all_to_all.15.gathered = bf16[8,160,128]{2,1,0:T(8,128)(2,1)S(1)} all-to-all(bf16[8,160,128]{2,1,0:T(8,128)(2,1)S(1)} %pad_maximum_fusion), channel_id=1, replica_groups=mesh['z'=8,'y'=8,'x'=8,'core'=2] {'x'}, dimensions={0} | all-to-all | bytes 655360 | tf_op jit(solution)/shard_map/all_to_all | solution.py:274
  85.3 0.0 copy-start.1
  85.3 1.1 %shard_map.104 = f32[128,128]{1,0:T(8,128)S(1)} custom-call(s32[1]{0:T(128)} %bitcast.place, bf16[8,160,128]{2,1,0:T(8,128)(2,1)S(1)} %all_to_all.15.gathered, bf16[128,512]{1,0:T(8,128)(2,1)S(1)} %get-tuple-element.14.high, bf16[128,512]{1,0:T(8,128)(2,1)S(1)} %get-tuple-element.15.low, bf16[256,128]{1,0:T(8,128)(2,1)} %collective-permute-done.3.down), custom_call_target="tpu_custom_call" | custom-call | tf_op jit(solution)/shard_map/pallas_call | solution.py:133
  86.4 6.2 %collective-permute-start.4 = (f32[128,128]{1,0:T(8,128)S(1)}, f32[128,128]{1,0:T(8,128)S(1)}, u32[]{:S(2)}, u32[]{:S(2)}) collective-permute-start(f32[128,128]{1,0:T(8,128)S(1)} %shard_map.104), channel_id=1, source_target_pairs={{0,1},{1,0},{2,3},{3,2},{4,5},{5,4},{6,7},{7,6},{8,9},{9,8},{10,11... | collective-permute-start | bytes 196616 | tf_op jit(solution)/shard_map/ppermute | solution.py:291
  92.7 0.0 copy-done.1
  92.7 0.2 shard_map.103
  92.9 0.6 collective-permute-done.4
  93.5 0.6 add_convert_fusion
  (6 shorter events, 0.1 us)
Async XLA Ops:
  0.0 55.9 %copy-start = (bf16[2048,32]{0,1:T(8,128)(2,1)S(1)}, bf16[2048,32]{0,1:T(8,128)(2,1)}, u32[]{:S(2)}) copy-start(bf16[2048,32]{0,1:T(8,128)(2,1)} %param.17) | copy-start | bytes 393220
  2.4 31.6 %copy-start.3 = (bf16[512,128]{1,0:T(8,128)(2,1)S(1)}, bf16[512,128]{1,0:T(8,128)(2,1)}, u32[]{:S(2)}) copy-start(bf16[512,128]{1,0:T(8,128)(2,1)} %param.19) | copy-start | bytes 393220
  2.4 37.0 %all-to-all-start = ((bf16[64,16,128]{2,1,0:T(8,128)(2,1)}), bf16[64,16,128]{2,1,0:T(8,128)(2,1)}, u32[]{:S(2)}, u32[]{:S(2)}) async-start(bf16[64,16,128]{2,1,0:T(8,128)(2,1)} %bitcast.4), calls=%async_computation | async-start | bytes 524288 | tf_op jit(solution)/shard_map/all_to_all | solution.py:217
  26.7 13.7 %collective-permute-start = (bf16[2048,256]{1,0:T(8,128)(2,1)}, bf16[2048,256]{1,0:T(8,128)(2,1)S(1)}, u32[]{:S(2)}, u32[]{:S(2)}) collective-permute-start(bf16[2048,256]{1,0:T(8,128)(2,1)} %bitcast.5.gate_b), channel_id=1, source_target_pairs={{0,1},{1,0},{2,3},{3,2},{4,5},{5,4},{6,7},{7,6},{8,9},{9,8},{10,11... | collective-permute-start | bytes 3145736 | tf_op jit(solution)/shard_map/ppermute | solution.py:224
  29.6 10.8 %collective-permute-start.1 = (bf16[2048,256]{1,0:T(8,128)(2,1)}, bf16[2048,256]{1,0:T(8,128)(2,1)S(1)}, u32[]{:S(2)}, u32[]{:S(2)}) collective-permute-start(bf16[2048,256]{1,0:T(8,128)(2,1)} %bitcast.6.up_b), channel_id=1, source_target_pairs={{0,1},{1,0},{2,3},{3,2},{4,5},{5,4},{6,7},{7,6},{8,9},{9,8},{10,11... | collective-permute-start | bytes 3145736 | tf_op jit(solution)/shard_map/ppermute | solution.py:224
  31.6 11.0 %collective-permute-start.2 = (bf16[256,2048]{1,0:T(8,128)(2,1)}, bf16[256,2048]{1,0:T(8,128)(2,1)S(1)}, u32[]{:S(2)}, u32[]{:S(2)}) collective-permute-start(bf16[256,2048]{1,0:T(8,128)(2,1)} %bitcast.60), channel_id=1, source_target_pairs={{0,1},{1,0},{2,3},{3,2},{4,5},{5,4},{6,7},{7,6},{8,9},{9,8},{10,11... | collective-permute-start | bytes 3145736 | tf_op jit(solution)/shard_map/ppermute | solution.py:224
  34.6 34.3 %collective-permute-start.3 = (bf16[256,128]{1,0:T(8,128)(2,1)}, bf16[256,128]{1,0:T(8,128)(2,1)}, u32[]{:S(2)}, u32[]{:S(2)}) collective-permute-start(bf16[256,128]{1,0:T(8,128)(2,1)} %bitcast.14), channel_id=1, source_target_pairs={{0,1},{1,0},{2,3},{3,2},{4,5},{5,4},{6,7},{7,6},{8,9},{9,8},{10,11... | collective-permute-start | bytes 196616 | tf_op jit(solution)/shard_map/ppermute | solution.py:264
  36.6 1.2 %copy-start.4 = (s32[128,6]{0,1:T(8,128)S(1)}, s32[128,6]{0,1:T(8,128)}, u32[]{:S(2)}) copy-start(s32[128,6]{0,1:T(8,128)} %param.12) | copy-start | bytes 9220
  37.8 0.7 copy-start.6
  42.6 13.3 %copy-start.5 = (f32[2048]{0:T(1024)S(1)}, f32[2048]{0:T(1024)}, u32[]{:S(2)}) copy-start(f32[2048]{0:T(1024)} %param.11) | copy-start | bytes 24580
  43.8 12.1 %copy-start.2 = (bf16[128,2048]{1,0:T(8,128)(2,1)S(1)}, bf16[128,2048]{1,0:T(8,128)(2,1)}, u32[]{:S(2)}) copy-start(bf16[128,2048]{1,0:T(8,128)(2,1)} %far_tokens.1) | copy-start | bytes 1572868
  43.9 25.0 %all-to-all-start.1 = ((bf16[64,16,128]{2,1,0:T(8,128)(2,1)}), bf16[64,16,128]{2,1,0:T(8,128)(2,1)S(1)}, u32[]{:S(2)}, u32[]{:S(2)}) async-start(bf16[64,16,128]{2,1,0:T(8,128)(2,1)} %bitcast.8), calls=%async_computation.1 | async-start | bytes 524288 | tf_op jit(solution)/shard_map/all_to_all | solution.py:255
  55.9 0.9 copy-start.7
  85.3 7.4 %copy-start.1 = (bf16[8,1,32,128]{3,2,1,0:T(8,128)(2,1)S(1)}, bf16[8,1,32,128]{3,2,1,0:T(8,128)(2,1)}, u32[]{:S(2)}) copy-start(bf16[8,1,32,128]{3,2,1,0:T(8,128)(2,1)} %get-tuple-element.19) | copy-start | bytes 196612
  86.4 7.1 %collective-permute-start.4 = (f32[128,128]{1,0:T(8,128)S(1)}, f32[128,128]{1,0:T(8,128)S(1)}, u32[]{:S(2)}, u32[]{:S(2)}) collective-permute-start(f32[128,128]{1,0:T(8,128)S(1)} %shard_map.104), channel_id=1, source_target_pairs={{0,1},{1,0},{2,3},{3,2},{4,5},{5,4},{6,7},{7,6},{8,9},{9,8},{10,11... | collective-permute-start | bytes 196616 | tf_op jit(solution)/shard_map/ppermute | solution.py:291
